TPU v7x, 32 devices: a whole 2x2x4 slice. The times are simulated.
32 devices in a mesh: grp: 2 (over x), ep: 8 (over z, y), tp: 2 (over core).
Axes of the slice: x: 2, y: 2, z: 4, core: 2. Of those that a mesh axis runs over, the one named last changes fastest.
Arguments:
- tokens: bfloat16 [1024, 2048], P(('grp', 'ep')), parts along dimension 0, may hold values from -6 to 6
- routes: int32 [1024, 4], P(('grp', 'ep')), parts along dimension 0, may hold values from 0 to 7, all different within a row; in each aligned block of 64 rows (0 to 63, 64 to 127, ...) at most 64 rows name the same one
- gate_weights: float32 [1024, 4], P(('grp', 'ep')), parts along dimension 0, may hold values from 0.05 to 1
- w_gate: bfloat16 [8, 2048, 1280], P('ep', None, 'tp'), may hold values from -0.125 to 0.125
- w_up: bfloat16 [8, 2048, 1280], P('ep', None, 'tp'), may hold values from -0.125 to 0.125
- w_down: bfloat16 [8, 1280, 2048], P('ep', 'tp'), may hold values from -0.15625 to 0.15625
- norm_gain: float32 [2048], P('tp'), may hold values from 0.1 to 1.9
- norm_bias: float32 [2048], P('tp'), may hold values from -2 to 2
Outputs:
- normed: bfloat16 [1024, 2048], P(('grp', 'ep'), 'tp'), parts along dimension 0
There are 2 independent parts, one for each index of `grp`. A program takes and returns all parts, laid end to end along the dimension named above; an argument that names none is the same for every part. Nothing has to cross between parts.
Inputs may be any that keep to these rules, and one draw needn't show every extreme that they name: `routes`: the rows of a token name distinct experts; in each aligned block of 64 rows (the tokens of one index of ep) no expert is named more than 64 times, a bound that some block reaches.
All inputs are finite; a program needn't handle non-finite values.
Results may differ from a plain program's by a relative error of at most 0.0037.
Values may be sent and summed in bfloat16 or wider, within the bound.
No kernel may reach another device: no remote copies, remote signals or barrier semaphores. Data moves between devices by JAX's collectives and lax.ppermute only.
A program may use at most 64 MiB of HBM per device.

v0:
```python
import jax
import jax.numpy as jnp
from jax import lax
from jax.sharding import PartitionSpec as P

residual_scale = 1.4142135
norm_eps = 1e-05


def shards(tokens, routes, gate_weights, w_gate, w_up, w_down, norm_gain, norm_bias):
    num_ep = lax.axis_size("ep")
    num_tp = lax.axis_size("tp")
    tp_index = lax.axis_index("tp")
    tok_rows, width = tokens.shape
    top_count = routes.shape[1]
    experts = num_ep * w_gate.shape[0]
    capacity = 2 * tok_rows * top_count // experts
    half_width = width // num_tp
    pair_list = routes.reshape(-1)
    onehot = (pair_list[:, None] == jnp.arange(experts, dtype=jnp.int32)).astype(jnp.int32)
    slots = jnp.sum((jnp.cumsum(onehot, axis=0) - onehot) * onehot, axis=1)
    target = pair_list * capacity + slots
    placing = jnp.arange(experts * capacity, dtype=jnp.int32)[:, None] == target[None, :]
    placing = jnp.sum(
        placing.reshape(experts * capacity, tok_rows, top_count).astype(jnp.float32), axis=2
    )
    placing = placing.astype(jnp.bfloat16)
    own_half = lax.dynamic_slice_in_dim(tokens, tp_index * half_width, half_width, 1)
    outgoing = jnp.dot(placing, own_half, preferred_element_type=jnp.float32).astype(jnp.bfloat16)
    arrived = lax.all_to_all(outgoing, "ep", split_axis=0, concat_axis=0, tiled=True)
    received = lax.all_gather(arrived, "tp", axis=1, tiled=True)
    gate = jnp.dot(received, w_gate[0], preferred_element_type=jnp.float32)
    upper = jnp.dot(received, w_up[0], preferred_element_type=jnp.float32)
    hidden = (jax.nn.silu(gate) * upper).astype(jnp.bfloat16)
    partial_sum = jnp.dot(hidden, w_down[0], preferred_element_type=jnp.float32).astype(
        jnp.bfloat16
    )
    expert_out = (
        lax.psum_scatter(partial_sum, "tp", scatter_dimension=1, tiled=True)
        .astype(jnp.float32)
        .astype(jnp.bfloat16)
    )
    came_back = lax.all_to_all(expert_out, "ep", split_axis=0, concat_axis=0, tiled=True)
    chosen = came_back[target].astype(jnp.float32).reshape(tok_rows, top_count, half_width)
    mixture = jnp.sum(gate_weights[:, :, None] * chosen, axis=1).astype(jnp.bfloat16)
    own_tokens = lax.dynamic_slice_in_dim(tokens, tp_index * half_width, half_width, 1)
    summed = residual_scale * own_tokens.astype(jnp.float32) + mixture.astype(jnp.float32)
    row_sum, row_squares = lax.psum(
        (jnp.sum(summed, axis=1), jnp.sum(summed * summed, axis=1)), "tp"
    )
    mean = row_sum / width
    variance = row_squares / width - mean * mean
    normed = (summed - mean[:, None]) * lax.rsqrt(
        variance[:, None] + norm_eps
    ) * norm_gain + norm_bias
    return normed.astype(jnp.bfloat16)


def solution(mesh):
    in_specs = (
        P(("grp", "ep"), None),
        P(("grp", "ep"), None),
        P(("grp", "ep"), None),
        P("ep", None, "tp"),
        P("ep", None, "tp"),
        P("ep", "tp", None),
        P("tp"),
        P("tp"),
    )
    out_specs = P(("grp", "ep"), "tp")
    return jax.shard_map(shards, mesh=mesh, in_specs=in_specs, out_specs=out_specs, check_vma=False)
```

profile of v0, /device:TPU:0, one launch (start us, length us, event | category | flops | bytes accessed | tf_op | source)
XLA Modules:
  0.0 125.9 jit_solution(16409182615999726836)
XLA Ops:
  6.5 0.9 copy.16
  7.5 0.1 eq.44
  7.6 0.1 eq.40
  7.7 0.6 reduce-window.6
  8.3 0.2 slice_reduce_fusion
  8.5 0.1 fusion.18
  8.6 0.1 reduce_sum.50
  8.8 0.1 convert_reduce_fusion
  9.0 1.4 %convolution_convert_fusion.1 = bf16[512,1024]{1,0:T(8,128)(2,1)S(1)} fusion(bf16[64,2048]{1,0:T(8,128)(2,1)} %param.8, s32[]{:T(128)S(6)} %select_n.14, bf16[512,64]{0,1:T(8,128)(2,1)S(1)} %convert_reduce_fusion), kind=kOutput, calls=%fused_computation.7 | convolution fusion | flops 67633152 | bytes 1245188 | tf_op jit(solution)/shard_map/dot_general | solution.py:29
  10.3 33.0 %all_to_all.24 = bf16[8,64,1024]{2,1,0:T(8,128)(2,1)} all-to-all(bf16[8,64,1024]{2,1,0:T(8,128)(2,1)S(1)} %bitcast.33), channel_id=1, replica_groups=mesh['grp'=2,'ep'=8,'tp'=2] {'ep'}, dimensions={0} | all-to-all | bytes 2097152 | tf_op jit(solution)/shard_map/all_to_all | solution.py:30
  43.4 9.7 %all-gather.2.cloned.1.call-done = bf16[512,2048]{1,0:T(8,128)(2,1)} async-done(((bf16[512,1024]{1,0:T(8,128)(2,1)}), bf16[512,2048]{1,0:T(8,128)(2,1)}) %all-gather.2.cloned.1.call-update) | async-done | bytes 2097168 | tf_op jit(solution)/shard_map/all_gather | solution.py:31
  53.1 5.2 %fusion.3 = f32[512,640]{1,0:T(8,128)} fusion(bf16[512,2048]{1,0:T(8,128)(2,1)} %all-gather.2.cloned.1.call-done, bf16[1,2048,640]{2,1,0:T(8,128)(2,1)} %param.11), kind=kOutput, calls=%fused_computation.5 | convolution fusion | flops 1342177280 | bytes 6029312 | tf_op jit(solution)/shard_map/dot_general | solution.py:32
  58.3 8.0 %convolution_convert_fusion = bf16[512,2048]{1,0:T(8,128)(2,1)} fusion(bf16[1,640,2048]{2,1,0:T(8,128)(2,1)S(1)} %copy-done, bf16[512,2048]{1,0:T(8,128)(2,1)} %all-gather.2.cloned.1.call-done, bf16[1,2048,640]{2,1,0:T(8,128)(2,1)} %param.12, f32[512,640]{1,0:T(8,128)} %fusion.3), kind=kOutput, calls=%fused_computation.1 | convolution fusion | flops 2687369216 | bytes 10747904 | tf_op jit(solution)/shard_map/dot_general | solution.py:35
  66.3 11.0 %reduce-scatter.2.cloned.1.call-done = bf16[512,1024]{1,0:T(8,128)(2,1)} async-done(((bf16[512,2048]{1,0:T(8,128)(2,1)}), bf16[512,1024]{1,0:T(8,128)(2,1)}) %reduce-scatter.2.cloned.1.call-update) | async-done | bytes 1048592 | tf_op jit(solution)/shard_map/reduce_scatter | solution.py:39
  77.3 5.9 %all-to-all-start.1 = ((bf16[8,64,1024]{2,1,0:T(8,128)(2,1)}), bf16[8,64,1024]{2,1,0:T(8,128)(2,1)}, u32[]{:S(2)}, u32[]{:S(2)}) async-start(bf16[8,64,1024]{2,1,0:T(8,128)(2,1)} %bitcast.34), calls=%async_computation.2 | async-start | bytes 2097152 | tf_op jit(solution)/shard_map/all_to_all | solution.py:43
  83.1 0.1 mul.79
  83.2 0.1 copy.15
  83.3 26.0 %all-to-all-done.1 = bf16[8,64,1024]{2,1,0:T(8,128)(2,1)} async-done(((bf16[8,64,1024]{2,1,0:T(8,128)(2,1)}), bf16[8,64,1024]{2,1,0:T(8,128)(2,1)}, u32[]{:S(2)}, u32[]{:S(2)}) %all-to-all-start.1) | async-done | bytes 1048608 | tf_op jit(solution)/shard_map/all_to_all | solution.py:43
  109.3 2.9 %gather_fusion = bf16[256,1024]{1,0:T(8,128)(2,1)S(1)} fusion(bf16[512,1024]{1,0:T(8,128)(2,1)} %bitcast.8, s32[1024]{0:T(1024)S(1)} %pad_clamp_fusion), kind=kCustom, calls=%fused_computation | custom fusion | bytes 1049600 | tf_op jit(solution)/shard_map/gather | solution.py:44
  112.3 1.3 %reshape.79 = f32[64,4,1024]{2,1,0:T(4,128)} reshape(bf16[256,1024]{1,0:T(8,128)(2,1)S(1)} %gather_fusion) | data formatting | bytes 1572864 | tf_op jit(solution)/shard_map/convert_element_type | solution.py:44
  113.6 2.0 %multiply_reduce_fusion = bf16[64,1024]{1,0:T(8,128)(2,1)S(1)} fusion(f32[64,4,1024]{2,1,0:T(4,128)} %reshape.79, f32[64,4]{1,0:T(8,128)S(1)} %copy.15), kind=kLoop, calls=%fused_computation.10 | loop fusion | flops 458752 | bytes 1180672 | tf_op jit(solution)/shard_map/reduce_sum | solution.py:45
  115.6 0.2 fusion.14
  115.8 2.5 %all-reduce = (f32[64]{0:T(128)S(1)}, f32[64]{0:T(128)S(1)}) all-reduce(f32[64]{0:T(128)S(1)} %get-tuple-element.6, f32[64]{0:T(128)S(1)} %get-tuple-element.5), channel_id=1, replica_groups=mesh['grp'=2,'ep'=8,'tp'=2] {'tp'}, use_global_device_ids=true, to_apply=%region_9.10 | all-reduce | flops 128 | bytes 1024 | tf_op jit(solution)/shard_map/psum | solution.py:48
  118.3 0.8 add_convert_fusion
  (22 shorter events, 0.3 us)
Async XLA Ops:
  6.5 51.8 %copy-start = (bf16[1,640,2048]{2,1,0:T(8,128)(2,1)S(1)}, bf16[1,640,2048]{2,1,0:T(8,128)(2,1)}, u32[]{:S(2)}) copy-start(bf16[1,640,2048]{2,1,0:T(8,128)(2,1)} %param.13) | copy-start | bytes 7864324
  6.5 46.5 %all-gather.2.cloned.1.call-start = ((), (), s32[]{:S(2)}) async-start(), calls=%async_computation.3 | async-start | bytes 3145728 | tf_op jit(solution)/shard_map/all_gather | solution.py:31
  43.3 33.9 %reduce-scatter.2.cloned.1.call-start = ((), (), s32[]{:S(2)}) async-start(), calls=%async_computation.4 | async-start | bytes 3145728 | tf_op jit(solution)/shard_map/reduce_scatter | solution.py:39
  66.3 17.0 %copy-start.4 = (f32[64,4]{0,1:T(4,128)S(1)}, f32[64,4]{0,1:T(4,128)}, u32[]{:S(2)}) copy-start(f32[64,4]{0,1:T(4,128)} %param.10) | copy-start | bytes 3076
  77.3 32.1 %all-to-all-start.1 = ((bf16[8,64,1024]{2,1,0:T(8,128)(2,1)}), bf16[8,64,1024]{2,1,0:T(8,128)(2,1)}, u32[]{:S(2)}, u32[]{:S(2)}) async-start(bf16[8,64,1024]{2,1,0:T(8,128)(2,1)} %bitcast.34), calls=%async_computation.2 | async-start | bytes 2097152 | tf_op jit(solution)/shard_map/all_to_all | solution.py:43
  112.3 3.3 %copy-start.1 = (bf16[64,2048]{1,0:T(8,128)(2,1)S(1)}, bf16[64,2048]{1,0:T(8,128)(2,1)}, u32[]{:S(2)}) copy-start(bf16[64,2048]{1,0:T(8,128)(2,1)} %param.8) | copy-start | bytes 786436
  112.3 6.0 %copy-start.2 = (f32[1024]{0:T(1024)S(1)}, f32[1024]{0:T(1024)}, u32[]{:S(2)}) copy-start(f32[1024]{0:T(1024)} %param.15) | copy-start | bytes 12292
  112.3 6.0 %copy-start.3 = (f32[1024]{0:T(1024)S(1)}, f32[1024]{0:T(1024)}, u32[]{:S(2)}) copy-start(f32[1024]{0:T(1024)} %param.14) | copy-start | bytes 12292
Sparse Core Ops, SparseCore 0:
  43.5 9.5 all-gather.1
  66.4 10.7 reduce-scatter.1
where the time goes:
time: 126 us
  waiting for transfers between devices  46.7 us (37%)
  blocking collectives  35.4 us (28%)
  matrix products  14.6 us (12%)
  between operations  13.5 us (11%)
  local copies, waits for them, and re-layouts  5.99 us (5%)
  starting transfers between devices  5.91 us (5%)
  other arithmetic  3.78 us (3%)
    all_to_all x1, blocking collectives, shards(): lax.all_to_all(outgoing, 'ep', split_axis=0, concat_axis=0, tiled=True)  33 us
    all_to_all x1, waiting for transfers between devices, shards(): lax.all_to_all(expert_out, 'ep', split_axis=0, concat_axis=0, tiled=True)  26 us
    reduce_scatter x1, waiting for transfers between devices, shards(): lax.psum_scatter(partial_sum, 'tp', scatter_dimension=1, tiled=True)  11 us
    all_gather x1, waiting for transfers between devices, shards(): received = lax.all_gather(arrived, 'tp', axis=1, tiled=True)  9.68 us
    dot_general x1, matrix products, shards(): jnp.dot(hidden, w_down[0], preferred_element_type=jnp.float32)  7.98 us
    all_to_all x1, starting transfers between devices, shards(): lax.all_to_all(expert_out, 'ep', split_axis=0, concat_axis=0, tiled=True)  5.87 us
    dot_general x1, matrix products, shards(): gate = jnp.dot(received, w_gate[0], preferred_element_type=jnp.float32)  5.21 us
    gather x1, local copies, waits for them, and re-layouts, shards(): came_back[target].astype(jnp.float32)  2.92 us
  transfers between devices with their start and end apart: 3, of which 3 were waited for; matrix products, arithmetic and copies ran while one was open for 0% of the time, Pallas kernels for 0%

commit v1 on v0

--- a/solution.py
+++ b/solution.py
@@ -1,13 +1,19 @@
+import functools
+
 import jax
 import jax.numpy as jnp
 from jax import lax
+from jax.experimental import pallas as pl
+from jax.experimental.pallas import tpu as pltpu
 from jax.sharding import PartitionSpec as P
+
 
 residual_scale = 1.4142135
 norm_eps = 1e-05
-
-
-def shards(tokens, routes, gate_weights, w_gate, w_up, w_down, norm_gain, norm_bias):
+LANES = 128
+
+
+def by_slots(tokens, routes, gate_weights, w_gate, w_up, w_down, norm_gain, norm_bias):
     num_ep = lax.axis_size("ep")
     num_tp = lax.axis_size("tp")
     tp_index = lax.axis_index("tp")
@@ -43,8 +49,7 @@
     came_back = lax.all_to_all(expert_out, "ep", split_axis=0, concat_axis=0, tiled=True)
     chosen = came_back[target].astype(jnp.float32).reshape(tok_rows, top_count, half_width)
     mixture = jnp.sum(gate_weights[:, :, None] * chosen, axis=1).astype(jnp.bfloat16)
-    own_tokens = lax.dynamic_slice_in_dim(tokens, tp_index * half_width, half_width, 1)
-    summed = residual_scale * own_tokens.astype(jnp.float32) + mixture.astype(jnp.float32)
+    summed = residual_scale * own_half.astype(jnp.float32) + mixture.astype(jnp.float32)
     row_sum, row_squares = lax.psum(
         (jnp.sum(summed, axis=1), jnp.sum(summed * summed, axis=1)), "tp"
     )
@@ -54,6 +59,257 @@
         variance[:, None] + norm_eps
     ) * norm_gain + norm_bias
     return normed.astype(jnp.bfloat16)
+
+
+VMEM = pl.BlockSpec(memory_space=pltpu.VMEM)
+HBM = pl.BlockSpec(memory_space=pltpu.HBM)
+ANY = pl.BlockSpec(memory_space=pl.ANY)
+MIB = 1 << 20
+
+
+def rows_kernel(experts, tokens_hbm, routes_hbm, gates_hbm, own_ref, other_ref, *scratch):
+    tokens_ref, routes_ref, gates_ref, done = scratch
+    pairs = ((routes_hbm, routes_ref), (gates_hbm, gates_ref), (tokens_hbm, tokens_ref))
+    copies = [pltpu.make_async_copy(a, b, done.at[i]) for i, (a, b) in enumerate(pairs)]
+    for copy in copies:
+        copy.start()
+    copies[0].wait()
+    copies[1].wait()
+    rows, width = tokens_ref.shape
+    share = own_ref.shape[0]
+    routes, gates = routes_ref[...], gates_ref[...]
+    top = routes.shape[0]
+    ids = lax.broadcasted_iota(jnp.int32, (experts, rows), 0)
+    scale = jnp.zeros((experts, rows), jnp.float32)
+    for k in range(top):
+        scale += jnp.where(routes[k : k + 1] == ids, gates[k : k + 1], 0.0)
+    high = scale.astype(jnp.bfloat16).astype(jnp.float32)
+    spare = jnp.zeros((own_ref.shape[1] - width - 2 * experts, rows), jnp.float32)
+    codes = jnp.concatenate([high, scale - high, spare], axis=0)
+    codes = jnp.concatenate([codes, jnp.zeros((codes.shape[0], -rows % LANES), jnp.float32)], axis=1)
+    codes = codes.T.astype(jnp.bfloat16)
+    first = lax.axis_index("tp") == 0
+    low, top_half = codes[:share], codes[share : 2 * share]
+    own_ref[:, width:] = jnp.where(first, low, top_half)
+    other_ref[:, width:] = jnp.where(first, top_half, low)
+    copies[2].wait()
+    low, top_half = tokens_ref[:share], tokens_ref[share:]
+    own_ref[:, :width] = jnp.where(first, low, top_half)
+    other_ref[:, :width] = jnp.where(first, top_half, low)
+
+
+def expert_kernel(experts, width, kept, *refs):
+    *row_refs, wg_ref, wu_ref, wd_ref, mine_ref, theirs_ref = refs
+    packed = jnp.concatenate([r[...] for r in row_refs], axis=0)
+    rows, codes = packed[:, :width], packed[:, width:].astype(jnp.float32)
+    lane = lax.broadcasted_iota(jnp.int32, codes.shape, 1)
+    expert = lax.axis_index("ep")
+    named = (lane == expert) | (lane == expert + experts)
+    weight = jnp.sum(jnp.where(named, codes, 0.0), axis=1, keepdims=True)
+    ff = wg_ref.shape[1]
+    step = 2 * LANES
+    dot = functools.partial(jnp.dot, preferred_element_type=jnp.float32)
+    hidden = []
+    for start in range(0, ff - step + 1, step):
+        gate = dot(rows, wg_ref[:, start : start + step])
+        upper = dot(rows, wu_ref[:, start : start + step])
+        hidden.append((jax.nn.silu(gate) * upper).astype(jnp.bfloat16))
+    rest = ff % step
+    if rest:
+        both = dot(rows, jnp.concatenate([wg_ref[:, ff - rest :], wu_ref[:, ff - rest :]], axis=1))
+        hidden.append((jax.nn.silu(both[:, :rest]) * both[:, rest:]).astype(jnp.bfloat16))
+    hidden = jnp.concatenate(hidden, axis=1)
+    for start in range(0, width, 2 * step):
+        out = dot(hidden, wd_ref[:, start : start + 2 * step]) * weight
+        mine_ref[:, start : start + 2 * step] = out[:kept]
+        theirs_ref[:, start : start + 2 * step] = out[kept:].astype(jnp.bfloat16)
+
+
+def run_expert(experts, mine, theirs, weights):
+    width = weights[0].shape[0]
+    kept, sent = (sum(b.shape[0] for b in blocks) for blocks in (mine, theirs))
+    flops = 6 * (kept + sent) * width * weights[0].shape[1]
+    return pl.pallas_call(
+        functools.partial(expert_kernel, experts, width, kept),
+        out_shape=(
+            jax.ShapeDtypeStruct((kept, width), jnp.float32),
+            jax.ShapeDtypeStruct((sent, width), jnp.bfloat16),
+        ),
+        in_specs=[VMEM] * (len(mine) + len(theirs) + 3),
+        out_specs=(VMEM, VMEM),
+        compiler_params=pltpu.CompilerParams(vmem_limit_bytes=24 * MIB),
+        cost_estimate=pl.CostEstimate(flops=flops, bytes_accessed=8 * MIB, transcendentals=0),
+        name="expert",
+    )(*mine, *theirs, *weights)
+
+
+PIECES = 4
+
+
+def fetch_kernel(*refs):
+    sources, targets, done = refs[:3], refs[4:7], refs[7]
+    copies = []
+    for i, (source, target) in enumerate(zip(sources, targets)):
+        rows = source.shape[0] // PIECES
+        for j in range(PIECES):
+            part = pl.ds(j * rows, rows)
+            copies.append(pltpu.make_async_copy(source.at[part], target.at[part], done.at[i, j]))
+    for copy in copies:
+        copy.start()
+    for copy in copies:
+        copy.wait()
+
+
+def fetch(weights, after):
+    return pl.pallas_call(
+        fetch_kernel,
+        out_shape=tuple(pltpu.VMEM(w.shape, w.dtype) for w in weights),
+        in_specs=[HBM] * 3 + [ANY],
+        out_specs=(VMEM,) * 3,
+        scratch_shapes=[pltpu.SemaphoreType.DMA((3, PIECES))],
+        compiler_params=pltpu.CompilerParams(vmem_limit_bytes=12 * MIB),
+        cost_estimate=pl.CostEstimate(flops=1 << 30, bytes_accessed=8 * MIB, transcendentals=0),
+        name="fetch",
+    )(*(pltpu.with_memory_space_constraint(w, pltpu.HBM) for w in weights), after)
+
+
+def small_call(body, out_shape, *operands):
+    several = isinstance(out_shape, tuple)
+    return pl.pallas_call(
+        body,
+        out_shape=out_shape,
+        in_specs=[VMEM] * len(operands),
+        out_specs=(VMEM,) * len(out_shape) if several else VMEM,
+        compiler_params=pltpu.CompilerParams(vmem_limit_bytes=8 * MIB),
+        cost_estimate=pl.CostEstimate(flops=1 << 26, bytes_accessed=MIB, transcendentals=0),
+    )(*operands)
+
+
+def join_kernel(kept_ref, came_ref, *out_refs):
+    share = out_refs[0].shape[0]
+    for i, out in enumerate(out_refs):
+        part = pl.ds(i * share, share)
+        out[...] = (kept_ref[part] + came_ref[part].astype(jnp.float32)).astype(out.dtype)
+
+
+def add_kernel(kept_ref, came_ref, out_ref):
+    total = kept_ref[...].astype(jnp.float32) + came_ref[...].astype(jnp.float32)
+    out_ref[...] = total.astype(out_ref.dtype)
+
+
+def norm_kernel(count, *refs):
+    terms, (rows_ref, gain_ref, bias_ref, gain_other_ref, bias_other_ref), (stay_ref, go_ref) = (
+        refs[:count],
+        refs[count : count + 5],
+        refs[count + 5 :],
+    )
+    half = stay_ref.shape[1]
+    total = terms[0][...].astype(jnp.float32)
+    for term in terms[1:]:
+        total += term[...].astype(jnp.float32)
+    mixture = total.astype(jnp.bfloat16).astype(jnp.float32)
+    summed = residual_scale * rows_ref[:, : 2 * half].astype(jnp.float32) + mixture
+    mean = jnp.mean(summed, axis=1, keepdims=True)
+    centred = summed - mean
+    variance = jnp.mean(centred * centred, axis=1, keepdims=True)
+    unit = centred * lax.rsqrt(variance + norm_eps)
+    first = lax.axis_index("tp") == 0
+    left, right = unit[:, :half], unit[:, half:]
+    stay = jnp.where(first, left, right) * gain_ref[...] + bias_ref[...]
+    go = jnp.where(first, right, left) * gain_other_ref[...] + bias_other_ref[...]
+    stay_ref[...] = stay.astype(jnp.bfloat16)
+    go_ref[...] = go.astype(jnp.bfloat16)
+
+
+def by_tokens(tokens, routes, gate_weights, w_gate, w_up, w_down, norm_gain, norm_bias):
+    num_ep = lax.axis_size("ep")
+    num_tp = lax.axis_size("tp")
+    tok_rows, width = tokens.shape
+    experts = num_ep * w_gate.shape[0]
+    share = tok_rows // num_tp
+    half = width // num_tp
+    bf16, f32 = jnp.bfloat16, jnp.float32
+
+    def over_ep(x, flip):
+        return lax.ppermute(x, "ep", [(i, i ^ flip) for i in range(num_ep)])
+
+    def over_tp(x):
+        return lax.ppermute(x, "tp", [(i, i ^ 1) for i in range(num_tp)])
+
+    packed = jax.ShapeDtypeStruct((share, width + 2 * experts + (-2 * experts) % LANES), bf16)
+    sources = (tokens, routes.T, gate_weights.T)
+    own, other = pl.pallas_call(
+        functools.partial(rows_kernel, experts),
+        out_shape=(packed, packed),
+        in_specs=[HBM] * 3,
+        out_specs=(VMEM, VMEM),
+        scratch_shapes=[pltpu.VMEM(x.shape, x.dtype) for x in sources] + [pltpu.SemaphoreType.DMA((3,))],
+        compiler_params=pltpu.CompilerParams(vmem_limit_bytes=8 * MIB),
+        cost_estimate=pl.CostEstimate(flops=1 << 26, bytes_accessed=MIB, transcendentals=0),
+        name="rows",
+    )(*(pltpu.with_memory_space_constraint(x, pltpu.HBM) for x in sources))
+
+    bits = flips(num_ep)
+    rows = {0: own}
+    for flip in bits:
+        rows |= {r | flip: over_ep(rows[r], flip) for r in list(rows)}
+    rows_sib = {0: other} | {r: over_tp(rows[r]) for r in range(1, num_ep)}
+    affine = [norm_gain[None], norm_bias[None]]
+    affine_other = [over_tp(a) for a in affine]
+    weights = fetch((w_gate[0], w_up[0], w_down[0]), rows[bits[1]])
+
+    sums = {}
+    for group in groups(num_ep):
+        kept, sent = run_expert(
+            experts, [rows[r] for r in group], [rows_sib[r] for r in group], weights
+        )
+        came = over_tp(sent)
+        kinds = tuple(jax.ShapeDtypeStruct((share, width), bf16 if r & 1 else f32) for r in group)
+        sums |= dict(zip(group, small_call(join_kernel, kinds, kept, came)))
+    terms = []
+    for flip in reversed(bits):
+        for r in sorted(sums, reverse=True):
+            if r & flip:
+                came = over_ep(sums.pop(r), flip)
+                left = r ^ flip
+                if left == 0:
+                    terms.append(came)
+                    continue
+                sends = (left & -left) == flip * 2
+                kind = jax.ShapeDtypeStruct((share, width), bf16 if sends else f32)
+                sums[left] = small_call(add_kernel, kind, sums[left], came)
+    terms.append(sums[0])
+    out = jax.ShapeDtypeStruct((share, half), bf16)
+    stay, go = small_call(functools.partial(norm_kernel, len(terms)), (out, out), *terms, own, *affine, *affine_other)
+    came = over_tp(go)
+    first = lax.axis_index("tp") == 0
+    return jnp.concatenate([jnp.where(first, stay, came), jnp.where(first, came, stay)], axis=0)
+
+
+def flips(num_ep):
+    bits = []
+    flip = num_ep // 2
+    while flip:
+        bits.append(flip)
+        flip //= 2
+    return bits
+
+
+def groups(num_ep):
+    far = num_ep // 2
+    return [tuple(range(far))] + [(r, r + 1) for r in range(far, num_ep, 2)]
+
+
+def shards(tokens, routes, gate_weights, w_gate, w_up, w_down, norm_gain, norm_bias):
+    num_ep = lax.axis_size("ep")
+    num_tp = lax.axis_size("tp")
+    top_count = routes.shape[1]
+    tok_rows = tokens.shape[0]
+    experts = num_ep * w_gate.shape[0]
+    slots = 2 * tok_rows * top_count
+    few = num_ep * tok_rows <= slots and num_ep in (4, 8) and num_tp == 2 and experts == num_ep
+    plan = by_tokens if few else by_slots
+    return plan(tokens, routes, gate_weights, w_gate, w_up, w_down, norm_gain, norm_bias)
 
 
 def solution(mesh):

time: 126 us -> 55.2 us (0.44)
  blocking collectives: 35.4 us -> 0 us
  waiting for transfers between devices: 46.7 us -> 19.1 us
  starting transfers between devices: 5.91 us -> 24.3 us
  matrix products: 14.6 us -> 0 us
  between operations: 13.5 us -> 0.12 us
  Pallas kernels: 0 us -> 10.8 us
  local copies, waits for them, and re-layouts: 5.99 us -> 0.01 us
  other arithmetic: 3.78 us -> 0.68 us
    all_to_all x1 -> x0, blocking collectives: 33 us -> none  [shards(): lax.all_to_all(outgoing, 'ep', split_axis=0, concat_axis=0, tiled=True)]
    all_to_all x1 -> x0, waiting for transfers between devices: 26 us -> none  [shards(): lax.all_to_all(expert_out, 'ep', split_axis=0, concat_axis=0, tiled=True)]
    ppermute x0 -> x27, starting transfers between devices: none -> 24.3 us  [the longest x14 21.2 us: over_ep(): return lax.ppermute(x, 'ep', [(i, i ^ flip) for i in range(num_ep)])]
    ppermute x0 -> x27, waiting for transfers between devices: none -> 19.1 us  [the longest x14 16.9 us: over_ep(): return lax.ppermute(x, 'ep', [(i, i ^ flip) for i in range(num_ep)])]
    dot_general x3 -> x0, matrix products: 14.6 us -> none  [the longest x1 7.98 us: shards(): jnp.dot(hidden, w_down[0], preferred_element_type=jnp.float32)]
    reduce_scatter x1 -> x0, waiting for transfers between devices: 11 us -> none  [shards(): lax.psum_scatter(partial_sum, 'tp', scatter_dimension=1, tiled=True)]
    pallas_call x0 -> x13, Pallas kernels: none -> 10.8 us  [the longest x3 5.82 us: run_expert(): pl.pallas_call(functools.partial(expert_kernel, experts, width, kept), ou...]
    all_gather x1 -> x0, waiting for transfers between devices: 9.68 us -> none  [shards(): received = lax.all_gather(arrived, 'tp', axis=1, tiled=True)]
  transfers between devices with their start and end apart: 3 -> 27, of which waited for: 3 -> 11; matrix products, arithmetic and copies ran while one was open for 0% -> 0% of each run, Pallas kernels for 0% -> 17%
where the time goes in v1:
time: 55.2 us; the launch traced here: 55.1 us
  starting transfers between devices  24.3 us (44%)
  waiting for transfers between devices  19.1 us (35%)
  Pallas kernels  10.8 us (20%)
  other arithmetic  0.68 us (1%)
    ppermute x14, starting transfers between devices, over_ep(): return lax.ppermute(x, 'ep', [(i, i ^ flip) for i in range(num_ep)])  21.2 us
    ppermute x14, waiting for transfers between devices, over_ep(): return lax.ppermute(x, 'ep', [(i, i ^ flip) for i in range(num_ep)])  16.9 us
    pallas_call x3, Pallas kernels, run_expert(): pl.pallas_call(functools.partial(expert_kernel, experts, width, kept), ou...  5.82 us
    pallas_call x1, Pallas kernels, fetch(): pl.pallas_call(fetch_kernel, out_shape=tuple((pltpu.VMEM(w.shape, w.dtype...  3.33 us
    ppermute x13, starting transfers between devices, over_tp(): return lax.ppermute(x, 'tp', [(i, i ^ 1) for i in range(num_tp)])  3.1 us
    ppermute x13, waiting for transfers between devices, over_tp(): return lax.ppermute(x, 'tp', [(i, i ^ 1) for i in range(num_tp)])  2.16 us
  transfers between devices with their start and end apart: 27, of which 11 were waited for; matrix products, arithmetic and copies ran while one was open for 0% of the time, Pallas kernels for 17%

profile of v1, /device:TPU:0, one launch (start us, length us, event | category | flops | bytes accessed | tf_op | source)
XLA Modules:
  0.0 55.1 jit_solution(11247285061480745907)
XLA Ops:
  0.0 1.0 %rows.1 = (bf16[32,2176]{1,0:T(8,128)(2,1)S(1)}, bf16[32,2176]{1,0:T(8,128)(2,1)S(1)}) custom-call(bf16[64,2048]{1,0:T(8,128)(2,1)} %tokens_hbm.1, s32[4,64]{1,0:T(4,128)} %bitcast.14, f32[4,64]{1,0:T(4,128)} %bitcast.15), custom_call_target="tpu_custom_call" | custom-call | flops 67108864 | bytes 1048576 | tf_op jit(solution)/shard_map/rows/pallas_call | solution.py:241
  1.0 4.1 %collective-permute-start.10 = (bf16[32,2176]{1,0:T(8,128)(2,1)S(1)}, bf16[32,2176]{1,0:T(8,128)(2,1)S(1)}, u32[]{:S(2)}, u32[]{:S(2)}) collective-permute-start(bf16[32,2176]{1,0:T(8,128)(2,1)S(1)} %get-tuple-element.26.refs_0_.refs_4_), channel_id=1, source_target_pairs={{0,8},{2,10},{4,12},{6,14},{8,0},{10,2},{12,4},{14,6},{1,9},{3,11}... | collective-permute-start | bytes 417800 | tf_op jit(solution)/shard_map/ppermute | solution.py:234
  5.2 1.6 %collective-permute-start.1 = (bf16[32,2176]{1,0:T(8,128)(2,1)S(1)}, bf16[32,2176]{1,0:T(8,128)(2,1)S(1)}, u32[]{:S(2)}, u32[]{:S(2)}) collective-permute-start(bf16[32,2176]{1,0:T(8,128)(2,1)S(1)} %get-tuple-element.26.refs_0_.refs_4_), channel_id=1, source_target_pairs={{0,4},{2,6},{4,0},{6,2},{8,12},{10,14},{12,8},{14,10},{1,5},{3,7},... | collective-permute-start | bytes 417800 | tf_op jit(solution)/shard_map/ppermute | solution.py:234
  6.7 1.5 %collective-permute-start = (bf16[32,2176]{1,0:T(8,128)(2,1)S(1)}, bf16[32,2176]{1,0:T(8,128)(2,1)S(1)}, u32[]{:S(2)}, u32[]{:S(2)}) collective-permute-start(bf16[32,2176]{1,0:T(8,128)(2,1)S(1)} %get-tuple-element.26.refs_0_.refs_4_), channel_id=1, source_target_pairs={{0,2},{2,0},{4,6},{6,4},{8,10},{10,8},{12,14},{14,12},{1,3},{3,1},... | collective-permute-start | bytes 417800 | tf_op jit(solution)/shard_map/ppermute | solution.py:234
  8.3 3.7 %collective-permute-done.10.refs_0_ = bf16[32,2176]{1,0:T(8,128)(2,1)S(1)} collective-permute-done((bf16[32,2176]{1,0:T(8,128)(2,1)S(1)}, bf16[32,2176]{1,0:T(8,128)(2,1)S(1)}, u32[]{:S(2)}, u32[]{:S(2)}) %collective-permute-start.10) | collective-permute-done | bytes 139296 | tf_op jit(solution)/shard_map/ppermute | solution.py:234
  12.5 1.5 %collective-permute-start.2 = (bf16[32,2176]{1,0:T(8,128)(2,1)S(1)}, bf16[32,2176]{1,0:T(8,128)(2,1)S(1)}, u32[]{:S(2)}, u32[]{:S(2)}) collective-permute-start(bf16[32,2176]{1,0:T(8,128)(2,1)S(1)} %collective-permute-done.1.refs_3_.refs_2_), channel_id=1, source_target_pairs={{0,2},{2,0},{4,6},{6,4},{8,10},{10,8},{12,14},{14,12},{1,3},{3,1},... | collective-permute-start | bytes 417800 | tf_op jit(solution)/shard_map/ppermute | solution.py:234
  14.1 2.9 %collective-permute-done.16.refs_0_ = bf16[32,2176]{1,0:T(8,128)(2,1)S(1)} collective-permute-done((bf16[32,2176]{1,0:T(8,128)(2,1)S(1)}, bf16[32,2176]{1,0:T(8,128)(2,1)S(1)}, u32[]{:S(2)}, u32[]{:S(2)}) %collective-permute-start.16) | collective-permute-done | bytes 139296 | tf_op jit(solution)/shard_map/ppermute | solution.py:234
  17.0 1.6 %collective-permute-start.17 = (bf16[32,2176]{1,0:T(8,128)(2,1)S(1)}, bf16[32,2176]{1,0:T(8,128)(2,1)S(1)}, u32[]{:S(2)}, u32[]{:S(2)}) collective-permute-start(bf16[32,2176]{1,0:T(8,128)(2,1)S(1)} %collective-permute-done.16.refs_0_), channel_id=1, source_target_pairs={{0,2},{2,0},{4,6},{6,4},{8,10},{10,8},{12,14},{14,12},{1,3},{3,1},... | collective-permute-start | bytes 417800 | tf_op jit(solution)/shard_map/ppermute | solution.py:234
  19.8 3.3 %fetch.1 = (bf16[2048,640]{1,0:T(8,128)(2,1)S(1)}, bf16[2048,640]{1,0:T(8,128)(2,1)S(1)}, bf16[640,2048]{1,0:T(8,128)(2,1)S(1)}) custom-call(bf16[2048,640]{1,0:T(8,128)(2,1)} %bitcast.11, bf16[2048,640]{1,0:T(8,128)(2,1)} %bitcast.12, bf16[640,2048]{1,0:T(8,128)(2,1)} %bitcast.13, bf16[32,2176]{1,0:T(8,128)(2,1)S(1)} %collective-permute-done.1.refs_3_.refs_2_), custom_call_target="tpu_custom_call" | custom-call | flops 1073741824 | bytes 8388608 | tf_op jit(solution)/shard_map/fetch/pallas_call | solution.py:164
  23.8 2.7 %expert.3 = (f32[128,2048]{1,0:T(8,128)S(1)}, bf16[128,2048]{1,0:T(8,128)(2,1)S(1)}) custom-call(bf16[32,2176]{1,0:T(8,128)(2,1)S(1)} %get-tuple-element.26.refs_0_.refs_4_, bf16[32,2176]{1,0:T(8,128)(2,1)S(1)} %collective-permute-done.refs_1_, bf16[32,2176]{1,0:T(8,128)(2,1)S(1)} %collective-permute-done.1.refs_3_.refs_2_, ...), custom_call_target="tpu_custom_call" | custom-call | flops 2013265920 | bytes 8388608 | tf_op jit(solution)/shard_map/expert/pallas_call | solution.py:132
  27.3 1.6 %expert.5 = (f32[64,2048]{1,0:T(8,128)S(1)}, bf16[64,2048]{1,0:T(8,128)(2,1)S(1)}) custom-call(bf16[32,2176]{1,0:T(8,128)(2,1)S(1)} %collective-permute-done.16.refs_0_, bf16[32,2176]{1,0:T(8,128)(2,1)S(1)} %collective-permute-done.17.refs_1_, bf16[32,2176]{1,0:T(8,128)(2,1)S(1)} %collective-permute-done.18.refs_2_, ...), custom_call_target="tpu_custom_call" | custom-call | flops 1006632960 | bytes 8388608 | tf_op jit(solution)/shard_map/expert/pallas_call | solution.py:132
  29.2 1.5 %expert.4 = (f32[64,2048]{1,0:T(8,128)S(1)}, bf16[64,2048]{1,0:T(8,128)(2,1)S(1)}) custom-call(bf16[32,2176]{1,0:T(8,128)(2,1)S(1)} %collective-permute-done.10.refs_0_, bf16[32,2176]{1,0:T(8,128)(2,1)S(1)} %collective-permute-done.11.refs_1_, bf16[32,2176]{1,0:T(8,128)(2,1)S(1)} %collective-permute-done.12.refs_2_, ...), custom_call_target="tpu_custom_call" | custom-call | flops 1006632960 | bytes 8388608 | tf_op jit(solution)/shard_map/expert/pallas_call | solution.py:132
  31.1 1.2 %collective-permute-start.21 = (bf16[32,2048]{1,0:T(8,128)(2,1)S(1)}, bf16[32,2048]{1,0:T(8,128)(2,1)S(1)}, u32[]{:S(2)}, u32[]{:S(2)}) collective-permute-start(bf16[32,2048]{1,0:T(8,128)(2,1)S(1)} %get-tuple-element.43), channel_id=1, source_target_pairs={{0,2},{2,0},{4,6},{6,4},{8,10},{10,8},{12,14},{14,12},{1,3},{3,1},... | collective-permute-start | bytes 393224 | tf_op jit(solution)/shard_map/ppermute | solution.py:234
  32.4 1.3 %collective-permute-start.15 = (bf16[32,2048]{1,0:T(8,128)(2,1)S(1)}, bf16[32,2048]{1,0:T(8,128)(2,1)S(1)}, u32[]{:S(2)}, u32[]{:S(2)}) collective-permute-start(bf16[32,2048]{1,0:T(8,128)(2,1)S(1)} %get-tuple-element.39), channel_id=1, source_target_pairs={{0,2},{2,0},{4,6},{6,4},{8,10},{10,8},{12,14},{14,12},{1,3},{3,1},... | collective-permute-start | bytes 393224 | tf_op jit(solution)/shard_map/ppermute | solution.py:234
  33.9 0.8 %collective-permute-start.8 = (bf16[32,2048]{1,0:T(8,128)(2,1)S(1)}, bf16[32,2048]{1,0:T(8,128)(2,1)S(1)}, u32[]{:S(2)}, u32[]{:S(2)}) collective-permute-start(bf16[32,2048]{1,0:T(8,128)(2,1)S(1)} %get-tuple-element.35), channel_id=1, source_target_pairs={{0,2},{2,0},{4,6},{6,4},{8,10},{10,8},{12,14},{14,12},{1,3},{3,1},... | collective-permute-start | bytes 393224 | tf_op jit(solution)/shard_map/ppermute | solution.py:234
  34.7 2.8 %collective-permute-done.21.came_ref = bf16[32,2048]{1,0:T(8,128)(2,1)S(1)} collective-permute-done((bf16[32,2048]{1,0:T(8,128)(2,1)S(1)}, bf16[32,2048]{1,0:T(8,128)(2,1)S(1)}, u32[]{:S(2)}, u32[]{:S(2)}) %collective-permute-start.21) | collective-permute-done | bytes 131104 | tf_op jit(solution)/shard_map/ppermute | solution.py:234
  38.4 2.0 %collective-permute-done.15.came_ref = bf16[32,2048]{1,0:T(8,128)(2,1)S(1)} collective-permute-done((bf16[32,2048]{1,0:T(8,128)(2,1)S(1)}, bf16[32,2048]{1,0:T(8,128)(2,1)S(1)}, u32[]{:S(2)}, u32[]{:S(2)}) %collective-permute-start.15) | collective-permute-done | bytes 131104 | tf_op jit(solution)/shard_map/ppermute | solution.py:234
  40.4 1.2 %collective-permute-start.7 = (bf16[32,2048]{1,0:T(8,128)(2,1)S(1)}, bf16[32,2048]{1,0:T(8,128)(2,1)S(1)}, u32[]{:S(2)}, u32[]{:S(2)}) collective-permute-start(bf16[32,2048]{1,0:T(8,128)(2,1)S(1)} %get-tuple-element.33), channel_id=1, source_target_pairs={{0,2},{2,0},{4,6},{6,4},{8,10},{10,8},{12,14},{14,12},{1,3},{3,1},... | collective-permute-start | bytes 393224 | tf_op jit(solution)/shard_map/ppermute | solution.py:234
  41.6 1.6 %collective-permute-done.8.came_ref = bf16[32,2048]{1,0:T(8,128)(2,1)S(1)} collective-permute-done((bf16[32,2048]{1,0:T(8,128)(2,1)S(1)}, bf16[32,2048]{1,0:T(8,128)(2,1)S(1)}, u32[]{:S(2)}, u32[]{:S(2)}) %collective-permute-start.8) | collective-permute-done | bytes 131104 | tf_op jit(solution)/shard_map/ppermute | solution.py:234
  43.2 0.8 %collective-permute-start.9 = (bf16[32,2048]{1,0:T(8,128)(2,1)S(1)}, bf16[32,2048]{1,0:T(8,128)(2,1)S(1)}, u32[]{:S(2)}, u32[]{:S(2)}) collective-permute-start(bf16[32,2048]{1,0:T(8,128)(2,1)S(1)} %shard_map.83), channel_id=1, source_target_pairs={{0,4},{2,6},{4,0},{6,2},{8,12},{10,14},{12,8},{14,10},{1,5},{3,7},... | collective-permute-start | bytes 393224 | tf_op jit(solution)/shard_map/ppermute | solution.py:234
  44.1 3.4 %collective-permute-start.23 = (bf16[32,2048]{1,0:T(8,128)(2,1)S(1)}, bf16[32,2048]{1,0:T(8,128)(2,1)S(1)}, u32[]{:S(2)}, u32[]{:S(2)}) collective-permute-start(bf16[32,2048]{1,0:T(8,128)(2,1)S(1)} %shard_map.88), channel_id=1, source_target_pairs={{0,8},{2,10},{4,12},{6,14},{8,0},{10,2},{12,4},{14,6},{1,9},{3,11}... | collective-permute-start | bytes 393224 | tf_op jit(solution)/shard_map/ppermute | solution.py:234
  48.8 1.1 %collective-permute-done.9.refs_1_ = bf16[32,2048]{1,0:T(8,128)(2,1)S(1)} collective-permute-done((bf16[32,2048]{1,0:T(8,128)(2,1)S(1)}, bf16[32,2048]{1,0:T(8,128)(2,1)S(1)}, u32[]{:S(2)}, u32[]{:S(2)}) %collective-permute-start.9) | collective-permute-done | bytes 131104 | tf_op jit(solution)/shard_map/ppermute | solution.py:234
  49.9 2.9 %collective-permute-done.23.refs_2_ = bf16[32,2048]{1,0:T(8,128)(2,1)S(1)} collective-permute-done((bf16[32,2048]{1,0:T(8,128)(2,1)S(1)}, bf16[32,2048]{1,0:T(8,128)(2,1)S(1)}, u32[]{:S(2)}, u32[]{:S(2)}) %collective-permute-start.23) | collective-permute-done | bytes 131104 | tf_op jit(solution)/shard_map/ppermute | solution.py:234
  53.1 1.2 %collective-permute-done.26 = bf16[32,1024]{1,0:T(8,128)(2,1)S(1)} collective-permute-done((bf16[32,1024]{1,0:T(8,128)(2,1)S(1)}, bf16[32,1024]{1,0:T(8,128)(2,1)S(1)}, u32[]{:S(2)}, u32[]{:S(2)}) %collective-permute-start.26) | collective-permute-done | bytes 65568 | tf_op jit(solution)/shard_map/ppermute | solution.py:237
  (49 shorter events, 7.6 us)
Async XLA Ops:
  1.0 10.9 %collective-permute-start.10 = (bf16[32,2176]{1,0:T(8,128)(2,1)S(1)}, bf16[32,2176]{1,0:T(8,128)(2,1)S(1)}, u32[]{:S(2)}, u32[]{:S(2)}) collective-permute-start(bf16[32,2176]{1,0:T(8,128)(2,1)S(1)} %get-tuple-element.26.refs_0_.refs_4_), channel_id=1, source_target_pairs={{0,8},{2,10},{4,12},{6,14},{8,0},{10,2},{12,4},{14,6},{1,9},{3,11}... | collective-permute-start | bytes 417800 | tf_op jit(solution)/shard_map/ppermute | solution.py:234
  5.2 7.4 %collective-permute-start.1 = (bf16[32,2176]{1,0:T(8,128)(2,1)S(1)}, bf16[32,2176]{1,0:T(8,128)(2,1)S(1)}, u32[]{:S(2)}, u32[]{:S(2)}) collective-permute-start(bf16[32,2176]{1,0:T(8,128)(2,1)S(1)} %get-tuple-element.26.refs_0_.refs_4_), channel_id=1, source_target_pairs={{0,4},{2,6},{4,0},{6,2},{8,12},{10,14},{12,8},{14,10},{1,5},{3,7},... | collective-permute-start | bytes 417800 | tf_op jit(solution)/shard_map/ppermute | solution.py:234
  6.7 7.3 %collective-permute-start = (bf16[32,2176]{1,0:T(8,128)(2,1)S(1)}, bf16[32,2176]{1,0:T(8,128)(2,1)S(1)}, u32[]{:S(2)}, u32[]{:S(2)}) collective-permute-start(bf16[32,2176]{1,0:T(8,128)(2,1)S(1)} %get-tuple-element.26.refs_0_.refs_4_), channel_id=1, source_target_pairs={{0,2},{2,0},{4,6},{6,4},{8,10},{10,8},{12,14},{14,12},{1,3},{3,1},... | collective-permute-start | bytes 417800 | tf_op jit(solution)/shard_map/ppermute | solution.py:234
  11.9 5.1 %collective-permute-start.16 = (bf16[32,2176]{1,0:T(8,128)(2,1)S(1)}, bf16[32,2176]{1,0:T(8,128)(2,1)S(1)}, u32[]{:S(2)}, u32[]{:S(2)}) collective-permute-start(bf16[32,2176]{1,0:T(8,128)(2,1)S(1)} %collective-permute-done.10.refs_0_), channel_id=1, source_target_pairs={{0,4},{2,6},{4,0},{6,2},{8,12},{10,14},{12,8},{14,10},{1,5},{3,7},... | collective-permute-start | bytes 417800 | tf_op jit(solution)/shard_map/ppermute | solution.py:234
  12.5 6.0 %collective-permute-start.2 = (bf16[32,2176]{1,0:T(8,128)(2,1)S(1)}, bf16[32,2176]{1,0:T(8,128)(2,1)S(1)}, u32[]{:S(2)}, u32[]{:S(2)}) collective-permute-start(bf16[32,2176]{1,0:T(8,128)(2,1)S(1)} %collective-permute-done.1.refs_3_.refs_2_), channel_id=1, source_target_pairs={{0,2},{2,0},{4,6},{6,4},{8,10},{10,8},{12,14},{14,12},{1,3},{3,1},... | collective-permute-start | bytes 417800 | tf_op jit(solution)/shard_map/ppermute | solution.py:234
  14.1 9.1 %collective-permute-start.3 = (bf16[32,2176]{1,0:T(8,128)(2,1)S(1)}, bf16[32,2176]{1,0:T(8,128)(2,1)S(1)}, u32[]{:S(2)}, u32[]{:S(2)}) collective-permute-start(bf16[32,2176]{1,0:T(8,128)(2,1)S(1)} %collective-permute-done.refs_1_), channel_id=1, source_target_pairs={{0,1},{1,0},{2,3},{3,2},{4,5},{5,4},{6,7},{7,6},{8,9},{9,8},{10,11... | collective-permute-start | bytes 417800 | tf_op jit(solution)/shard_map/ppermute | solution.py:237
  17.0 6.5 %collective-permute-start.17 = (bf16[32,2176]{1,0:T(8,128)(2,1)S(1)}, bf16[32,2176]{1,0:T(8,128)(2,1)S(1)}, u32[]{:S(2)}, u32[]{:S(2)}) collective-permute-start(bf16[32,2176]{1,0:T(8,128)(2,1)S(1)} %collective-permute-done.16.refs_0_), channel_id=1, source_target_pairs={{0,2},{2,0},{4,6},{6,4},{8,10},{10,8},{12,14},{14,12},{1,3},{3,1},... | collective-permute-start | bytes 417800 | tf_op jit(solution)/shard_map/ppermute | solution.py:234
  18.5 5.2 %collective-permute-start.4 = (bf16[32,2176]{1,0:T(8,128)(2,1)S(1)}, bf16[32,2176]{1,0:T(8,128)(2,1)S(1)}, u32[]{:S(2)}, u32[]{:S(2)}) collective-permute-start(bf16[32,2176]{1,0:T(8,128)(2,1)S(1)} %collective-permute-done.1.refs_3_.refs_2_), channel_id=1, source_target_pairs={{0,1},{1,0},{2,3},{3,2},{4,5},{5,4},{6,7},{7,6},{8,9},{9,8},{10,11... | collective-permute-start | bytes 417800 | tf_op jit(solution)/shard_map/ppermute | solution.py:237
  18.6 5.2 %collective-permute-start.5 = (bf16[32,2176]{1,0:T(8,128)(2,1)S(1)}, bf16[32,2176]{1,0:T(8,128)(2,1)S(1)}, u32[]{:S(2)}, u32[]{:S(2)}) collective-permute-start(bf16[32,2176]{1,0:T(8,128)(2,1)S(1)} %collective-permute-done.2.refs_3_), channel_id=1, source_target_pairs={{0,1},{1,0},{2,3},{3,2},{4,5},{5,4},{6,7},{7,6},{8,9},{9,8},{10,11... | collective-permute-start | bytes 417800 | tf_op jit(solution)/shard_map/ppermute | solution.py:237
  19.1 8.0 %collective-permute-start.11 = (bf16[32,2176]{1,0:T(8,128)(2,1)S(1)}, bf16[32,2176]{1,0:T(8,128)(2,1)S(1)}, u32[]{:S(2)}, u32[]{:S(2)}) collective-permute-start(bf16[32,2176]{1,0:T(8,128)(2,1)S(1)} %collective-permute-done.10.refs_0_), channel_id=1, source_target_pairs={{0,2},{2,0},{4,6},{6,4},{8,10},{10,8},{12,14},{14,12},{1,3},{3,1},... | collective-permute-start | bytes 417800 | tf_op jit(solution)/shard_map/ppermute | solution.py:234
  23.2 4.1 %collective-permute-start.18 = (bf16[32,2176]{1,0:T(8,128)(2,1)S(1)}, bf16[32,2176]{1,0:T(8,128)(2,1)S(1)}, u32[]{:S(2)}, u32[]{:S(2)}) collective-permute-start(bf16[32,2176]{1,0:T(8,128)(2,1)S(1)} %collective-permute-done.16.refs_0_), channel_id=1, source_target_pairs={{0,1},{1,0},{2,3},{3,2},{4,5},{5,4},{6,7},{7,6},{8,9},{9,8},{10,11... | collective-permute-start | bytes 417800 | tf_op jit(solution)/shard_map/ppermute | solution.py:237
  23.5 3.8 %collective-permute-start.19 = (bf16[32,2176]{1,0:T(8,128)(2,1)S(1)}, bf16[32,2176]{1,0:T(8,128)(2,1)S(1)}, u32[]{:S(2)}, u32[]{:S(2)}) collective-permute-start(bf16[32,2176]{1,0:T(8,128)(2,1)S(1)} %collective-permute-done.17.refs_1_), channel_id=1, source_target_pairs={{0,1},{1,0},{2,3},{3,2},{4,5},{5,4},{6,7},{7,6},{8,9},{9,8},{10,11... | collective-permute-start | bytes 417800 | tf_op jit(solution)/shard_map/ppermute | solution.py:237
  26.5 7.3 %collective-permute-start.6 = (bf16[128,2048]{1,0:T(8,128)(2,1)S(1)}, bf16[128,2048]{1,0:T(8,128)(2,1)S(1)}, u32[]{:S(2)}, u32[]{:S(2)}) collective-permute-start(bf16[128,2048]{1,0:T(8,128)(2,1)S(1)} %get-tuple-element.32), channel_id=1, source_target_pairs={{0,1},{1,0},{2,3},{3,2},{4,5},{5,4},{6,7},{7,6},{8,9},{9,8},{10,11... | collective-permute-start | bytes 1572872 | tf_op jit(solution)/shard_map/ppermute | solution.py:237
  26.8 2.4 %collective-permute-start.12 = (bf16[32,2176]{1,0:T(8,128)(2,1)S(1)}, bf16[32,2176]{1,0:T(8,128)(2,1)S(1)}, u32[]{:S(2)}, u32[]{:S(2)}) collective-permute-start(bf16[32,2176]{1,0:T(8,128)(2,1)S(1)} %collective-permute-done.10.refs_0_), channel_id=1, source_target_pairs={{0,1},{1,0},{2,3},{3,2},{4,5},{5,4},{6,7},{7,6},{8,9},{9,8},{10,11... | collective-permute-start | bytes 417800 | tf_op jit(solution)/shard_map/ppermute | solution.py:237
  27.1 2.1 %collective-permute-start.13 = (bf16[32,2176]{1,0:T(8,128)(2,1)S(1)}, bf16[32,2176]{1,0:T(8,128)(2,1)S(1)}, u32[]{:S(2)}, u32[]{:S(2)}) collective-permute-start(bf16[32,2176]{1,0:T(8,128)(2,1)S(1)} %collective-permute-done.11.refs_1_), channel_id=1, source_target_pairs={{0,1},{1,0},{2,3},{3,2},{4,5},{5,4},{6,7},{7,6},{8,9},{9,8},{10,11... | collective-permute-start | bytes 417800 | tf_op jit(solution)/shard_map/ppermute | solution.py:237
  28.9 2.2 %collective-permute-start.20 = (bf16[64,2048]{1,0:T(8,128)(2,1)S(1)}, bf16[64,2048]{1,0:T(8,128)(2,1)S(1)}, u32[]{:S(2)}, u32[]{:S(2)}) collective-permute-start(bf16[64,2048]{1,0:T(8,128)(2,1)S(1)} %get-tuple-element.41), channel_id=1, source_target_pairs={{0,1},{1,0},{2,3},{3,2},{4,5},{5,4},{6,7},{7,6},{8,9},{9,8},{10,11... | collective-permute-start | bytes 786440 | tf_op jit(solution)/shard_map/ppermute | solution.py:237
  30.8 1.6 %collective-permute-start.14 = (bf16[64,2048]{1,0:T(8,128)(2,1)S(1)}, bf16[64,2048]{1,0:T(8,128)(2,1)S(1)}, u32[]{:S(2)}, u32[]{:S(2)}) collective-permute-start(bf16[64,2048]{1,0:T(8,128)(2,1)S(1)} %get-tuple-element.37), channel_id=1, source_target_pairs={{0,1},{1,0},{2,3},{3,2},{4,5},{5,4},{6,7},{7,6},{8,9},{9,8},{10,11... | collective-permute-start | bytes 786440 | tf_op jit(solution)/shard_map/ppermute | solution.py:237
  31.1 6.4 %collective-permute-start.21 = (bf16[32,2048]{1,0:T(8,128)(2,1)S(1)}, bf16[32,2048]{1,0:T(8,128)(2,1)S(1)}, u32[]{:S(2)}, u32[]{:S(2)}) collective-permute-start(bf16[32,2048]{1,0:T(8,128)(2,1)S(1)} %get-tuple-element.43), channel_id=1, source_target_pairs={{0,2},{2,0},{4,6},{6,4},{8,10},{10,8},{12,14},{14,12},{1,3},{3,1},... | collective-permute-start | bytes 393224 | tf_op jit(solution)/shard_map/ppermute | solution.py:234
  32.4 7.9 %collective-permute-start.15 = (bf16[32,2048]{1,0:T(8,128)(2,1)S(1)}, bf16[32,2048]{1,0:T(8,128)(2,1)S(1)}, u32[]{:S(2)}, u32[]{:S(2)}) collective-permute-start(bf16[32,2048]{1,0:T(8,128)(2,1)S(1)} %get-tuple-element.39), channel_id=1, source_target_pairs={{0,2},{2,0},{4,6},{6,4},{8,10},{10,8},{12,14},{14,12},{1,3},{3,1},... | collective-permute-start | bytes 393224 | tf_op jit(solution)/shard_map/ppermute | solution.py:234
  33.9 9.3 %collective-permute-start.8 = (bf16[32,2048]{1,0:T(8,128)(2,1)S(1)}, bf16[32,2048]{1,0:T(8,128)(2,1)S(1)}, u32[]{:S(2)}, u32[]{:S(2)}) collective-permute-start(bf16[32,2048]{1,0:T(8,128)(2,1)S(1)} %get-tuple-element.35), channel_id=1, source_target_pairs={{0,2},{2,0},{4,6},{6,4},{8,10},{10,8},{12,14},{14,12},{1,3},{3,1},... | collective-permute-start | bytes 393224 | tf_op jit(solution)/shard_map/ppermute | solution.py:234
  37.6 6.4 %collective-permute-start.22 = (bf16[32,2048]{1,0:T(8,128)(2,1)S(1)}, bf16[32,2048]{1,0:T(8,128)(2,1)S(1)}, u32[]{:S(2)}, u32[]{:S(2)}) collective-permute-start(bf16[32,2048]{1,0:T(8,128)(2,1)S(1)} %shard_map.87), channel_id=1, source_target_pairs={{0,4},{2,6},{4,0},{6,2},{8,12},{10,14},{12,8},{14,10},{1,5},{3,7},... | collective-permute-start | bytes 393224 | tf_op jit(solution)/shard_map/ppermute | solution.py:234
  40.4 8.4 %collective-permute-start.7 = (bf16[32,2048]{1,0:T(8,128)(2,1)S(1)}, bf16[32,2048]{1,0:T(8,128)(2,1)S(1)}, u32[]{:S(2)}, u32[]{:S(2)}) collective-permute-start(bf16[32,2048]{1,0:T(8,128)(2,1)S(1)} %get-tuple-element.33), channel_id=1, source_target_pairs={{0,2},{2,0},{4,6},{6,4},{8,10},{10,8},{12,14},{14,12},{1,3},{3,1},... | collective-permute-start | bytes 393224 | tf_op jit(solution)/shard_map/ppermute | solution.py:234
  43.2 6.7 %collective-permute-start.9 = (bf16[32,2048]{1,0:T(8,128)(2,1)S(1)}, bf16[32,2048]{1,0:T(8,128)(2,1)S(1)}, u32[]{:S(2)}, u32[]{:S(2)}) collective-permute-start(bf16[32,2048]{1,0:T(8,128)(2,1)S(1)} %shard_map.83), channel_id=1, source_target_pairs={{0,4},{2,6},{4,0},{6,2},{8,12},{10,14},{12,8},{14,10},{1,5},{3,7},... | collective-permute-start | bytes 393224 | tf_op jit(solution)/shard_map/ppermute | solution.py:234
  44.1 8.7 %collective-permute-start.23 = (bf16[32,2048]{1,0:T(8,128)(2,1)S(1)}, bf16[32,2048]{1,0:T(8,128)(2,1)S(1)}, u32[]{:S(2)}, u32[]{:S(2)}) collective-permute-start(bf16[32,2048]{1,0:T(8,128)(2,1)S(1)} %shard_map.88), channel_id=1, source_target_pairs={{0,8},{2,10},{4,12},{6,14},{8,0},{10,2},{12,4},{14,6},{1,9},{3,11}... | collective-permute-start | bytes 393224 | tf_op jit(solution)/shard_map/ppermute | solution.py:234
  (5 other events, 36.6 us)

commit v2 on v1

--- a/solution.py
+++ b/solution.py
@@ -67,7 +67,7 @@
 MIB = 1 << 20
 
 
-def rows_kernel(experts, tokens_hbm, routes_hbm, gates_hbm, own_ref, other_ref, *scratch):
+def rows_kernel(experts, tokens_hbm, routes_hbm, gates_hbm, all_ref, own_ref, *scratch):
     tokens_ref, routes_ref, gates_ref, done = scratch
     pairs = ((routes_hbm, routes_ref), (gates_hbm, gates_ref), (tokens_hbm, tokens_ref))
     copies = [pltpu.make_async_copy(a, b, done.at[i]) for i, (a, b) in enumerate(pairs)]
@@ -78,29 +78,27 @@
     rows, width = tokens_ref.shape
     share = own_ref.shape[0]
     routes, gates = routes_ref[...], gates_ref[...]
-    top = routes.shape[0]
     ids = lax.broadcasted_iota(jnp.int32, (experts, rows), 0)
     scale = jnp.zeros((experts, rows), jnp.float32)
-    for k in range(top):
+    for k in range(routes.shape[0]):
         scale += jnp.where(routes[k : k + 1] == ids, gates[k : k + 1], 0.0)
     high = scale.astype(jnp.bfloat16).astype(jnp.float32)
     spare = jnp.zeros((own_ref.shape[1] - width - 2 * experts, rows), jnp.float32)
     codes = jnp.concatenate([high, scale - high, spare], axis=0)
     codes = jnp.concatenate([codes, jnp.zeros((codes.shape[0], -rows % LANES), jnp.float32)], axis=1)
-    codes = codes.T.astype(jnp.bfloat16)
-    first = lax.axis_index("tp") == 0
-    low, top_half = codes[:share], codes[share : 2 * share]
-    own_ref[:, width:] = jnp.where(first, low, top_half)
-    other_ref[:, width:] = jnp.where(first, top_half, low)
+    codes = codes.T[:rows].astype(jnp.bfloat16)
+    first = lax.axis_index("tp") == 0
+    own_ref[:, width:] = jnp.where(first, codes[:share], codes[share:])
+    all_ref[:, width:] = codes
     copies[2].wait()
-    low, top_half = tokens_ref[:share], tokens_ref[share:]
-    own_ref[:, :width] = jnp.where(first, low, top_half)
-    other_ref[:, :width] = jnp.where(first, top_half, low)
-
-
-def expert_kernel(experts, width, kept, *refs):
+    own_ref[:, :width] = jnp.where(first, tokens_ref[:share], tokens_ref[share:])
+    all_ref[:, :width] = tokens_ref[...]
+
+
+def expert_kernel(experts, width, arrange, *refs):
     *row_refs, wg_ref, wu_ref, wd_ref, mine_ref, theirs_ref = refs
-    packed = jnp.concatenate([r[...] for r in row_refs], axis=0)
+    kept = mine_ref.shape[0]
+    packed = jnp.concatenate(arrange(*(r[...] for r in row_refs)), axis=0)
     rows, codes = packed[:, :width], packed[:, width:].astype(jnp.float32)
     lane = lax.broadcasted_iota(jnp.int32, codes.shape, 1)
     expert = lax.axis_index("ep")
@@ -125,22 +123,32 @@
         theirs_ref[:, start : start + 2 * step] = out[kept:].astype(jnp.bfloat16)
 
 
-def run_expert(experts, mine, theirs, weights):
+def as_given(*blocks):
+    return blocks
+
+
+def near_blocks(own, came, other, across, across_other):
+    first = lax.axis_index("tp") == 0
+    pick = functools.partial(jnp.where, first)
+    across = pick(across_other, across)
+    return pick(own, came), pick(came, across), pick(other, own), pick(across, other)
+
+
+def run_expert(experts, blocks, arrange, kept, weights):
     width = weights[0].shape[0]
-    kept, sent = (sum(b.shape[0] for b in blocks) for blocks in (mine, theirs))
-    flops = 6 * (kept + sent) * width * weights[0].shape[1]
+    flops = 12 * kept * width * weights[0].shape[1]
     return pl.pallas_call(
-        functools.partial(expert_kernel, experts, width, kept),
+        functools.partial(expert_kernel, experts, width, arrange),
         out_shape=(
             jax.ShapeDtypeStruct((kept, width), jnp.float32),
-            jax.ShapeDtypeStruct((sent, width), jnp.bfloat16),
+            jax.ShapeDtypeStruct((kept, width), jnp.bfloat16),
         ),
-        in_specs=[VMEM] * (len(mine) + len(theirs) + 3),
+        in_specs=[VMEM] * (len(blocks) + 3),
         out_specs=(VMEM, VMEM),
         compiler_params=pltpu.CompilerParams(vmem_limit_bytes=24 * MIB),
         cost_estimate=pl.CostEstimate(flops=flops, bytes_accessed=8 * MIB, transcendentals=0),
         name="expert",
-    )(*mine, *theirs, *weights)
+    )(*blocks, *weights)
 
 
 PIECES = 4
@@ -197,6 +205,14 @@
     out_ref[...] = total.astype(out_ref.dtype)
 
 
+def cut_kernel(here_ref, came_ref, stay_ref, go_ref):
+    share = stay_ref.shape[0]
+    first = lax.axis_index("tp") == 0
+    low, high = here_ref[...], came_ref[...]
+    stay_ref[...] = jnp.where(first, low[:share], high[share:])
+    go_ref[...] = jnp.where(first, low[share:], high[:share])
+
+
 def norm_kernel(count, *refs):
     terms, (rows_ref, gain_ref, bias_ref, gain_other_ref, bias_other_ref), (stay_ref, go_ref) = (
         refs[:count],
@@ -229,18 +245,25 @@
     share = tok_rows // num_tp
     half = width // num_tp
     bf16, f32 = jnp.bfloat16, jnp.float32
-
-    def over_ep(x, flip):
-        return lax.ppermute(x, "ep", [(i, i ^ flip) for i in range(num_ep)])
-
-    def over_tp(x):
-        return lax.ppermute(x, "tp", [(i, i ^ 1) for i in range(num_tp)])
-
-    packed = jax.ShapeDtypeStruct((share, width + 2 * experts + (-2 * experts) % LANES), bf16)
+    shape = jax.ShapeDtypeStruct
+
+    def over_ep(x, flips):
+        pairs = [
+            (i * num_tp + c, (i ^ flips[c]) * num_tp + c)
+            for i in range(num_ep)
+            for c in range(num_tp)
+            if flips[c] is not None
+        ]
+        return lax.ppermute(x, ("ep", "tp"), pairs)
+
+    def over_tp(x, pairs=((0, 1), (1, 0))):
+        return lax.ppermute(x, "tp", pairs)
+
+    packed = width + 2 * experts + (-2 * experts) % LANES
     sources = (tokens, routes.T, gate_weights.T)
-    own, other = pl.pallas_call(
+    full, own = pl.pallas_call(
         functools.partial(rows_kernel, experts),
-        out_shape=(packed, packed),
+        out_shape=(shape((tok_rows, packed), bf16), shape((share, packed), bf16)),
         in_specs=[HBM] * 3,
         out_specs=(VMEM, VMEM),
         scratch_shapes=[pltpu.VMEM(x.shape, x.dtype) for x in sources] + [pltpu.SemaphoreType.DMA((3,))],
@@ -248,56 +271,53 @@
         cost_estimate=pl.CostEstimate(flops=1 << 26, bytes_accessed=MIB, transcendentals=0),
         name="rows",
     )(*(pltpu.with_memory_space_constraint(x, pltpu.HBM) for x in sources))
-
-    bits = flips(num_ep)
-    rows = {0: own}
-    for flip in bits:
-        rows |= {r | flip: over_ep(rows[r], flip) for r in list(rows)}
-    rows_sib = {0: other} | {r: over_tp(rows[r]) for r in range(1, num_ep)}
     affine = [norm_gain[None], norm_bias[None]]
     affine_other = [over_tp(a) for a in affine]
-    weights = fetch((w_gate[0], w_up[0], w_down[0]), rows[bits[1]])
-
-    sums = {}
-    for group in groups(num_ep):
-        kept, sent = run_expert(
-            experts, [rows[r] for r in group], [rows_sib[r] for r in group], weights
-        )
+
+    far = far_places(num_ep)
+    near = over_ep(full, (1, 2))
+    got = {z: over_ep(own, (2 * z, 2 * z)) for z in far}
+    near_other = over_tp(near)
+    near_across = over_ep(near, (None, 1))
+    near_across_other = over_tp(near_across, ((1, 0),))
+    weights = fetch((w_gate[0], w_up[0], w_down[0]), near)
+
+    blocks = (full, near, near_other, near_across, near_across_other)
+    kept, sent = run_expert(experts, blocks, near_blocks, 2 * tok_rows, weights)
+    came = over_tp(sent)
+    kinds = (shape((tok_rows, width), f32), shape((tok_rows, width), bf16))
+    near_here, near_there = small_call(join_kernel, kinds, kept, came)
+    here, there = {}, {}
+    for z in far:
+        across = over_ep(got[z], (1, 1))
+        blocks = (got[z], across, over_tp(got[z]), over_tp(across))
+        kept, sent = run_expert(experts, blocks, as_given, 2 * share, weights)
         came = over_tp(sent)
-        kinds = tuple(jax.ShapeDtypeStruct((share, width), bf16 if r & 1 else f32) for r in group)
-        sums |= dict(zip(group, small_call(join_kernel, kinds, kept, came)))
-    terms = []
-    for flip in reversed(bits):
-        for r in sorted(sums, reverse=True):
-            if r & flip:
-                came = over_ep(sums.pop(r), flip)
-                left = r ^ flip
-                if left == 0:
-                    terms.append(came)
-                    continue
-                sends = (left & -left) == flip * 2
-                kind = jax.ShapeDtypeStruct((share, width), bf16 if sends else f32)
-                sums[left] = small_call(add_kernel, kind, sums[left], came)
-    terms.append(sums[0])
-    out = jax.ShapeDtypeStruct((share, half), bf16)
-    stay, go = small_call(functools.partial(norm_kernel, len(terms)), (out, out), *terms, own, *affine, *affine_other)
+        kinds = (shape((share, width), f32), shape((share, width), bf16))
+        here[z], there[z] = small_call(join_kernel, kinds, kept, came)
+
+    came = over_ep(near_there, (1, 1))
+    total = small_call(add_kernel, shape((tok_rows, width), bf16), near_here, came)
+    came = over_ep(total, (None, 2))
+    part = shape((share, width), bf16)
+    stay, go = small_call(cut_kernel, (part, part), total, came)
+    terms = [stay, over_tp(go)]
+    for z in far:
+        came = over_ep(there[z], (1, 1))
+        total = small_call(add_kernel, shape((share, width), bf16), here[z], came)
+        terms.append(over_ep(total, (2 * z, 2 * z)))
+
+    out = shape((share, half), bf16)
+    stay, go = small_call(
+        functools.partial(norm_kernel, len(terms)), (out, out), *terms, own, *affine, *affine_other
+    )
     came = over_tp(go)
     first = lax.axis_index("tp") == 0
     return jnp.concatenate([jnp.where(first, stay, came), jnp.where(first, came, stay)], axis=0)
 
 
-def flips(num_ep):
-    bits = []
-    flip = num_ep // 2
-    while flip:
-        bits.append(flip)
-        flip //= 2
-    return bits
-
-
-def groups(num_ep):
-    far = num_ep // 2
-    return [tuple(range(far))] + [(r, r + 1) for r in range(far, num_ep, 2)]
+def far_places(num_ep):
+    return list(range(num_ep // 2 - 1, 1, -1))
 
 
 def shards(tokens, routes, gate_weights, w_gate, w_up, w_down, norm_gain, norm_bias):

time: 55.2 us -> 76.1 us (1.38)
  waiting for transfers between devices: 19.1 us -> 36.6 us
  starting transfers between devices: 24.3 us -> 27.6 us
    ppermute x27 -> x25, waiting for transfers between devices: 19.1 us -> 36.6 us  [the longest x12 33.3 us: over_ep(): return lax.ppermute(x, ('ep', 'tp'), pairs)]
    ppermute x27 -> x25, starting transfers between devices: 24.3 us -> 27.6 us  [the longest x12 18.6 us: over_ep(): return lax.ppermute(x, ('ep', 'tp'), pairs)]
  transfers between devices with their start and end apart: 27 -> 25, of which waited for: 11 -> 12; matrix products, arithmetic and copies ran while one was open for 0% -> 0% of each run, Pallas kernels for 17% -> 9%
where the time goes in v2:
time: 76.1 us; the launch traced here: 75.9 us
  waiting for transfers between devices  36.6 us (48%)
  starting transfers between devices  27.6 us (36%)
  Pallas kernels  10.8 us (14%)
    ppermute x12, waiting for transfers between devices, over_ep(): return lax.ppermute(x, ('ep', 'tp'), pairs)  33.3 us
    ppermute x12, starting transfers between devices, over_ep(): return lax.ppermute(x, ('ep', 'tp'), pairs)  18.6 us
    ppermute x13, starting transfers between devices, over_tp(): return lax.ppermute(x, 'tp', pairs)  9.02 us
    pallas_call x3, Pallas kernels, run_expert(): pl.pallas_call(functools.partial(expert_kernel, experts, width, arrange),...  5.8 us
    pallas_call x1, Pallas kernels, fetch(): pl.pallas_call(fetch_kernel, out_shape=tuple((pltpu.VMEM(w.shape, w.dtype...  3.34 us
    ppermute x13, waiting for transfers between devices, over_tp(): return lax.ppermute(x, 'tp', pairs)  3.32 us
  transfers between devices with their start and end apart: 25, of which 12 were waited for; matrix products, arithmetic and copies ran while one was open for 0% of the time, Pallas kernels for 9%

profile of v2, /device:TPU:0, one launch (start us, length us, event | category | flops | bytes accessed | tf_op | source)
XLA Modules:
  0.0 75.9 jit_solution(2357277008388501110)
XLA Ops:
  1.0 3.1 %collective-permute-start = (bf16[64,2176]{1,0:T(8,128)(2,1)S(1)}, bf16[64,2176]{1,0:T(8,128)(2,1)S(1)}, u32[]{:S(2)}, u32[]{:S(2)}) collective-permute-start(bf16[64,2176]{1,0:T(8,128)(2,1)S(1)} %get-tuple-element.26.refs_0_), channel_id=1, source_target_pairs={{0,2},{1,5},{2,0},{3,7},{4,6},{5,1},{6,4},{7,3},{8,10},{9,13},{10,... | collective-permute-start | bytes 835592 | tf_op jit(solution)/shard_map/ppermute | solution.py:257
  4.1 4.5 %collective-permute-done.refs_3_.refs_1_ = bf16[64,2176]{1,0:T(8,128)(2,1)S(1)} collective-permute-done((bf16[64,2176]{1,0:T(8,128)(2,1)S(1)}, bf16[64,2176]{1,0:T(8,128)(2,1)S(1)}, u32[]{:S(2)}, u32[]{:S(2)}) %collective-permute-start) | collective-permute-done | bytes 278560 | tf_op jit(solution)/shard_map/ppermute | solution.py:257
  9.3 2.0 %collective-permute-start.1 = (bf16[64,2176]{1,0:T(8,128)(2,1)S(1)}, bf16[64,2176]{1,0:T(8,128)(2,1)S(1)}, u32[]{:S(2)}, u32[]{:S(2)}) collective-permute-start(bf16[64,2176]{1,0:T(8,128)(2,1)S(1)} %collective-permute-done.refs_3_.refs_1_), channel_id=1, source_target_pairs={{0,1},{1,0},{2,3},{3,2},{4,5},{5,4},{6,7},{7,6},{8,9},{9,8},{10,11... | collective-permute-start | bytes 835592 | tf_op jit(solution)/shard_map/ppermute | solution.py:260
  11.3 1.3 %collective-permute-start.3 = (bf16[64,2176]{1,0:T(8,128)(2,1)S(1)}, bf16[64,2176]{1,0:T(8,128)(2,1)S(1)}, u32[]{:S(2)}, u32[]{:S(2)}) collective-permute-start(bf16[64,2176]{1,0:T(8,128)(2,1)S(1)} %collective-permute-done.2.refs_3_), channel_id=1, source_target_pairs={{1,0},{3,2},{5,4},{7,6},{9,8},{11,10},{13,12},{15,14},{17,16},{19,... | collective-permute-start | bytes 835592 | tf_op jit(solution)/shard_map/ppermute | solution.py:260
  12.6 3.3 %fetch.1 = (bf16[2048,640]{1,0:T(8,128)(2,1)S(1)}, bf16[2048,640]{1,0:T(8,128)(2,1)S(1)}, bf16[640,2048]{1,0:T(8,128)(2,1)S(1)}) custom-call(bf16[2048,640]{1,0:T(8,128)(2,1)} %bitcast.11, bf16[2048,640]{1,0:T(8,128)(2,1)} %bitcast.12, bf16[640,2048]{1,0:T(8,128)(2,1)} %bitcast.13, bf16[64,2176]{1,0:T(8,128)(2,1)S(1)} %collective-permute-done.refs_3_.refs_1_), custom_call_target="tpu_custom_call" | custom-call | flops 1073741824 | bytes 8388608 | tf_op jit(solution)/shard_map/fetch/pallas_call | solution.py:172
  16.0 1.6 %collective-permute-done.3.refs_4_ = bf16[64,2176]{1,0:T(8,128)(2,1)S(1)} collective-permute-done((bf16[64,2176]{1,0:T(8,128)(2,1)S(1)}, bf16[64,2176]{1,0:T(8,128)(2,1)S(1)}, u32[]{:S(2)}, u32[]{:S(2)}) %collective-permute-start.3) | collective-permute-done | bytes 278560 | tf_op jit(solution)/shard_map/ppermute | solution.py:260
  17.5 2.7 %expert.3 = (f32[128,2048]{1,0:T(8,128)S(1)}, bf16[128,2048]{1,0:T(8,128)(2,1)S(1)}) custom-call(bf16[64,2176]{1,0:T(8,128)(2,1)S(1)} %get-tuple-element.26.refs_0_, bf16[64,2176]{1,0:T(8,128)(2,1)S(1)} %collective-permute-done.refs_3_.refs_1_, bf16[64,2176]{1,0:T(8,128)(2,1)S(1)} %collective-permute-done.1.refs_2_, ...), custom_call_target="tpu_custom_call" | custom-call | flops 2013265920 | bytes 8388608 | tf_op jit(solution)/shard_map/expert/pallas_call | solution.py:140
  20.2 2.4 %collective-permute-start.4 = (bf16[128,2048]{1,0:T(8,128)(2,1)S(1)}, bf16[128,2048]{1,0:T(8,128)(2,1)S(1)}, u32[]{:S(2)}, u32[]{:S(2)}) collective-permute-start(bf16[128,2048]{1,0:T(8,128)(2,1)S(1)} %get-tuple-element.31), channel_id=1, source_target_pairs={{0,1},{1,0},{2,3},{3,2},{4,5},{5,4},{6,7},{7,6},{8,9},{9,8},{10,11... | collective-permute-start | bytes 1572872 | tf_op jit(solution)/shard_map/ppermute | solution.py:260
  22.7 3.8 %collective-permute-start.8 = (bf16[32,2176]{1,0:T(8,128)(2,1)S(1)}, bf16[32,2176]{1,0:T(8,128)(2,1)S(1)}, u32[]{:S(2)}, u32[]{:S(2)}) collective-permute-start(bf16[32,2176]{1,0:T(8,128)(2,1)S(1)} %get-tuple-element.36.refs_4_), channel_id=1, source_target_pairs={{0,12},{1,13},{2,14},{3,15},{4,8},{5,9},{6,10},{7,11},{8,4},{9,5},... | collective-permute-start | bytes 417800 | tf_op jit(solution)/shard_map/ppermute | solution.py:257
  26.4 4.7 %collective-permute-done.8.refs_0_ = bf16[32,2176]{1,0:T(8,128)(2,1)S(1)} collective-permute-done((bf16[32,2176]{1,0:T(8,128)(2,1)S(1)}, bf16[32,2176]{1,0:T(8,128)(2,1)S(1)}, u32[]{:S(2)}, u32[]{:S(2)}) %collective-permute-start.8) | collective-permute-done | bytes 139296 | tf_op jit(solution)/shard_map/ppermute | solution.py:257
  31.1 1.7 %collective-permute-start.9 = (bf16[32,2176]{1,0:T(8,128)(2,1)S(1)}, bf16[32,2176]{1,0:T(8,128)(2,1)S(1)}, u32[]{:S(2)}, u32[]{:S(2)}) collective-permute-start(bf16[32,2176]{1,0:T(8,128)(2,1)S(1)} %collective-permute-done.8.refs_0_), channel_id=1, source_target_pairs={{0,2},{1,3},{2,0},{3,1},{4,6},{5,7},{6,4},{7,5},{8,10},{9,11},{10,... | collective-permute-start | bytes 417800 | tf_op jit(solution)/shard_map/ppermute | solution.py:257
  32.8 5.7 %collective-permute-done.15.refs_0_ = bf16[32,2176]{1,0:T(8,128)(2,1)S(1)} collective-permute-done((bf16[32,2176]{1,0:T(8,128)(2,1)S(1)}, bf16[32,2176]{1,0:T(8,128)(2,1)S(1)}, u32[]{:S(2)}, u32[]{:S(2)}) %collective-permute-start.15) | collective-permute-done | bytes 139296 | tf_op jit(solution)/shard_map/ppermute | solution.py:257
  38.4 1.5 %collective-permute-start.16 = (bf16[32,2176]{1,0:T(8,128)(2,1)S(1)}, bf16[32,2176]{1,0:T(8,128)(2,1)S(1)}, u32[]{:S(2)}, u32[]{:S(2)}) collective-permute-start(bf16[32,2176]{1,0:T(8,128)(2,1)S(1)} %collective-permute-done.15.refs_0_), channel_id=1, source_target_pairs={{0,2},{1,3},{2,0},{3,1},{4,6},{5,7},{6,4},{7,5},{8,10},{9,11},{10,... | collective-permute-start | bytes 417800 | tf_op jit(solution)/shard_map/ppermute | solution.py:257
  40.5 3.0 %collective-permute-done.16.refs_1_ = bf16[32,2176]{1,0:T(8,128)(2,1)S(1)} collective-permute-done((bf16[32,2176]{1,0:T(8,128)(2,1)S(1)}, bf16[32,2176]{1,0:T(8,128)(2,1)S(1)}, u32[]{:S(2)}, u32[]{:S(2)}) %collective-permute-start.16) | collective-permute-done | bytes 139296 | tf_op jit(solution)/shard_map/ppermute | solution.py:257
  43.6 1.6 %collective-permute-start.5 = (bf16[64,2048]{1,0:T(8,128)(2,1)S(1)}, bf16[64,2048]{1,0:T(8,128)(2,1)S(1)}, u32[]{:S(2)}, u32[]{:S(2)}) collective-permute-start(bf16[64,2048]{1,0:T(8,128)(2,1)S(1)} %get-tuple-element.33), channel_id=1, source_target_pairs={{0,2},{1,3},{2,0},{3,1},{4,6},{5,7},{6,4},{7,5},{8,10},{9,11},{10,... | collective-permute-start | bytes 786440 | tf_op jit(solution)/shard_map/ppermute | solution.py:257
  45.2 1.6 %expert.4 = (f32[64,2048]{1,0:T(8,128)S(1)}, bf16[64,2048]{1,0:T(8,128)(2,1)S(1)}) custom-call(bf16[32,2176]{1,0:T(8,128)(2,1)S(1)} %collective-permute-done.8.refs_0_, bf16[32,2176]{1,0:T(8,128)(2,1)S(1)} %collective-permute-done.9.refs_1_, bf16[32,2176]{1,0:T(8,128)(2,1)S(1)} %collective-permute-done.10.refs_2_, ...), custom_call_target="tpu_custom_call" | custom-call | flops 1006632960 | bytes 8388608 | tf_op jit(solution)/shard_map/expert/pallas_call | solution.py:140
  47.1 1.6 %expert.5 = (f32[64,2048]{1,0:T(8,128)S(1)}, bf16[64,2048]{1,0:T(8,128)(2,1)S(1)}) custom-call(bf16[32,2176]{1,0:T(8,128)(2,1)S(1)} %collective-permute-done.15.refs_0_, bf16[32,2176]{1,0:T(8,128)(2,1)S(1)} %collective-permute-done.16.refs_1_, bf16[32,2176]{1,0:T(8,128)(2,1)S(1)} %collective-permute-done.17.refs_2_, ...), custom_call_target="tpu_custom_call" | custom-call | flops 1006632960 | bytes 8388608 | tf_op jit(solution)/shard_map/expert/pallas_call | solution.py:140
  49.0 3.4 %collective-permute-done.5.came_ref = bf16[64,2048]{1,0:T(8,128)(2,1)S(1)} collective-permute-done((bf16[64,2048]{1,0:T(8,128)(2,1)S(1)}, bf16[64,2048]{1,0:T(8,128)(2,1)S(1)}, u32[]{:S(2)}, u32[]{:S(2)}) %collective-permute-start.5) | collective-permute-done | bytes 262176 | tf_op jit(solution)/shard_map/ppermute | solution.py:257
  53.2 1.6 %collective-permute-start.13 = (bf16[32,2048]{1,0:T(8,128)(2,1)S(1)}, bf16[32,2048]{1,0:T(8,128)(2,1)S(1)}, u32[]{:S(2)}, u32[]{:S(2)}) collective-permute-start(bf16[32,2048]{1,0:T(8,128)(2,1)S(1)} %get-tuple-element.40), channel_id=1, source_target_pairs={{0,2},{1,3},{2,0},{3,1},{4,6},{5,7},{6,4},{7,5},{8,10},{9,11},{10,... | collective-permute-start | bytes 393224 | tf_op jit(solution)/shard_map/ppermute | solution.py:257
  55.4 3.7 %collective-permute-done.13.came_ref = bf16[32,2048]{1,0:T(8,128)(2,1)S(1)} collective-permute-done((bf16[32,2048]{1,0:T(8,128)(2,1)S(1)}, bf16[32,2048]{1,0:T(8,128)(2,1)S(1)}, u32[]{:S(2)}, u32[]{:S(2)}) %collective-permute-start.13) | collective-permute-done | bytes 131104 | tf_op jit(solution)/shard_map/ppermute | solution.py:257
  59.1 3.1 %collective-permute-start.14 = (bf16[32,2048]{1,0:T(8,128)(2,1)S(1)}, bf16[32,2048]{1,0:T(8,128)(2,1)S(1)}, u32[]{:S(2)}, u32[]{:S(2)}) collective-permute-start(bf16[32,2048]{1,0:T(8,128)(2,1)S(1)} %shard_map.86), channel_id=1, source_target_pairs={{0,12},{1,13},{2,14},{3,15},{4,8},{5,9},{6,10},{7,11},{8,4},{9,5},... | collective-permute-start | bytes 393224 | tf_op jit(solution)/shard_map/ppermute | solution.py:257
  62.7 1.1 %collective-permute-start.7 = (bf16[32,2048]{1,0:T(8,128)(2,1)S(1)}, bf16[32,2048]{1,0:T(8,128)(2,1)S(1)}, u32[]{:S(2)}, u32[]{:S(2)}) collective-permute-start(bf16[32,2048]{1,0:T(8,128)(2,1)S(1)} %get-tuple-element.35), channel_id=1, source_target_pairs={{0,1},{1,0},{2,3},{3,2},{4,5},{5,4},{6,7},{7,6},{8,9},{9,8},{10,11... | collective-permute-start | bytes 393224 | tf_op jit(solution)/shard_map/ppermute | solution.py:260
  65.1 2.2 %collective-permute-done.14.refs_2_ = bf16[32,2048]{1,0:T(8,128)(2,1)S(1)} collective-permute-done((bf16[32,2048]{1,0:T(8,128)(2,1)S(1)}, bf16[32,2048]{1,0:T(8,128)(2,1)S(1)}, u32[]{:S(2)}, u32[]{:S(2)}) %collective-permute-start.14) | collective-permute-done | bytes 131104 | tf_op jit(solution)/shard_map/ppermute | solution.py:257
  67.3 6.1 %collective-permute-done.21.refs_3_ = bf16[32,2048]{1,0:T(8,128)(2,1)S(1)} collective-permute-done((bf16[32,2048]{1,0:T(8,128)(2,1)S(1)}, bf16[32,2048]{1,0:T(8,128)(2,1)S(1)}, u32[]{:S(2)}, u32[]{:S(2)}) %collective-permute-start.21) | collective-permute-done | bytes 131104 | tf_op jit(solution)/shard_map/ppermute | solution.py:257
  (45 shorter events, 8.7 us)
Async XLA Ops:
  1.0 7.6 %collective-permute-start = (bf16[64,2176]{1,0:T(8,128)(2,1)S(1)}, bf16[64,2176]{1,0:T(8,128)(2,1)S(1)}, u32[]{:S(2)}, u32[]{:S(2)}) collective-permute-start(bf16[64,2176]{1,0:T(8,128)(2,1)S(1)} %get-tuple-element.26.refs_0_), channel_id=1, source_target_pairs={{0,2},{1,5},{2,0},{3,7},{4,6},{5,1},{6,4},{7,3},{8,10},{9,13},{10,... | collective-permute-start | bytes 835592 | tf_op jit(solution)/shard_map/ppermute | solution.py:257
  8.6 2.7 %collective-permute-start.2 = (bf16[64,2176]{1,0:T(8,128)(2,1)S(1)}, bf16[64,2176]{1,0:T(8,128)(2,1)S(1)}, u32[]{:S(2)}, u32[]{:S(2)}) collective-permute-start(bf16[64,2176]{1,0:T(8,128)(2,1)S(1)} %collective-permute-done.refs_3_.refs_1_), channel_id=1, source_target_pairs={{1,3},{3,1},{5,7},{7,5},{9,11},{11,9},{13,15},{15,13},{17,19},{19,... | collective-permute-start | bytes 835592 | tf_op jit(solution)/shard_map/ppermute | solution.py:257
  9.3 6.7 %collective-permute-start.1 = (bf16[64,2176]{1,0:T(8,128)(2,1)S(1)}, bf16[64,2176]{1,0:T(8,128)(2,1)S(1)}, u32[]{:S(2)}, u32[]{:S(2)}) collective-permute-start(bf16[64,2176]{1,0:T(8,128)(2,1)S(1)} %collective-permute-done.refs_3_.refs_1_), channel_id=1, source_target_pairs={{0,1},{1,0},{2,3},{3,2},{4,5},{5,4},{6,7},{7,6},{8,9},{9,8},{10,11... | collective-permute-start | bytes 835592 | tf_op jit(solution)/shard_map/ppermute | solution.py:260
  11.3 6.2 %collective-permute-start.3 = (bf16[64,2176]{1,0:T(8,128)(2,1)S(1)}, bf16[64,2176]{1,0:T(8,128)(2,1)S(1)}, u32[]{:S(2)}, u32[]{:S(2)}) collective-permute-start(bf16[64,2176]{1,0:T(8,128)(2,1)S(1)} %collective-permute-done.2.refs_3_), channel_id=1, source_target_pairs={{1,0},{3,2},{5,4},{7,6},{9,8},{11,10},{13,12},{15,14},{17,16},{19,... | collective-permute-start | bytes 835592 | tf_op jit(solution)/shard_map/ppermute | solution.py:260
  20.2 23.3 %collective-permute-start.4 = (bf16[128,2048]{1,0:T(8,128)(2,1)S(1)}, bf16[128,2048]{1,0:T(8,128)(2,1)S(1)}, u32[]{:S(2)}, u32[]{:S(2)}) collective-permute-start(bf16[128,2048]{1,0:T(8,128)(2,1)S(1)} %get-tuple-element.31), channel_id=1, source_target_pairs={{0,1},{1,0},{2,3},{3,2},{4,5},{5,4},{6,7},{7,6},{8,9},{9,8},{10,11... | collective-permute-start | bytes 1572872 | tf_op jit(solution)/shard_map/ppermute | solution.py:260
  22.7 8.4 %collective-permute-start.8 = (bf16[32,2176]{1,0:T(8,128)(2,1)S(1)}, bf16[32,2176]{1,0:T(8,128)(2,1)S(1)}, u32[]{:S(2)}, u32[]{:S(2)}) collective-permute-start(bf16[32,2176]{1,0:T(8,128)(2,1)S(1)} %get-tuple-element.36.refs_4_), channel_id=1, source_target_pairs={{0,12},{1,13},{2,14},{3,15},{4,8},{5,9},{6,10},{7,11},{8,4},{9,5},... | collective-permute-start | bytes 417800 | tf_op jit(solution)/shard_map/ppermute | solution.py:257
  26.4 12.0 %collective-permute-start.15 = (bf16[32,2176]{1,0:T(8,128)(2,1)S(1)}, bf16[32,2176]{1,0:T(8,128)(2,1)S(1)}, u32[]{:S(2)}, u32[]{:S(2)}) collective-permute-start(bf16[32,2176]{1,0:T(8,128)(2,1)S(1)} %get-tuple-element.36.refs_4_), channel_id=1, source_target_pairs={{0,8},{1,9},{2,10},{3,11},{4,12},{5,13},{6,14},{7,15},{8,0},{9,1},... | collective-permute-start | bytes 417800 | tf_op jit(solution)/shard_map/ppermute | solution.py:257
  31.1 8.9 %collective-permute-start.9 = (bf16[32,2176]{1,0:T(8,128)(2,1)S(1)}, bf16[32,2176]{1,0:T(8,128)(2,1)S(1)}, u32[]{:S(2)}, u32[]{:S(2)}) collective-permute-start(bf16[32,2176]{1,0:T(8,128)(2,1)S(1)} %collective-permute-done.8.refs_0_), channel_id=1, source_target_pairs={{0,2},{1,3},{2,0},{3,1},{4,6},{5,7},{6,4},{7,5},{8,10},{9,11},{10,... | collective-permute-start | bytes 417800 | tf_op jit(solution)/shard_map/ppermute | solution.py:257
  38.4 5.1 %collective-permute-start.16 = (bf16[32,2176]{1,0:T(8,128)(2,1)S(1)}, bf16[32,2176]{1,0:T(8,128)(2,1)S(1)}, u32[]{:S(2)}, u32[]{:S(2)}) collective-permute-start(bf16[32,2176]{1,0:T(8,128)(2,1)S(1)} %collective-permute-done.15.refs_0_), channel_id=1, source_target_pairs={{0,2},{1,3},{2,0},{3,1},{4,6},{5,7},{6,4},{7,5},{8,10},{9,11},{10,... | collective-permute-start | bytes 417800 | tf_op jit(solution)/shard_map/ppermute | solution.py:257
  40.0 5.2 %collective-permute-start.10 = (bf16[32,2176]{1,0:T(8,128)(2,1)S(1)}, bf16[32,2176]{1,0:T(8,128)(2,1)S(1)}, u32[]{:S(2)}, u32[]{:S(2)}) collective-permute-start(bf16[32,2176]{1,0:T(8,128)(2,1)S(1)} %collective-permute-done.8.refs_0_), channel_id=1, source_target_pairs={{0,1},{1,0},{2,3},{3,2},{4,5},{5,4},{6,7},{7,6},{8,9},{9,8},{10,11... | collective-permute-start | bytes 417800 | tf_op jit(solution)/shard_map/ppermute | solution.py:260
  40.0 5.2 %collective-permute-start.11 = (bf16[32,2176]{1,0:T(8,128)(2,1)S(1)}, bf16[32,2176]{1,0:T(8,128)(2,1)S(1)}, u32[]{:S(2)}, u32[]{:S(2)}) collective-permute-start(bf16[32,2176]{1,0:T(8,128)(2,1)S(1)} %collective-permute-done.9.refs_1_), channel_id=1, source_target_pairs={{0,1},{1,0},{2,3},{3,2},{4,5},{5,4},{6,7},{7,6},{8,9},{9,8},{10,11... | collective-permute-start | bytes 417800 | tf_op jit(solution)/shard_map/ppermute | solution.py:260
  40.5 6.6 %collective-permute-start.17 = (bf16[32,2176]{1,0:T(8,128)(2,1)S(1)}, bf16[32,2176]{1,0:T(8,128)(2,1)S(1)}, u32[]{:S(2)}, u32[]{:S(2)}) collective-permute-start(bf16[32,2176]{1,0:T(8,128)(2,1)S(1)} %collective-permute-done.15.refs_0_), channel_id=1, source_target_pairs={{0,1},{1,0},{2,3},{3,2},{4,5},{5,4},{6,7},{7,6},{8,9},{9,8},{10,11... | collective-permute-start | bytes 417800 | tf_op jit(solution)/shard_map/ppermute | solution.py:260
  43.5 3.6 %collective-permute-start.18 = (bf16[32,2176]{1,0:T(8,128)(2,1)S(1)}, bf16[32,2176]{1,0:T(8,128)(2,1)S(1)}, u32[]{:S(2)}, u32[]{:S(2)}) collective-permute-start(bf16[32,2176]{1,0:T(8,128)(2,1)S(1)} %collective-permute-done.16.refs_1_), channel_id=1, source_target_pairs={{0,1},{1,0},{2,3},{3,2},{4,5},{5,4},{6,7},{7,6},{8,9},{9,8},{10,11... | collective-permute-start | bytes 417800 | tf_op jit(solution)/shard_map/ppermute | solution.py:260
  43.6 8.8 %collective-permute-start.5 = (bf16[64,2048]{1,0:T(8,128)(2,1)S(1)}, bf16[64,2048]{1,0:T(8,128)(2,1)S(1)}, u32[]{:S(2)}, u32[]{:S(2)}) collective-permute-start(bf16[64,2048]{1,0:T(8,128)(2,1)S(1)} %get-tuple-element.33), channel_id=1, source_target_pairs={{0,2},{1,3},{2,0},{3,1},{4,6},{5,7},{6,4},{7,5},{8,10},{9,11},{10,... | collective-permute-start | bytes 786440 | tf_op jit(solution)/shard_map/ppermute | solution.py:257
  46.8 6.4 %collective-permute-start.12 = (bf16[64,2048]{1,0:T(8,128)(2,1)S(1)}, bf16[64,2048]{1,0:T(8,128)(2,1)S(1)}, u32[]{:S(2)}, u32[]{:S(2)}) collective-permute-start(bf16[64,2048]{1,0:T(8,128)(2,1)S(1)} %get-tuple-element.38), channel_id=1, source_target_pairs={{0,1},{1,0},{2,3},{3,2},{4,5},{5,4},{6,7},{7,6},{8,9},{9,8},{10,11... | collective-permute-start | bytes 786440 | tf_op jit(solution)/shard_map/ppermute | solution.py:260
  48.6 6.1 %collective-permute-start.19 = (bf16[64,2048]{1,0:T(8,128)(2,1)S(1)}, bf16[64,2048]{1,0:T(8,128)(2,1)S(1)}, u32[]{:S(2)}, u32[]{:S(2)}) collective-permute-start(bf16[64,2048]{1,0:T(8,128)(2,1)S(1)} %get-tuple-element.42), channel_id=1, source_target_pairs={{0,1},{1,0},{2,3},{3,2},{4,5},{5,4},{6,7},{7,6},{8,9},{9,8},{10,11... | collective-permute-start | bytes 786440 | tf_op jit(solution)/shard_map/ppermute | solution.py:260
  52.4 10.2 %collective-permute-start.6 = (bf16[64,2048]{1,0:T(8,128)(2,1)S(1)}, bf16[64,2048]{1,0:T(8,128)(2,1)S(1)}, u32[]{:S(2)}, u32[]{:S(2)}) collective-permute-start(bf16[64,2048]{1,0:T(8,128)(2,1)S(1)} %shard_map.83.here_ref), channel_id=1, source_target_pairs={{1,5},{3,7},{5,1},{7,3},{9,13},{11,15},{13,9},{15,11},{17,21},{19,... | collective-permute-start | bytes 786440 | tf_op jit(solution)/shard_map/ppermute | solution.py:257
  53.2 5.9 %collective-permute-start.13 = (bf16[32,2048]{1,0:T(8,128)(2,1)S(1)}, bf16[32,2048]{1,0:T(8,128)(2,1)S(1)}, u32[]{:S(2)}, u32[]{:S(2)}) collective-permute-start(bf16[32,2048]{1,0:T(8,128)(2,1)S(1)} %get-tuple-element.40), channel_id=1, source_target_pairs={{0,2},{1,3},{2,0},{3,1},{4,6},{5,7},{6,4},{7,5},{8,10},{9,11},{10,... | collective-permute-start | bytes 393224 | tf_op jit(solution)/shard_map/ppermute | solution.py:257
  54.8 7.4 %collective-permute-start.20 = (bf16[32,2048]{1,0:T(8,128)(2,1)S(1)}, bf16[32,2048]{1,0:T(8,128)(2,1)S(1)}, u32[]{:S(2)}, u32[]{:S(2)}) collective-permute-start(bf16[32,2048]{1,0:T(8,128)(2,1)S(1)} %get-tuple-element.44), channel_id=1, source_target_pairs={{0,2},{1,3},{2,0},{3,1},{4,6},{5,7},{6,4},{7,5},{8,10},{9,11},{10,... | collective-permute-start | bytes 393224 | tf_op jit(solution)/shard_map/ppermute | solution.py:257
  59.1 8.2 %collective-permute-start.14 = (bf16[32,2048]{1,0:T(8,128)(2,1)S(1)}, bf16[32,2048]{1,0:T(8,128)(2,1)S(1)}, u32[]{:S(2)}, u32[]{:S(2)}) collective-permute-start(bf16[32,2048]{1,0:T(8,128)(2,1)S(1)} %shard_map.86), channel_id=1, source_target_pairs={{0,12},{1,13},{2,14},{3,15},{4,8},{5,9},{6,10},{7,11},{8,4},{9,5},... | collective-permute-start | bytes 393224 | tf_op jit(solution)/shard_map/ppermute | solution.py:257
  62.2 11.2 %collective-permute-start.21 = (bf16[32,2048]{1,0:T(8,128)(2,1)S(1)}, bf16[32,2048]{1,0:T(8,128)(2,1)S(1)}, u32[]{:S(2)}, u32[]{:S(2)}) collective-permute-start(bf16[32,2048]{1,0:T(8,128)(2,1)S(1)} %shard_map.88), channel_id=1, source_target_pairs={{0,8},{1,9},{2,10},{3,11},{4,12},{5,13},{6,14},{7,15},{8,0},{9,1},... | collective-permute-start | bytes 393224 | tf_op jit(solution)/shard_map/ppermute | solution.py:257
  62.7 10.7 %collective-permute-start.7 = (bf16[32,2048]{1,0:T(8,128)(2,1)S(1)}, bf16[32,2048]{1,0:T(8,128)(2,1)S(1)}, u32[]{:S(2)}, u32[]{:S(2)}) collective-permute-start(bf16[32,2048]{1,0:T(8,128)(2,1)S(1)} %get-tuple-element.35), channel_id=1, source_target_pairs={{0,1},{1,0},{2,3},{3,2},{4,5},{5,4},{6,7},{7,6},{8,9},{9,8},{10,11... | collective-permute-start | bytes 393224 | tf_op jit(solution)/shard_map/ppermute | solution.py:260
  63.9 1.2 %collective-permute-start.23 = (f32[1,1024]{1,0:T(1,128)S(1)}, f32[1,1024]{1,0:T(1,128)S(1)}, u32[]{:S(2)}, u32[]{:S(2)}) collective-permute-start(f32[1,1024]{1,0:T(1,128)S(1)} %bitcast.9), channel_id=1, source_target_pairs={{0,1},{1,0},{2,3},{3,2},{4,5},{5,4},{6,7},{7,6},{8,9},{9,8},{10,11... | collective-permute-start | bytes 12296 | tf_op jit(solution)/shard_map/ppermute | solution.py:260
  73.7 1.5 %collective-permute-start.24 = (bf16[32,1024]{1,0:T(8,128)(2,1)S(1)}, bf16[32,1024]{1,0:T(8,128)(2,1)S(1)}, u32[]{:S(2)}, u32[]{:S(2)}) collective-permute-start(bf16[32,1024]{1,0:T(8,128)(2,1)S(1)} %get-tuple-element.46), channel_id=1, source_target_pairs={{0,1},{1,0},{2,3},{3,2},{4,5},{5,4},{6,7},{7,6},{8,9},{9,8},{10,11... | collective-permute-start | bytes 196616 | tf_op jit(solution)/shard_map/ppermute | solution.py:260
  (3 other events, 31.6 us)

commit v3 on v2

--- a/solution.py
+++ b/solution.py
@@ -128,10 +128,13 @@
 
 
 def near_blocks(own, came, other, across, across_other):
-    first = lax.axis_index("tp") == 0
+    core = lax.axis_index("tp")
+    first = core == 0
+    share = own.shape[0] // 2
     pick = functools.partial(jnp.where, first)
-    across = pick(across_other, across)
-    return pick(own, came), pick(came, across), pick(other, own), pick(across, other)
+    kinds = own, pick(other, came), pick(came, other), pick(across_other, across)
+    low, high = [k[:share] for k in kinds], [k[share:] for k in kinds]
+    return [pick(x, y) for x, y in zip(low + high, high + low)]
 
 
 def run_expert(experts, blocks, arrange, kept, weights):
@@ -203,14 +206,6 @@
 def add_kernel(kept_ref, came_ref, out_ref):
     total = kept_ref[...].astype(jnp.float32) + came_ref[...].astype(jnp.float32)
     out_ref[...] = total.astype(out_ref.dtype)
-
-
-def cut_kernel(here_ref, came_ref, stay_ref, go_ref):
-    share = stay_ref.shape[0]
-    first = lax.axis_index("tp") == 0
-    low, high = here_ref[...], came_ref[...]
-    stay_ref[...] = jnp.where(first, low[:share], high[share:])
-    go_ref[...] = jnp.where(first, low[share:], high[:share])
 
 
 def norm_kernel(count, *refs):
@@ -297,11 +292,9 @@
         here[z], there[z] = small_call(join_kernel, kinds, kept, came)
 
     came = over_ep(near_there, (1, 1))
-    total = small_call(add_kernel, shape((tok_rows, width), bf16), near_here, came)
-    came = over_ep(total, (None, 2))
-    part = shape((share, width), bf16)
-    stay, go = small_call(cut_kernel, (part, part), total, came)
-    terms = [stay, over_tp(go)]
+    kinds = (shape((share, width), f32), shape((share, width), bf16))
+    total, go = small_call(join_kernel, kinds, near_here, came)
+    terms = [total, over_ep(go, (2, 2))]
     for z in far:
         came = over_ep(there[z], (1, 1))
         total = small_call(add_kernel, shape((share, width), bf16), here[z], came)

time: 76.1 us -> 69.8 us (0.917)
  waiting for transfers between devices: 36.6 us -> 29.9 us
    ppermute x12, waiting for transfers between devices: 33.3 us -> 27.8 us  [over_ep(): return lax.ppermute(x, ('ep', 'tp'), pairs)]
    ppermute x13 -> x12, waiting for transfers between devices: 3.32 us -> 2.08 us  [over_tp(): return lax.ppermute(x, 'tp', pairs)]
    ppermute x13 -> x12, starting transfers between devices: 9.02 us -> 9.05 us  [over_tp(): return lax.ppermute(x, 'tp', pairs)]
  transfers between devices with their start and end apart: 25 -> 24, of which waited for: 12 -> 9; matrix products, arithmetic and copies ran while one was open for 0% -> 0% of each run, Pallas kernels for 9% -> 14%
where the time goes in v3:
time: 69.8 us; the launch traced here: 69.6 us
  waiting for transfers between devices  29.9 us (43%)
  starting transfers between devices  28 us (40%)
  Pallas kernels  10.8 us (15%)
    ppermute x12, waiting for transfers between devices, over_ep(): return lax.ppermute(x, ('ep', 'tp'), pairs)  27.8 us
    ppermute x12, starting transfers between devices, over_ep(): return lax.ppermute(x, ('ep', 'tp'), pairs)  19 us
    ppermute x12, starting transfers between devices, over_tp(): return lax.ppermute(x, 'tp', pairs)  9.05 us
    pallas_call x3, Pallas kernels, run_expert(): pl.pallas_call(functools.partial(expert_kernel, experts, width, arrange),...  5.8 us
    pallas_call x1, Pallas kernels, fetch(): pl.pallas_call(fetch_kernel, out_shape=tuple((pltpu.VMEM(w.shape, w.dtype...  3.33 us
    ppermute x12, waiting for transfers between devices, over_tp(): return lax.ppermute(x, 'tp', pairs)  2.08 us
  transfers between devices with their start and end apart: 24, of which 9 were waited for; matrix products, arithmetic and copies ran while one was open for 0% of the time, Pallas kernels for 14%

profile of v3, /device:TPU:0, one launch (start us, length us, event | category | flops | bytes accessed | tf_op | source)
XLA Modules:
  0.0 69.6 jit_solution(15196377665957854751)
XLA Ops:
  0.0 1.0 %rows.1 = (bf16[64,2176]{1,0:T(8,128)(2,1)S(1)}, bf16[32,2176]{1,0:T(8,128)(2,1)S(1)}) custom-call(bf16[64,2048]{1,0:T(8,128)(2,1)} %tokens_hbm.1, s32[4,64]{1,0:T(4,128)} %bitcast.14, f32[4,64]{1,0:T(4,128)} %bitcast.15), custom_call_target="tpu_custom_call" | custom-call | flops 67108864 | bytes 1048576 | tf_op jit(solution)/shard_map/rows/pallas_call | solution.py:259
  1.0 3.1 %collective-permute-start = (bf16[64,2176]{1,0:T(8,128)(2,1)S(1)}, bf16[64,2176]{1,0:T(8,128)(2,1)S(1)}, u32[]{:S(2)}, u32[]{:S(2)}) collective-permute-start(bf16[64,2176]{1,0:T(8,128)(2,1)S(1)} %get-tuple-element.26.refs_0_), channel_id=1, source_target_pairs={{0,2},{1,5},{2,0},{3,7},{4,6},{5,1},{6,4},{7,3},{8,10},{9,13},{10,... | collective-permute-start | bytes 835592 | tf_op jit(solution)/shard_map/ppermute | solution.py:252
  4.1 4.5 %collective-permute-done.refs_3_.refs_1_ = bf16[64,2176]{1,0:T(8,128)(2,1)S(1)} collective-permute-done((bf16[64,2176]{1,0:T(8,128)(2,1)S(1)}, bf16[64,2176]{1,0:T(8,128)(2,1)S(1)}, u32[]{:S(2)}, u32[]{:S(2)}) %collective-permute-start) | collective-permute-done | bytes 278560 | tf_op jit(solution)/shard_map/ppermute | solution.py:252
  8.6 0.7 collective-permute-start.2
  9.3 2.0 %collective-permute-start.1 = (bf16[64,2176]{1,0:T(8,128)(2,1)S(1)}, bf16[64,2176]{1,0:T(8,128)(2,1)S(1)}, u32[]{:S(2)}, u32[]{:S(2)}) collective-permute-start(bf16[64,2176]{1,0:T(8,128)(2,1)S(1)} %collective-permute-done.refs_3_.refs_1_), channel_id=1, source_target_pairs={{0,1},{1,0},{2,3},{3,2},{4,5},{5,4},{6,7},{7,6},{8,9},{9,8},{10,11... | collective-permute-start | bytes 835592 | tf_op jit(solution)/shard_map/ppermute | solution.py:255
  11.3 1.3 %collective-permute-start.3 = (bf16[64,2176]{1,0:T(8,128)(2,1)S(1)}, bf16[64,2176]{1,0:T(8,128)(2,1)S(1)}, u32[]{:S(2)}, u32[]{:S(2)}) collective-permute-start(bf16[64,2176]{1,0:T(8,128)(2,1)S(1)} %collective-permute-done.2.refs_3_), channel_id=1, source_target_pairs={{1,0},{3,2},{5,4},{7,6},{9,8},{11,10},{13,12},{15,14},{17,16},{19,... | collective-permute-start | bytes 835592 | tf_op jit(solution)/shard_map/ppermute | solution.py:255
  12.6 3.7 %collective-permute-start.7 = (bf16[32,2176]{1,0:T(8,128)(2,1)S(1)}, bf16[32,2176]{1,0:T(8,128)(2,1)S(1)}, u32[]{:S(2)}, u32[]{:S(2)}) collective-permute-start(bf16[32,2176]{1,0:T(8,128)(2,1)S(1)} %get-tuple-element.36.refs_4_), channel_id=1, source_target_pairs={{0,12},{1,13},{2,14},{3,15},{4,8},{5,9},{6,10},{7,11},{8,4},{9,5},... | collective-permute-start | bytes 417800 | tf_op jit(solution)/shard_map/ppermute | solution.py:252
  16.3 3.4 %collective-permute-done.7.refs_0_ = bf16[32,2176]{1,0:T(8,128)(2,1)S(1)} collective-permute-done((bf16[32,2176]{1,0:T(8,128)(2,1)S(1)}, bf16[32,2176]{1,0:T(8,128)(2,1)S(1)}, u32[]{:S(2)}, u32[]{:S(2)}) %collective-permute-start.7) | collective-permute-done | bytes 139296 | tf_op jit(solution)/shard_map/ppermute | solution.py:252
  20.0 3.3 %fetch.1 = (bf16[2048,640]{1,0:T(8,128)(2,1)S(1)}, bf16[2048,640]{1,0:T(8,128)(2,1)S(1)}, bf16[640,2048]{1,0:T(8,128)(2,1)S(1)}) custom-call(bf16[2048,640]{1,0:T(8,128)(2,1)} %bitcast.11, bf16[2048,640]{1,0:T(8,128)(2,1)} %bitcast.12, bf16[640,2048]{1,0:T(8,128)(2,1)} %bitcast.13, bf16[64,2176]{1,0:T(8,128)(2,1)S(1)} %collective-permute-done.refs_3_.refs_1_), custom_call_target="tpu_custom_call" | custom-call | flops 1073741824 | bytes 8388608 | tf_op jit(solution)/shard_map/fetch/pallas_call | solution.py:175
  23.3 2.7 %expert.3 = (f32[128,2048]{1,0:T(8,128)S(1)}, bf16[128,2048]{1,0:T(8,128)(2,1)S(1)}) custom-call(bf16[64,2176]{1,0:T(8,128)(2,1)S(1)} %get-tuple-element.26.refs_0_, bf16[64,2176]{1,0:T(8,128)(2,1)S(1)} %collective-permute-done.refs_3_.refs_1_, bf16[64,2176]{1,0:T(8,128)(2,1)S(1)} %collective-permute-done.1.refs_2_, ...), custom_call_target="tpu_custom_call" | custom-call | flops 2013265920 | bytes 8388608 | tf_op jit(solution)/shard_map/expert/pallas_call | solution.py:143
  26.0 4.0 %collective-permute-start.4 = (bf16[128,2048]{1,0:T(8,128)(2,1)S(1)}, bf16[128,2048]{1,0:T(8,128)(2,1)S(1)}, u32[]{:S(2)}, u32[]{:S(2)}) collective-permute-start(bf16[128,2048]{1,0:T(8,128)(2,1)S(1)} %get-tuple-element.31), channel_id=1, source_target_pairs={{0,1},{1,0},{2,3},{3,2},{4,5},{5,4},{6,7},{7,6},{8,9},{9,8},{10,11... | collective-permute-start | bytes 1572872 | tf_op jit(solution)/shard_map/ppermute | solution.py:255
  30.4 0.5 collective-permute-start.10
  30.9 4.7 %collective-permute-done.15.refs_1_ = bf16[32,2176]{1,0:T(8,128)(2,1)S(1)} collective-permute-done((bf16[32,2176]{1,0:T(8,128)(2,1)S(1)}, bf16[32,2176]{1,0:T(8,128)(2,1)S(1)}, u32[]{:S(2)}, u32[]{:S(2)}) %collective-permute-start.15) | collective-permute-done | bytes 139296 | tf_op jit(solution)/shard_map/ppermute | solution.py:252
  35.7 1.5 %expert.4 = (f32[64,2048]{1,0:T(8,128)S(1)}, bf16[64,2048]{1,0:T(8,128)(2,1)S(1)}) custom-call(bf16[32,2176]{1,0:T(8,128)(2,1)S(1)} %collective-permute-done.7.refs_0_, bf16[32,2176]{1,0:T(8,128)(2,1)S(1)} %collective-permute-done.8.refs_1_, bf16[32,2176]{1,0:T(8,128)(2,1)S(1)} %collective-permute-done.9.refs_2_, ...), custom_call_target="tpu_custom_call" | custom-call | flops 1006632960 | bytes 8388608 | tf_op jit(solution)/shard_map/expert/pallas_call | solution.py:143
  37.2 0.6 collective-permute-start.11
  37.8 1.6 %expert.5 = (f32[64,2048]{1,0:T(8,128)S(1)}, bf16[64,2048]{1,0:T(8,128)(2,1)S(1)}) custom-call(bf16[32,2176]{1,0:T(8,128)(2,1)S(1)} %collective-permute-done.14.refs_0_, bf16[32,2176]{1,0:T(8,128)(2,1)S(1)} %collective-permute-done.15.refs_1_, bf16[32,2176]{1,0:T(8,128)(2,1)S(1)} %collective-permute-done.16.refs_2_, ...), custom_call_target="tpu_custom_call" | custom-call | flops 1006632960 | bytes 8388608 | tf_op jit(solution)/shard_map/expert/pallas_call | solution.py:143
  40.1 1.7 %collective-permute-start.12 = (bf16[32,2048]{1,0:T(8,128)(2,1)S(1)}, bf16[32,2048]{1,0:T(8,128)(2,1)S(1)}, u32[]{:S(2)}, u32[]{:S(2)}) collective-permute-start(bf16[32,2048]{1,0:T(8,128)(2,1)S(1)} %get-tuple-element.40), channel_id=1, source_target_pairs={{0,2},{1,3},{2,0},{3,1},{4,6},{5,7},{6,4},{7,5},{8,10},{9,11},{10,... | collective-permute-start | bytes 393224 | tf_op jit(solution)/shard_map/ppermute | solution.py:252
  42.3 9.3 %collective-permute-done.12.came_ref = bf16[32,2048]{1,0:T(8,128)(2,1)S(1)} collective-permute-done((bf16[32,2048]{1,0:T(8,128)(2,1)S(1)}, bf16[32,2048]{1,0:T(8,128)(2,1)S(1)}, u32[]{:S(2)}, u32[]{:S(2)}) %collective-permute-start.12) | collective-permute-done | bytes 131104 | tf_op jit(solution)/shard_map/ppermute | solution.py:252
  51.7 3.6 %collective-permute-start.13 = (bf16[32,2048]{1,0:T(8,128)(2,1)S(1)}, bf16[32,2048]{1,0:T(8,128)(2,1)S(1)}, u32[]{:S(2)}, u32[]{:S(2)}) collective-permute-start(bf16[32,2048]{1,0:T(8,128)(2,1)S(1)} %shard_map.85), channel_id=1, source_target_pairs={{0,12},{1,13},{2,14},{3,15},{4,8},{5,9},{6,10},{7,11},{8,4},{9,5},... | collective-permute-start | bytes 393224 | tf_op jit(solution)/shard_map/ppermute | solution.py:252
  55.3 4.5 %collective-permute-start.20 = (bf16[32,2048]{1,0:T(8,128)(2,1)S(1)}, bf16[32,2048]{1,0:T(8,128)(2,1)S(1)}, u32[]{:S(2)}, u32[]{:S(2)}) collective-permute-start(bf16[32,2048]{1,0:T(8,128)(2,1)S(1)} %shard_map.87), channel_id=1, source_target_pairs={{0,8},{1,9},{2,10},{3,11},{4,12},{5,13},{6,14},{7,15},{8,0},{9,1},... | collective-permute-start | bytes 393224 | tf_op jit(solution)/shard_map/ppermute | solution.py:252
  60.5 0.7 collective-permute-done.21.refs_7_
  61.4 5.7 %collective-permute-done.20.refs_3_ = bf16[32,2048]{1,0:T(8,128)(2,1)S(1)} collective-permute-done((bf16[32,2048]{1,0:T(8,128)(2,1)S(1)}, bf16[32,2048]{1,0:T(8,128)(2,1)S(1)}, u32[]{:S(2)}, u32[]{:S(2)}) %collective-permute-start.20) | collective-permute-done | bytes 131104 | tf_op jit(solution)/shard_map/ppermute | solution.py:252
  67.7 1.2 %collective-permute-done.23 = bf16[32,1024]{1,0:T(8,128)(2,1)S(1)} collective-permute-done((bf16[32,1024]{1,0:T(8,128)(2,1)S(1)}, bf16[32,1024]{1,0:T(8,128)(2,1)S(1)}, u32[]{:S(2)}, u32[]{:S(2)}) %collective-permute-start.23) | collective-permute-done | bytes 65568 | tf_op jit(solution)/shard_map/ppermute | solution.py:255
  69.0 0.7 pad_maximum_fusion
  (42 shorter events, 3.7 us)
Async XLA Ops:
  1.0 7.6 %collective-permute-start = (bf16[64,2176]{1,0:T(8,128)(2,1)S(1)}, bf16[64,2176]{1,0:T(8,128)(2,1)S(1)}, u32[]{:S(2)}, u32[]{:S(2)}) collective-permute-start(bf16[64,2176]{1,0:T(8,128)(2,1)S(1)} %get-tuple-element.26.refs_0_), channel_id=1, source_target_pairs={{0,2},{1,5},{2,0},{3,7},{4,6},{5,1},{6,4},{7,3},{8,10},{9,13},{10,... | collective-permute-start | bytes 835592 | tf_op jit(solution)/shard_map/ppermute | solution.py:252
  8.6 2.7 %collective-permute-start.2 = (bf16[64,2176]{1,0:T(8,128)(2,1)S(1)}, bf16[64,2176]{1,0:T(8,128)(2,1)S(1)}, u32[]{:S(2)}, u32[]{:S(2)}) collective-permute-start(bf16[64,2176]{1,0:T(8,128)(2,1)S(1)} %collective-permute-done.refs_3_.refs_1_), channel_id=1, source_target_pairs={{1,3},{3,1},{5,7},{7,5},{9,11},{11,9},{13,15},{15,13},{17,19},{19,... | collective-permute-start | bytes 835592 | tf_op jit(solution)/shard_map/ppermute | solution.py:252
  9.3 14.0 %collective-permute-start.1 = (bf16[64,2176]{1,0:T(8,128)(2,1)S(1)}, bf16[64,2176]{1,0:T(8,128)(2,1)S(1)}, u32[]{:S(2)}, u32[]{:S(2)}) collective-permute-start(bf16[64,2176]{1,0:T(8,128)(2,1)S(1)} %collective-permute-done.refs_3_.refs_1_), channel_id=1, source_target_pairs={{0,1},{1,0},{2,3},{3,2},{4,5},{5,4},{6,7},{7,6},{8,9},{9,8},{10,11... | collective-permute-start | bytes 835592 | tf_op jit(solution)/shard_map/ppermute | solution.py:255
  11.3 12.0 %collective-permute-start.3 = (bf16[64,2176]{1,0:T(8,128)(2,1)S(1)}, bf16[64,2176]{1,0:T(8,128)(2,1)S(1)}, u32[]{:S(2)}, u32[]{:S(2)}) collective-permute-start(bf16[64,2176]{1,0:T(8,128)(2,1)S(1)} %collective-permute-done.2.refs_3_), channel_id=1, source_target_pairs={{1,0},{3,2},{5,4},{7,6},{9,8},{11,10},{13,12},{15,14},{17,16},{19,... | collective-permute-start | bytes 835592 | tf_op jit(solution)/shard_map/ppermute | solution.py:255
  12.6 7.0 %collective-permute-start.7 = (bf16[32,2176]{1,0:T(8,128)(2,1)S(1)}, bf16[32,2176]{1,0:T(8,128)(2,1)S(1)}, u32[]{:S(2)}, u32[]{:S(2)}) collective-permute-start(bf16[32,2176]{1,0:T(8,128)(2,1)S(1)} %get-tuple-element.36.refs_4_), channel_id=1, source_target_pairs={{0,12},{1,13},{2,14},{3,15},{4,8},{5,9},{6,10},{7,11},{8,4},{9,5},... | collective-permute-start | bytes 417800 | tf_op jit(solution)/shard_map/ppermute | solution.py:252
  16.3 13.7 %collective-permute-start.14 = (bf16[32,2176]{1,0:T(8,128)(2,1)S(1)}, bf16[32,2176]{1,0:T(8,128)(2,1)S(1)}, u32[]{:S(2)}, u32[]{:S(2)}) collective-permute-start(bf16[32,2176]{1,0:T(8,128)(2,1)S(1)} %get-tuple-element.36.refs_4_), channel_id=1, source_target_pairs={{0,8},{1,9},{2,10},{3,11},{4,12},{5,13},{6,14},{7,15},{8,0},{9,1},... | collective-permute-start | bytes 417800 | tf_op jit(solution)/shard_map/ppermute | solution.py:252
  19.6 10.8 %collective-permute-start.8 = (bf16[32,2176]{1,0:T(8,128)(2,1)S(1)}, bf16[32,2176]{1,0:T(8,128)(2,1)S(1)}, u32[]{:S(2)}, u32[]{:S(2)}) collective-permute-start(bf16[32,2176]{1,0:T(8,128)(2,1)S(1)} %collective-permute-done.7.refs_0_), channel_id=1, source_target_pairs={{0,2},{1,3},{2,0},{3,1},{4,6},{5,7},{6,4},{7,5},{8,10},{9,11},{10,... | collective-permute-start | bytes 417800 | tf_op jit(solution)/shard_map/ppermute | solution.py:252
  26.0 13.4 %collective-permute-start.4 = (bf16[128,2048]{1,0:T(8,128)(2,1)S(1)}, bf16[128,2048]{1,0:T(8,128)(2,1)S(1)}, u32[]{:S(2)}, u32[]{:S(2)}) collective-permute-start(bf16[128,2048]{1,0:T(8,128)(2,1)S(1)} %get-tuple-element.31), channel_id=1, source_target_pairs={{0,1},{1,0},{2,3},{3,2},{4,5},{5,4},{6,7},{7,6},{8,9},{9,8},{10,11... | collective-permute-start | bytes 1572872 | tf_op jit(solution)/shard_map/ppermute | solution.py:255
  30.0 5.7 %collective-permute-start.15 = (bf16[32,2176]{1,0:T(8,128)(2,1)S(1)}, bf16[32,2176]{1,0:T(8,128)(2,1)S(1)}, u32[]{:S(2)}, u32[]{:S(2)}) collective-permute-start(bf16[32,2176]{1,0:T(8,128)(2,1)S(1)} %collective-permute-done.14.refs_0_), channel_id=1, source_target_pairs={{0,2},{1,3},{2,0},{3,1},{4,6},{5,7},{6,4},{7,5},{8,10},{9,11},{10,... | collective-permute-start | bytes 417800 | tf_op jit(solution)/shard_map/ppermute | solution.py:252
  30.4 5.2 %collective-permute-start.9 = (bf16[32,2176]{1,0:T(8,128)(2,1)S(1)}, bf16[32,2176]{1,0:T(8,128)(2,1)S(1)}, u32[]{:S(2)}, u32[]{:S(2)}) collective-permute-start(bf16[32,2176]{1,0:T(8,128)(2,1)S(1)} %collective-permute-done.7.refs_0_), channel_id=1, source_target_pairs={{0,1},{1,0},{2,3},{3,2},{4,5},{5,4},{6,7},{7,6},{8,9},{9,8},{10,11... | collective-permute-start | bytes 417800 | tf_op jit(solution)/shard_map/ppermute | solution.py:255
  30.4 5.2 %collective-permute-start.10 = (bf16[32,2176]{1,0:T(8,128)(2,1)S(1)}, bf16[32,2176]{1,0:T(8,128)(2,1)S(1)}, u32[]{:S(2)}, u32[]{:S(2)}) collective-permute-start(bf16[32,2176]{1,0:T(8,128)(2,1)S(1)} %collective-permute-done.8.refs_1_), channel_id=1, source_target_pairs={{0,1},{1,0},{2,3},{3,2},{4,5},{5,4},{6,7},{7,6},{8,9},{9,8},{10,11... | collective-permute-start | bytes 417800 | tf_op jit(solution)/shard_map/ppermute | solution.py:255
  30.9 6.9 %collective-permute-start.16 = (bf16[32,2176]{1,0:T(8,128)(2,1)S(1)}, bf16[32,2176]{1,0:T(8,128)(2,1)S(1)}, u32[]{:S(2)}, u32[]{:S(2)}) collective-permute-start(bf16[32,2176]{1,0:T(8,128)(2,1)S(1)} %collective-permute-done.14.refs_0_), channel_id=1, source_target_pairs={{0,1},{1,0},{2,3},{3,2},{4,5},{5,4},{6,7},{7,6},{8,9},{9,8},{10,11... | collective-permute-start | bytes 417800 | tf_op jit(solution)/shard_map/ppermute | solution.py:255
  35.7 2.1 %collective-permute-start.17 = (bf16[32,2176]{1,0:T(8,128)(2,1)S(1)}, bf16[32,2176]{1,0:T(8,128)(2,1)S(1)}, u32[]{:S(2)}, u32[]{:S(2)}) collective-permute-start(bf16[32,2176]{1,0:T(8,128)(2,1)S(1)} %collective-permute-done.15.refs_1_), channel_id=1, source_target_pairs={{0,1},{1,0},{2,3},{3,2},{4,5},{5,4},{6,7},{7,6},{8,9},{9,8},{10,11... | collective-permute-start | bytes 417800 | tf_op jit(solution)/shard_map/ppermute | solution.py:255
  37.2 2.9 %collective-permute-start.11 = (bf16[64,2048]{1,0:T(8,128)(2,1)S(1)}, bf16[64,2048]{1,0:T(8,128)(2,1)S(1)}, u32[]{:S(2)}, u32[]{:S(2)}) collective-permute-start(bf16[64,2048]{1,0:T(8,128)(2,1)S(1)} %get-tuple-element.38), channel_id=1, source_target_pairs={{0,1},{1,0},{2,3},{3,2},{4,5},{5,4},{6,7},{7,6},{8,9},{9,8},{10,11... | collective-permute-start | bytes 786440 | tf_op jit(solution)/shard_map/ppermute | solution.py:255
  39.4 2.4 %collective-permute-start.18 = (bf16[64,2048]{1,0:T(8,128)(2,1)S(1)}, bf16[64,2048]{1,0:T(8,128)(2,1)S(1)}, u32[]{:S(2)}, u32[]{:S(2)}) collective-permute-start(bf16[64,2048]{1,0:T(8,128)(2,1)S(1)} %get-tuple-element.42), channel_id=1, source_target_pairs={{0,1},{1,0},{2,3},{3,2},{4,5},{5,4},{6,7},{7,6},{8,9},{9,8},{10,11... | collective-permute-start | bytes 786440 | tf_op jit(solution)/shard_map/ppermute | solution.py:255
  39.6 20.2 %collective-permute-start.5 = (bf16[64,2048]{1,0:T(8,128)(2,1)S(1)}, bf16[64,2048]{1,0:T(8,128)(2,1)S(1)}, u32[]{:S(2)}, u32[]{:S(2)}) collective-permute-start(bf16[64,2048]{1,0:T(8,128)(2,1)S(1)} %get-tuple-element.33), channel_id=1, source_target_pairs={{0,2},{1,3},{2,0},{3,1},{4,6},{5,7},{6,4},{7,5},{8,10},{9,11},{10,... | collective-permute-start | bytes 786440 | tf_op jit(solution)/shard_map/ppermute | solution.py:252
  40.1 11.5 %collective-permute-start.12 = (bf16[32,2048]{1,0:T(8,128)(2,1)S(1)}, bf16[32,2048]{1,0:T(8,128)(2,1)S(1)}, u32[]{:S(2)}, u32[]{:S(2)}) collective-permute-start(bf16[32,2048]{1,0:T(8,128)(2,1)S(1)} %get-tuple-element.40), channel_id=1, source_target_pairs={{0,2},{1,3},{2,0},{3,1},{4,6},{5,7},{6,4},{7,5},{8,10},{9,11},{10,... | collective-permute-start | bytes 393224 | tf_op jit(solution)/shard_map/ppermute | solution.py:252
  41.8 13.4 %collective-permute-start.19 = (bf16[32,2048]{1,0:T(8,128)(2,1)S(1)}, bf16[32,2048]{1,0:T(8,128)(2,1)S(1)}, u32[]{:S(2)}, u32[]{:S(2)}) collective-permute-start(bf16[32,2048]{1,0:T(8,128)(2,1)S(1)} %get-tuple-element.44), channel_id=1, source_target_pairs={{0,2},{1,3},{2,0},{3,1},{4,6},{5,7},{6,4},{7,5},{8,10},{9,11},{10,... | collective-permute-start | bytes 393224 | tf_op jit(solution)/shard_map/ppermute | solution.py:252
  51.7 9.7 %collective-permute-start.13 = (bf16[32,2048]{1,0:T(8,128)(2,1)S(1)}, bf16[32,2048]{1,0:T(8,128)(2,1)S(1)}, u32[]{:S(2)}, u32[]{:S(2)}) collective-permute-start(bf16[32,2048]{1,0:T(8,128)(2,1)S(1)} %shard_map.85), channel_id=1, source_target_pairs={{0,12},{1,13},{2,14},{3,15},{4,8},{5,9},{6,10},{7,11},{8,4},{9,5},... | collective-permute-start | bytes 393224 | tf_op jit(solution)/shard_map/ppermute | solution.py:252
  55.3 11.7 %collective-permute-start.20 = (bf16[32,2048]{1,0:T(8,128)(2,1)S(1)}, bf16[32,2048]{1,0:T(8,128)(2,1)S(1)}, u32[]{:S(2)}, u32[]{:S(2)}) collective-permute-start(bf16[32,2048]{1,0:T(8,128)(2,1)S(1)} %shard_map.87), channel_id=1, source_target_pairs={{0,8},{1,9},{2,10},{3,11},{4,12},{5,13},{6,14},{7,15},{8,0},{9,1},... | collective-permute-start | bytes 393224 | tf_op jit(solution)/shard_map/ppermute | solution.py:252
  59.9 7.4 %collective-permute-start.6 = (bf16[32,2048]{1,0:T(8,128)(2,1)S(1)}, bf16[32,2048]{1,0:T(8,128)(2,1)S(1)}, u32[]{:S(2)}, u32[]{:S(2)}) collective-permute-start(bf16[32,2048]{1,0:T(8,128)(2,1)S(1)} %get-tuple-element.35), channel_id=1, source_target_pairs={{0,4},{1,5},{2,6},{3,7},{4,0},{5,1},{6,2},{7,3},{8,12},{9,13},{10,... | collective-permute-start | bytes 393224 | tf_op jit(solution)/shard_map/ppermute | solution.py:252
  59.9 1.2 %collective-permute-start.21 = (f32[1,1024]{1,0:T(1,128)S(1)}, f32[1,1024]{1,0:T(1,128)S(1)}, u32[]{:S(2)}, u32[]{:S(2)}) collective-permute-start(f32[1,1024]{1,0:T(1,128)S(1)} %bitcast.7), channel_id=1, source_target_pairs={{0,1},{1,0},{2,3},{3,2},{4,5},{5,4},{6,7},{7,6},{8,9},{9,8},{10,11... | collective-permute-start | bytes 12296 | tf_op jit(solution)/shard_map/ppermute | solution.py:255
  60.0 1.3 %collective-permute-start.22 = (f32[1,1024]{1,0:T(1,128)S(1)}, f32[1,1024]{1,0:T(1,128)S(1)}, u32[]{:S(2)}, u32[]{:S(2)}) collective-permute-start(f32[1,1024]{1,0:T(1,128)S(1)} %bitcast.9), channel_id=1, source_target_pairs={{0,1},{1,0},{2,3},{3,2},{4,5},{5,4},{6,7},{7,6},{8,9},{9,8},{10,11... | collective-permute-start | bytes 12296 | tf_op jit(solution)/shard_map/ppermute | solution.py:255
  67.6 1.3 %collective-permute-start.23 = (bf16[32,1024]{1,0:T(8,128)(2,1)S(1)}, bf16[32,1024]{1,0:T(8,128)(2,1)S(1)}, u32[]{:S(2)}, u32[]{:S(2)}) collective-permute-start(bf16[32,1024]{1,0:T(8,128)(2,1)S(1)} %get-tuple-element.46), channel_id=1, source_target_pairs={{0,1},{1,0},{2,3},{3,2},{4,5},{5,4},{6,7},{7,6},{8,9},{9,8},{10,11... | collective-permute-start | bytes 196616 | tf_op jit(solution)/shard_map/ppermute | solution.py:255
  (2 other events, 41.2 us)

commit v4 on v3

--- a/solution.py
+++ b/solution.py
@@ -95,8 +95,36 @@
     all_ref[:, :width] = tokens_ref[...]
 
 
-def expert_kernel(experts, width, arrange, *refs):
-    *row_refs, wg_ref, wu_ref, wd_ref, mine_ref, theirs_ref = refs
+def expert_kernel(experts, width, arrange, blocks, extra, fetch, *refs):
+    row_refs, extra_refs = refs[:blocks], refs[blocks : blocks + extra]
+    blocks += extra
+    sources = refs[blocks : blocks + 3]
+    mine_ref, theirs_ref = refs[blocks + 3 : blocks + 5]
+    wg_ref, wu_ref, wd_ref = refs[blocks + 5 : blocks + 8] if fetch else sources
+    ff = wg_ref.shape[1]
+    step, wide = 2 * LANES, 4 * LANES
+    units = [(start, min(step, ff - start)) for start in range(0, ff, step)]
+    copies = {}
+    if fetch:
+        done = refs[blocks + 8]
+
+        def bring(which, start, size):
+            part = pl.ds(start, size)
+            source, target = sources[which].at[:, part], refs[blocks + 5 + which].at[:, part]
+            copies[which, start] = pltpu.make_async_copy(source, target, done.at[len(copies)])
+
+        for start, size in units:
+            bring(0, start, size)
+            bring(1, start, size)
+        for start in range(0, width, wide):
+            bring(2, start, wide)
+        for copy in copies.values():
+            copy.start()
+
+    def ready(which, start):
+        if fetch:
+            copies[which, start].wait()
+
     kept = mine_ref.shape[0]
     packed = jnp.concatenate(arrange(*(r[...] for r in row_refs)), axis=0)
     rows, codes = packed[:, :width], packed[:, width:].astype(jnp.float32)
@@ -104,87 +132,78 @@
     expert = lax.axis_index("ep")
     named = (lane == expert) | (lane == expert + experts)
     weight = jnp.sum(jnp.where(named, codes, 0.0), axis=1, keepdims=True)
-    ff = wg_ref.shape[1]
-    step = 2 * LANES
     dot = functools.partial(jnp.dot, preferred_element_type=jnp.float32)
     hidden = []
-    for start in range(0, ff - step + 1, step):
-        gate = dot(rows, wg_ref[:, start : start + step])
-        upper = dot(rows, wu_ref[:, start : start + step])
+    for start, size in units:
+        ready(0, start)
+        if size == step:
+            gate = dot(rows, wg_ref[:, start : start + size])
+            ready(1, start)
+            upper = dot(rows, wu_ref[:, start : start + size])
+        else:
+            ready(1, start)
+            both = jnp.concatenate([wg_ref[:, start:], wu_ref[:, start:]], axis=1)
+            both = dot(rows, both)
+            gate, upper = both[:, :size], both[:, size:]
         hidden.append((jax.nn.silu(gate) * upper).astype(jnp.bfloat16))
-    rest = ff % step
-    if rest:
-        both = dot(rows, jnp.concatenate([wg_ref[:, ff - rest :], wu_ref[:, ff - rest :]], axis=1))
-        hidden.append((jax.nn.silu(both[:, :rest]) * both[:, rest:]).astype(jnp.bfloat16))
     hidden = jnp.concatenate(hidden, axis=1)
-    for start in range(0, width, 2 * step):
-        out = dot(hidden, wd_ref[:, start : start + 2 * step]) * weight
-        mine_ref[:, start : start + 2 * step] = out[:kept]
-        theirs_ref[:, start : start + 2 * step] = out[kept:].astype(jnp.bfloat16)
+    for start in range(0, width, wide):
+        ready(2, start)
+        out = dot(hidden, wd_ref[:, start : start + wide]) * weight
+        mine_ref[:, start : start + wide] = out[:kept]
+        theirs_ref[:kept, start : start + wide] = out[kept:].astype(jnp.bfloat16)
+    for ref in extra_refs:
+        theirs_ref[kept:] = ref[...]
 
 
 def as_given(*blocks):
     return blocks
 
 
-def near_blocks(own, came, other, across, across_other):
-    core = lax.axis_index("tp")
-    first = core == 0
-    share = own.shape[0] // 2
-    pick = functools.partial(jnp.where, first)
-    kinds = own, pick(other, came), pick(came, other), pick(across_other, across)
-    low, high = [k[:share] for k in kinds], [k[share:] for k in kinds]
-    return [pick(x, y) for x, y in zip(low + high, high + low)]
-
-
-def run_expert(experts, blocks, arrange, kept, weights):
-    width = weights[0].shape[0]
-    flops = 12 * kept * width * weights[0].shape[1]
+def halves(*blocks):
+    first = lax.axis_index("tp") == 0
+    share = blocks[0].shape[0] // 2
+    low, high = [k[:share] for k in blocks], [k[share:] for k in blocks]
+    return [jnp.where(first, x, y) for x, y in zip(low + high, high + low)]
+
+
+def own_and_y(own, came, other):
+    return halves(own, jnp.where(lax.axis_index("tp") == 0, came, other))
+
+
+def z_and_zy(came, other, across, across_other):
+    first = lax.axis_index("tp") == 0
+    mine, theirs = halves(jnp.where(first, other, came))
+    return mine, across, theirs, across_other
+
+
+def run_expert(experts, blocks, arrange, kept, weights, fetch=False, also=None):
+    width, ff = weights[0].shape
+    flops = 12 * kept * width * ff
+    out_shape = [
+        jax.ShapeDtypeStruct((kept, width), jnp.float32),
+        jax.ShapeDtypeStruct((kept if also is None else kept + also.shape[0], width), jnp.bfloat16),
+    ]
+    scratch = []
+    extra = [] if also is None else [also]
+    if fetch:
+        weights = [pltpu.with_memory_space_constraint(w, pltpu.HBM) for w in weights]
+        out_shape += [pltpu.VMEM(w.shape, w.dtype) for w in weights]
+        pieces = 2 * -(-ff // (2 * LANES)) + width // (4 * LANES)
+        scratch = [pltpu.SemaphoreType.DMA((pieces,))]
     return pl.pallas_call(
-        functools.partial(expert_kernel, experts, width, arrange),
-        out_shape=(
-            jax.ShapeDtypeStruct((kept, width), jnp.float32),
-            jax.ShapeDtypeStruct((kept, width), jnp.bfloat16),
-        ),
-        in_specs=[VMEM] * (len(blocks) + 3),
-        out_specs=(VMEM, VMEM),
+        functools.partial(expert_kernel, experts, width, arrange, len(blocks), len(extra), fetch),
+        out_shape=tuple(out_shape),
+        in_specs=[VMEM] * len(blocks + tuple(extra)) + [HBM if fetch else VMEM] * 3,
+        out_specs=(VMEM,) * len(out_shape),
+        scratch_shapes=scratch,
         compiler_params=pltpu.CompilerParams(vmem_limit_bytes=24 * MIB),
         cost_estimate=pl.CostEstimate(flops=flops, bytes_accessed=8 * MIB, transcendentals=0),
         name="expert",
-    )(*blocks, *weights)
-
-
-PIECES = 4
-
-
-def fetch_kernel(*refs):
-    sources, targets, done = refs[:3], refs[4:7], refs[7]
-    copies = []
-    for i, (source, target) in enumerate(zip(sources, targets)):
-        rows = source.shape[0] // PIECES
-        for j in range(PIECES):
-            part = pl.ds(j * rows, rows)
-            copies.append(pltpu.make_async_copy(source.at[part], target.at[part], done.at[i, j]))
-    for copy in copies:
-        copy.start()
-    for copy in copies:
-        copy.wait()
-
-
-def fetch(weights, after):
-    return pl.pallas_call(
-        fetch_kernel,
-        out_shape=tuple(pltpu.VMEM(w.shape, w.dtype) for w in weights),
-        in_specs=[HBM] * 3 + [ANY],
-        out_specs=(VMEM,) * 3,
-        scratch_shapes=[pltpu.SemaphoreType.DMA((3, PIECES))],
-        compiler_params=pltpu.CompilerParams(vmem_limit_bytes=12 * MIB),
-        cost_estimate=pl.CostEstimate(flops=1 << 30, bytes_accessed=8 * MIB, transcendentals=0),
-        name="fetch",
-    )(*(pltpu.with_memory_space_constraint(w, pltpu.HBM) for w in weights), after)
-
-
-def small_call(body, out_shape, *operands):
+    )(*blocks, *extra, *weights)
+
+
+def small_call(body, out_shape, *operands, flops=1 << 26, moved=MIB):
     several = isinstance(out_shape, tuple)
     return pl.pallas_call(
         body,
@@ -192,20 +211,35 @@
         in_specs=[VMEM] * len(operands),
         out_specs=(VMEM,) * len(out_shape) if several else VMEM,
         compiler_params=pltpu.CompilerParams(vmem_limit_bytes=8 * MIB),
-        cost_estimate=pl.CostEstimate(flops=1 << 26, bytes_accessed=MIB, transcendentals=0),
+        cost_estimate=pl.CostEstimate(flops=flops, bytes_accessed=moved, transcendentals=0),
     )(*operands)
 
 
-def join_kernel(kept_ref, came_ref, *out_refs):
-    share = out_refs[0].shape[0]
-    for i, out in enumerate(out_refs):
-        part = pl.ds(i * share, share)
-        out[...] = (kept_ref[part] + came_ref[part].astype(jnp.float32)).astype(out.dtype)
-
-
-def add_kernel(kept_ref, came_ref, out_ref):
-    total = kept_ref[...].astype(jnp.float32) + came_ref[...].astype(jnp.float32)
-    out_ref[...] = total.astype(out_ref.dtype)
+def share_kernel(block_ref, out_ref):
+    share = out_ref.shape[0]
+    out_ref[...] = jnp.where(lax.axis_index("tp") == 0, block_ref[:share], block_ref[share:])
+
+
+def near_kernel(kept_ref, near_kept_ref, came_ref, there_ref, here_ref):
+    rows = there_ref.shape[0]
+    came = came_ref[...].astype(jnp.float32)
+    there_ref[...] = (kept_ref[...] + came[:rows]).astype(jnp.bfloat16)
+    here_ref[...] = near_kept_ref[...] + came[rows:]
+
+
+def join_kernel(inputs, *refs):
+    start = 0
+    for out in refs[inputs:]:
+        part = pl.ds(start, out.shape[0])
+        total = refs[0][part].astype(jnp.float32)
+        for ref in refs[1:inputs]:
+            total += ref[part].astype(jnp.float32)
+        out[...] = total.astype(out.dtype)
+        start += out.shape[0]
+
+
+def join(out_shape, *terms):
+    return small_call(functools.partial(join_kernel, len(terms)), out_shape, *terms)
 
 
 def norm_kernel(count, *refs):
@@ -263,7 +297,7 @@
         out_specs=(VMEM, VMEM),
         scratch_shapes=[pltpu.VMEM(x.shape, x.dtype) for x in sources] + [pltpu.SemaphoreType.DMA((3,))],
         compiler_params=pltpu.CompilerParams(vmem_limit_bytes=8 * MIB),
-        cost_estimate=pl.CostEstimate(flops=1 << 26, bytes_accessed=MIB, transcendentals=0),
+        cost_estimate=pl.CostEstimate(flops=1<<34, bytes_accessed=MIB, transcendentals=0),
         name="rows",
     )(*(pltpu.with_memory_space_constraint(x, pltpu.HBM) for x in sources))
     affine = [norm_gain[None], norm_bias[None]]
@@ -273,15 +307,18 @@
     near = over_ep(full, (1, 2))
     got = {z: over_ep(own, (2 * z, 2 * z)) for z in far}
     near_other = over_tp(near)
-    near_across = over_ep(near, (None, 1))
-    near_across_other = over_tp(near_across, ((1, 0),))
-    weights = fetch((w_gate[0], w_up[0], w_down[0]), near)
-
-    blocks = (full, near, near_other, near_across, near_across_other)
-    kept, sent = run_expert(experts, blocks, near_blocks, 2 * tok_rows, weights)
+    near_own = small_call(share_kernel, shape((share, packed), bf16), near, flops=1<<34, moved=MIB)
+    near_across = over_ep(near_own, (2, 1))
+    near_across_other = over_tp(near_across)
+
+    weights = w_gate[0], w_up[0], w_down[0]
+    kept, sent = run_expert(experts, (full, near, near_other), own_and_y, tok_rows, weights)
+    near_kept = kept
+    blocks = (near, near_other, near_across, near_across_other)
+    kept, sent = run_expert(experts, blocks, z_and_zy, tok_rows, weights, also=sent)
     came = over_tp(sent)
-    kinds = (shape((tok_rows, width), f32), shape((tok_rows, width), bf16))
-    near_here, near_there = small_call(join_kernel, kinds, kept, came)
+    kinds = (shape((tok_rows, width), bf16), shape((tok_rows, width), f32))
+    near_there, near_here = small_call(near_kernel, kinds, kept, near_kept, came)
     here, there = {}, {}
     for z in far:
         across = over_ep(got[z], (1, 1))
@@ -289,21 +326,19 @@
         kept, sent = run_expert(experts, blocks, as_given, 2 * share, weights)
         came = over_tp(sent)
         kinds = (shape((share, width), f32), shape((share, width), bf16))
-        here[z], there[z] = small_call(join_kernel, kinds, kept, came)
-
-    came = over_ep(near_there, (1, 1))
+        here[z], there[z] = join(kinds, kept, came)
+
+    came = over_ep(near_there, (2, 2))
     kinds = (shape((share, width), f32), shape((share, width), bf16))
-    total, go = small_call(join_kernel, kinds, near_here, came)
-    terms = [total, over_ep(go, (2, 2))]
+    total, go = join(kinds, near_here, came)
+    terms = [total, over_ep(go, (1, 1))]
     for z in far:
         came = over_ep(there[z], (1, 1))
-        total = small_call(add_kernel, shape((share, width), bf16), here[z], came)
+        total = join(shape((share, width), bf16), here[z], came)
         terms.append(over_ep(total, (2 * z, 2 * z)))
 
     out = shape((share, half), bf16)
-    stay, go = small_call(
-        functools.partial(norm_kernel, len(terms)), (out, out), *terms, own, *affine, *affine_other
-    )
+    stay, go = small_call(functools.partial(norm_kernel, len(terms)), (out, out), *terms, own, *affine, *affine_other)
     came = over_tp(go)
     first = lax.axis_index("tp") == 0
     return jnp.concatenate([jnp.where(first, stay, came), jnp.where(first, came, stay)], axis=0)

time: 69.8 us -> 60 us (0.86)
  waiting for transfers between devices: 29.9 us -> 26.2 us
  starting transfers between devices: 28 us -> 24.9 us
  Pallas kernels: 10.8 us -> 7.83 us
    ppermute x12, starting transfers between devices: 9.05 us -> 2.3 us  [over_tp(): return lax.ppermute(x, 'tp', pairs)]
    ppermute x12, waiting for transfers between devices: 27.8 us -> 24.1 us  [over_ep(): return lax.ppermute(x, ('ep', 'tp'), pairs)]
    ppermute x12, starting transfers between devices: 19 us -> 22.6 us  [over_ep(): return lax.ppermute(x, ('ep', 'tp'), pairs)]
    pallas_call x4, Pallas kernels: 9.14 us -> 6.18 us  [run_expert(): pl.pallas_call(functools.partial(expert_kernel, experts, width, arrange,...]
  transfers between devices with their start and end apart: 24 -> 24, of which waited for: 9 -> 11; matrix products, arithmetic and copies ran while one was open for 0% -> 0% of each run, Pallas kernels for 14% -> 11%
where the time goes in v4:
time: 60 us; the launch traced here: 59.8 us
  waiting for transfers between devices  26.2 us (44%)
  starting transfers between devices  24.9 us (42%)
  Pallas kernels  7.83 us (13%)
  other arithmetic  0.68 us (1%)
    ppermute x12, waiting for transfers between devices, over_ep(): return lax.ppermute(x, ('ep', 'tp'), pairs)  24.1 us
    ppermute x12, starting transfers between devices, over_ep(): return lax.ppermute(x, ('ep', 'tp'), pairs)  22.6 us
    pallas_call x4, Pallas kernels, run_expert(): pl.pallas_call(functools.partial(expert_kernel, experts, width, arrange,...  6.18 us
    ppermute x12, starting transfers between devices, over_tp(): return lax.ppermute(x, 'tp', pairs)  2.3 us
    ppermute x12, waiting for transfers between devices, over_tp(): return lax.ppermute(x, 'tp', pairs)  2.08 us
  transfers between devices with their start and end apart: 24, of which 11 were waited for; matrix products, arithmetic and copies ran while one was open for 0% of the time, Pallas kernels for 11%

profile of v4, /device:TPU:0, one launch (start us, length us, event | category | flops | bytes accessed | tf_op | source)
XLA Modules:
  0.0 59.8 jit_solution(9292749974141506926)
XLA Ops:
  0.0 1.0 %rows.1 = (bf16[64,2176]{1,0:T(8,128)(2,1)S(1)}, bf16[32,2176]{1,0:T(8,128)(2,1)S(1)}) custom-call(bf16[64,2048]{1,0:T(8,128)(2,1)} %tokens_hbm.1, s32[4,64]{1,0:T(4,128)} %bitcast.23, f32[4,64]{1,0:T(4,128)} %bitcast.24), custom_call_target="tpu_custom_call" | custom-call | flops 17179869184 | bytes 1048576 | tf_op jit(solution)/shard_map/rows/pallas_call | solution.py:293
  1.1 3.1 %collective-permute-start = (bf16[64,2176]{1,0:T(8,128)(2,1)S(1)}, bf16[64,2176]{1,0:T(8,128)(2,1)S(1)}, u32[]{:S(2)}, u32[]{:S(2)}) collective-permute-start(bf16[64,2176]{1,0:T(8,128)(2,1)S(1)} %get-tuple-element.25.refs_0_), channel_id=1, source_target_pairs={{0,2},{1,5},{2,0},{3,7},{4,6},{5,1},{6,4},{7,3},{8,10},{9,13},{10,... | collective-permute-start | bytes 835592 | tf_op jit(solution)/shard_map/ppermute | solution.py:286
  4.1 4.5 %collective-permute-done.block_ref.refs_1_.refs_0_ = bf16[64,2176]{1,0:T(8,128)(2,1)S(1)} collective-permute-done((bf16[64,2176]{1,0:T(8,128)(2,1)S(1)}, bf16[64,2176]{1,0:T(8,128)(2,1)S(1)}, u32[]{:S(2)}, u32[]{:S(2)}) %collective-permute-start) | collective-permute-done | bytes 278560 | tf_op jit(solution)/shard_map/ppermute | solution.py:286
  8.7 2.1 %collective-permute-start.2 = (bf16[32,2176]{1,0:T(8,128)(2,1)S(1)}, bf16[32,2176]{1,0:T(8,128)(2,1)S(1)}, u32[]{:S(2)}, u32[]{:S(2)}) collective-permute-start(bf16[32,2176]{1,0:T(8,128)(2,1)S(1)} %shard_map.82), channel_id=1, source_target_pairs={{0,4},{1,3},{2,6},{3,1},{4,0},{5,7},{6,2},{7,5},{8,12},{9,11},{10,... | collective-permute-start | bytes 417800 | tf_op jit(solution)/shard_map/ppermute | solution.py:286
  10.8 2.5 %collective-permute-start.7 = (bf16[32,2176]{1,0:T(8,128)(2,1)S(1)}, bf16[32,2176]{1,0:T(8,128)(2,1)S(1)}, u32[]{:S(2)}, u32[]{:S(2)}) collective-permute-start(bf16[32,2176]{1,0:T(8,128)(2,1)S(1)} %get-tuple-element.34.refs_4_), channel_id=1, source_target_pairs={{0,12},{1,13},{2,14},{3,15},{4,8},{5,9},{6,10},{7,11},{8,4},{9,5},... | collective-permute-start | bytes 417800 | tf_op jit(solution)/shard_map/ppermute | solution.py:286
  14.3 3.5 %collective-permute-start.14 = (bf16[32,2176]{1,0:T(8,128)(2,1)S(1)}, bf16[32,2176]{1,0:T(8,128)(2,1)S(1)}, u32[]{:S(2)}, u32[]{:S(2)}) collective-permute-start(bf16[32,2176]{1,0:T(8,128)(2,1)S(1)} %get-tuple-element.34.refs_4_), channel_id=1, source_target_pairs={{0,8},{1,9},{2,10},{3,11},{4,12},{5,13},{6,14},{7,15},{8,0},{9,1},... | collective-permute-start | bytes 417800 | tf_op jit(solution)/shard_map/ppermute | solution.py:286
  17.8 1.7 %collective-permute-done.7.refs_0_ = bf16[32,2176]{1,0:T(8,128)(2,1)S(1)} collective-permute-done((bf16[32,2176]{1,0:T(8,128)(2,1)S(1)}, bf16[32,2176]{1,0:T(8,128)(2,1)S(1)}, u32[]{:S(2)}, u32[]{:S(2)}) %collective-permute-start.7) | collective-permute-done | bytes 139296 | tf_op jit(solution)/shard_map/ppermute | solution.py:286
  19.5 1.0 %collective-permute-start.8 = (bf16[32,2176]{1,0:T(8,128)(2,1)S(1)}, bf16[32,2176]{1,0:T(8,128)(2,1)S(1)}, u32[]{:S(2)}, u32[]{:S(2)}) collective-permute-start(bf16[32,2176]{1,0:T(8,128)(2,1)S(1)} %collective-permute-done.7.refs_0_), channel_id=1, source_target_pairs={{0,2},{1,3},{2,0},{3,1},{4,6},{5,7},{6,4},{7,5},{8,10},{9,11},{10,... | collective-permute-start | bytes 417800 | tf_op jit(solution)/shard_map/ppermute | solution.py:286
  20.5 1.5 %expert.4 = (f32[64,2048]{1,0:T(8,128)S(1)}, bf16[64,2048]{1,0:T(8,128)(2,1)S(1)}) custom-call(bf16[64,2176]{1,0:T(8,128)(2,1)S(1)} %get-tuple-element.25.refs_0_, bf16[64,2176]{1,0:T(8,128)(2,1)S(1)} %collective-permute-done.block_ref.refs_1_.refs_0_, bf16[64,2176]{1,0:T(8,128)(2,1)S(1)} %collective-permute-done.1.refs_2_.refs_1_, ...), custom_call_target="tpu_custom_call" | custom-call | flops 1006632960 | bytes 8388608 | tf_op jit(solution)/shard_map/expert/pallas_call | solution.py:194
  22.0 1.5 %expert.5 = (f32[64,2048]{1,0:T(8,128)S(1)}, bf16[128,2048]{1,0:T(8,128)(2,1)S(1)}) custom-call(bf16[64,2176]{1,0:T(8,128)(2,1)S(1)} %collective-permute-done.block_ref.refs_1_.refs_0_, bf16[64,2176]{1,0:T(8,128)(2,1)S(1)} %collective-permute-done.1.refs_2_.refs_1_, bf16[32,2176]{1,0:T(8,128)(2,1)S(1)} %collective-permute-done.2.refs_2_, ...), custom_call_target="tpu_custom_call" | custom-call | flops 1006632960 | bytes 8388608 | tf_op jit(solution)/shard_map/expert/pallas_call | solution.py:194
  23.6 2.9 %collective-permute-done.14.refs_0_ = bf16[32,2176]{1,0:T(8,128)(2,1)S(1)} collective-permute-done((bf16[32,2176]{1,0:T(8,128)(2,1)S(1)}, bf16[32,2176]{1,0:T(8,128)(2,1)S(1)}, u32[]{:S(2)}, u32[]{:S(2)}) %collective-permute-start.14) | collective-permute-done | bytes 139296 | tf_op jit(solution)/shard_map/ppermute | solution.py:286
  27.6 4.3 %collective-permute-done.15.refs_1_ = bf16[32,2176]{1,0:T(8,128)(2,1)S(1)} collective-permute-done((bf16[32,2176]{1,0:T(8,128)(2,1)S(1)}, bf16[32,2176]{1,0:T(8,128)(2,1)S(1)}, u32[]{:S(2)}, u32[]{:S(2)}) %collective-permute-start.15) | collective-permute-done | bytes 139296 | tf_op jit(solution)/shard_map/ppermute | solution.py:286
  31.9 1.5 %expert.6 = (f32[64,2048]{1,0:T(8,128)S(1)}, bf16[64,2048]{1,0:T(8,128)(2,1)S(1)}) custom-call(bf16[32,2176]{1,0:T(8,128)(2,1)S(1)} %collective-permute-done.7.refs_0_, bf16[32,2176]{1,0:T(8,128)(2,1)S(1)} %collective-permute-done.8.refs_1_, bf16[32,2176]{1,0:T(8,128)(2,1)S(1)} %collective-permute-done.9.refs_2_, ...), custom_call_target="tpu_custom_call" | custom-call | flops 1006632960 | bytes 8388608 | tf_op jit(solution)/shard_map/expert/pallas_call | solution.py:194
  34.0 1.6 %expert.7 = (f32[64,2048]{1,0:T(8,128)S(1)}, bf16[64,2048]{1,0:T(8,128)(2,1)S(1)}) custom-call(bf16[32,2176]{1,0:T(8,128)(2,1)S(1)} %collective-permute-done.14.refs_0_, bf16[32,2176]{1,0:T(8,128)(2,1)S(1)} %collective-permute-done.15.refs_1_, bf16[32,2176]{1,0:T(8,128)(2,1)S(1)} %collective-permute-done.16.refs_2_, ...), custom_call_target="tpu_custom_call" | custom-call | flops 1006632960 | bytes 8388608 | tf_op jit(solution)/shard_map/expert/pallas_call | solution.py:194
  35.8 2.3 %collective-permute-start.5 = (bf16[64,2048]{1,0:T(8,128)(2,1)S(1)}, bf16[64,2048]{1,0:T(8,128)(2,1)S(1)}, u32[]{:S(2)}, u32[]{:S(2)}) collective-permute-start(bf16[64,2048]{1,0:T(8,128)(2,1)S(1)} %get-tuple-element.31), channel_id=1, source_target_pairs={{0,4},{1,5},{2,6},{3,7},{4,0},{5,1},{6,2},{7,3},{8,12},{9,13},{10,... | collective-permute-start | bytes 786440 | tf_op jit(solution)/shard_map/ppermute | solution.py:286
  38.2 1.7 %collective-permute-start.12 = (bf16[32,2048]{1,0:T(8,128)(2,1)S(1)}, bf16[32,2048]{1,0:T(8,128)(2,1)S(1)}, u32[]{:S(2)}, u32[]{:S(2)}) collective-permute-start(bf16[32,2048]{1,0:T(8,128)(2,1)S(1)} %get-tuple-element.38), channel_id=1, source_target_pairs={{0,2},{1,3},{2,0},{3,1},{4,6},{5,7},{6,4},{7,5},{8,10},{9,11},{10,... | collective-permute-start | bytes 393224 | tf_op jit(solution)/shard_map/ppermute | solution.py:286
  40.4 4.2 %collective-permute-done.12.refs_1_ = bf16[32,2048]{1,0:T(8,128)(2,1)S(1)} collective-permute-done((bf16[32,2048]{1,0:T(8,128)(2,1)S(1)}, bf16[32,2048]{1,0:T(8,128)(2,1)S(1)}, u32[]{:S(2)}, u32[]{:S(2)}) %collective-permute-start.12) | collective-permute-done | bytes 131104 | tf_op jit(solution)/shard_map/ppermute | solution.py:286
  44.7 2.9 %collective-permute-start.13 = (bf16[32,2048]{1,0:T(8,128)(2,1)S(1)}, bf16[32,2048]{1,0:T(8,128)(2,1)S(1)}, u32[]{:S(2)}, u32[]{:S(2)}) collective-permute-start(bf16[32,2048]{1,0:T(8,128)(2,1)S(1)} %shard_map.86), channel_id=1, source_target_pairs={{0,12},{1,13},{2,14},{3,15},{4,8},{5,9},{6,10},{7,11},{8,4},{9,5},... | collective-permute-start | bytes 393224 | tf_op jit(solution)/shard_map/ppermute | solution.py:286
  47.6 0.9 %collective-permute-start.20 = (bf16[32,2048]{1,0:T(8,128)(2,1)S(1)}, bf16[32,2048]{1,0:T(8,128)(2,1)S(1)}, u32[]{:S(2)}, u32[]{:S(2)}) collective-permute-start(bf16[32,2048]{1,0:T(8,128)(2,1)S(1)} %shard_map.88), channel_id=1, source_target_pairs={{0,8},{1,9},{2,10},{3,11},{4,12},{5,13},{6,14},{7,15},{8,0},{9,1},... | collective-permute-start | bytes 393224 | tf_op jit(solution)/shard_map/ppermute | solution.py:286
  48.5 1.8 %collective-permute-start.6 = (bf16[32,2048]{1,0:T(8,128)(2,1)S(1)}, bf16[32,2048]{1,0:T(8,128)(2,1)S(1)}, u32[]{:S(2)}, u32[]{:S(2)}) collective-permute-start(bf16[32,2048]{1,0:T(8,128)(2,1)S(1)} %get-tuple-element.33), channel_id=1, source_target_pairs={{0,2},{1,3},{2,0},{3,1},{4,6},{5,7},{6,4},{7,5},{8,10},{9,11},{10,... | collective-permute-start | bytes 393224 | tf_op jit(solution)/shard_map/ppermute | solution.py:286
  51.6 1.1 %collective-permute-done.13.refs_2_ = bf16[32,2048]{1,0:T(8,128)(2,1)S(1)} collective-permute-done((bf16[32,2048]{1,0:T(8,128)(2,1)S(1)}, bf16[32,2048]{1,0:T(8,128)(2,1)S(1)}, u32[]{:S(2)}, u32[]{:S(2)}) %collective-permute-start.13) | collective-permute-done | bytes 131104 | tf_op jit(solution)/shard_map/ppermute | solution.py:286
  52.7 4.8 %collective-permute-done.20.refs_3_ = bf16[32,2048]{1,0:T(8,128)(2,1)S(1)} collective-permute-done((bf16[32,2048]{1,0:T(8,128)(2,1)S(1)}, bf16[32,2048]{1,0:T(8,128)(2,1)S(1)}, u32[]{:S(2)}, u32[]{:S(2)}) %collective-permute-start.20) | collective-permute-done | bytes 131104 | tf_op jit(solution)/shard_map/ppermute | solution.py:286
  57.9 1.2 %collective-permute-done.23 = bf16[32,1024]{1,0:T(8,128)(2,1)S(1)} collective-permute-done((bf16[32,1024]{1,0:T(8,128)(2,1)S(1)}, bf16[32,1024]{1,0:T(8,128)(2,1)S(1)}, u32[]{:S(2)}, u32[]{:S(2)}) %collective-permute-start.23) | collective-permute-done | bytes 65568 | tf_op jit(solution)/shard_map/ppermute | solution.py:289
  59.2 0.7 %pad_maximum_fusion = bf16[64,1024]{1,0:T(8,128)(2,1)} fusion(bf16[32,1024]{1,0:T(8,128)(2,1)S(1)} %get-tuple-element.46, bf16[32,1024]{1,0:T(8,128)(2,1)S(1)} %get-tuple-element.45), kind=kLoop, calls=%fused_computation | loop fusion | flops 262144 | bytes 262144 | tf_op jit(solution)/shard_map/concatenate | solution.py:344
  (49 shorter events, 5.3 us)
Async XLA Ops:
  1.1 7.6 %collective-permute-start = (bf16[64,2176]{1,0:T(8,128)(2,1)S(1)}, bf16[64,2176]{1,0:T(8,128)(2,1)S(1)}, u32[]{:S(2)}, u32[]{:S(2)}) collective-permute-start(bf16[64,2176]{1,0:T(8,128)(2,1)S(1)} %get-tuple-element.25.refs_0_), channel_id=1, source_target_pairs={{0,2},{1,5},{2,0},{3,7},{4,6},{5,1},{6,4},{7,3},{8,10},{9,13},{10,... | collective-permute-start | bytes 835592 | tf_op jit(solution)/shard_map/ppermute | solution.py:286
  8.7 11.8 %collective-permute-start.1 = (bf16[64,2176]{1,0:T(8,128)(2,1)S(1)}, bf16[64,2176]{1,0:T(8,128)(2,1)S(1)}, u32[]{:S(2)}, u32[]{:S(2)}) collective-permute-start(bf16[64,2176]{1,0:T(8,128)(2,1)S(1)} %collective-permute-done.block_ref.refs_1_.refs_0_), channel_id=1, source_target_pairs={{0,1},{1,0},{2,3},{3,2},{4,5},{5,4},{6,7},{7,6},{8,9},{9,8},{10,11... | collective-permute-start | bytes 835592 | tf_op jit(solution)/shard_map/ppermute | solution.py:289
  8.7 5.2 %collective-permute-start.2 = (bf16[32,2176]{1,0:T(8,128)(2,1)S(1)}, bf16[32,2176]{1,0:T(8,128)(2,1)S(1)}, u32[]{:S(2)}, u32[]{:S(2)}) collective-permute-start(bf16[32,2176]{1,0:T(8,128)(2,1)S(1)} %shard_map.82), channel_id=1, source_target_pairs={{0,4},{1,3},{2,6},{3,1},{4,0},{5,7},{6,2},{7,5},{8,12},{9,11},{10,... | collective-permute-start | bytes 417800 | tf_op jit(solution)/shard_map/ppermute | solution.py:286
  10.8 8.6 %collective-permute-start.7 = (bf16[32,2176]{1,0:T(8,128)(2,1)S(1)}, bf16[32,2176]{1,0:T(8,128)(2,1)S(1)}, u32[]{:S(2)}, u32[]{:S(2)}) collective-permute-start(bf16[32,2176]{1,0:T(8,128)(2,1)S(1)} %get-tuple-element.34.refs_4_), channel_id=1, source_target_pairs={{0,12},{1,13},{2,14},{3,15},{4,8},{5,9},{6,10},{7,11},{8,4},{9,5},... | collective-permute-start | bytes 417800 | tf_op jit(solution)/shard_map/ppermute | solution.py:286
  13.9 8.1 %collective-permute-start.3 = (bf16[32,2176]{1,0:T(8,128)(2,1)S(1)}, bf16[32,2176]{1,0:T(8,128)(2,1)S(1)}, u32[]{:S(2)}, u32[]{:S(2)}) collective-permute-start(bf16[32,2176]{1,0:T(8,128)(2,1)S(1)} %collective-permute-done.2.refs_2_), channel_id=1, source_target_pairs={{0,1},{1,0},{2,3},{3,2},{4,5},{5,4},{6,7},{7,6},{8,9},{9,8},{10,11... | collective-permute-start | bytes 417800 | tf_op jit(solution)/shard_map/ppermute | solution.py:289
  14.3 12.2 %collective-permute-start.14 = (bf16[32,2176]{1,0:T(8,128)(2,1)S(1)}, bf16[32,2176]{1,0:T(8,128)(2,1)S(1)}, u32[]{:S(2)}, u32[]{:S(2)}) collective-permute-start(bf16[32,2176]{1,0:T(8,128)(2,1)S(1)} %get-tuple-element.34.refs_4_), channel_id=1, source_target_pairs={{0,8},{1,9},{2,10},{3,11},{4,12},{5,13},{6,14},{7,15},{8,0},{9,1},... | collective-permute-start | bytes 417800 | tf_op jit(solution)/shard_map/ppermute | solution.py:286
  19.5 7.6 %collective-permute-start.8 = (bf16[32,2176]{1,0:T(8,128)(2,1)S(1)}, bf16[32,2176]{1,0:T(8,128)(2,1)S(1)}, u32[]{:S(2)}, u32[]{:S(2)}) collective-permute-start(bf16[32,2176]{1,0:T(8,128)(2,1)S(1)} %collective-permute-done.7.refs_0_), channel_id=1, source_target_pairs={{0,2},{1,3},{2,0},{3,1},{4,6},{5,7},{6,4},{7,5},{8,10},{9,11},{10,... | collective-permute-start | bytes 417800 | tf_op jit(solution)/shard_map/ppermute | solution.py:286
  23.6 12.2 %collective-permute-start.4 = (bf16[128,2048]{1,0:T(8,128)(2,1)S(1)}, bf16[128,2048]{1,0:T(8,128)(2,1)S(1)}, u32[]{:S(2)}, u32[]{:S(2)}) collective-permute-start(bf16[128,2048]{1,0:T(8,128)(2,1)S(1)} %get-tuple-element.29), channel_id=1, source_target_pairs={{0,1},{1,0},{2,3},{3,2},{4,5},{5,4},{6,7},{7,6},{8,9},{9,8},{10,11... | collective-permute-start | bytes 1572872 | tf_op jit(solution)/shard_map/ppermute | solution.py:289
  26.6 5.3 %collective-permute-start.15 = (bf16[32,2176]{1,0:T(8,128)(2,1)S(1)}, bf16[32,2176]{1,0:T(8,128)(2,1)S(1)}, u32[]{:S(2)}, u32[]{:S(2)}) collective-permute-start(bf16[32,2176]{1,0:T(8,128)(2,1)S(1)} %collective-permute-done.14.refs_0_), channel_id=1, source_target_pairs={{0,2},{1,3},{2,0},{3,1},{4,6},{5,7},{6,4},{7,5},{8,10},{9,11},{10,... | collective-permute-start | bytes 417800 | tf_op jit(solution)/shard_map/ppermute | solution.py:286
  27.1 4.8 %collective-permute-start.9 = (bf16[32,2176]{1,0:T(8,128)(2,1)S(1)}, bf16[32,2176]{1,0:T(8,128)(2,1)S(1)}, u32[]{:S(2)}, u32[]{:S(2)}) collective-permute-start(bf16[32,2176]{1,0:T(8,128)(2,1)S(1)} %collective-permute-done.7.refs_0_), channel_id=1, source_target_pairs={{0,1},{1,0},{2,3},{3,2},{4,5},{5,4},{6,7},{7,6},{8,9},{9,8},{10,11... | collective-permute-start | bytes 417800 | tf_op jit(solution)/shard_map/ppermute | solution.py:289
  27.1 4.8 %collective-permute-start.10 = (bf16[32,2176]{1,0:T(8,128)(2,1)S(1)}, bf16[32,2176]{1,0:T(8,128)(2,1)S(1)}, u32[]{:S(2)}, u32[]{:S(2)}) collective-permute-start(bf16[32,2176]{1,0:T(8,128)(2,1)S(1)} %collective-permute-done.8.refs_1_), channel_id=1, source_target_pairs={{0,1},{1,0},{2,3},{3,2},{4,5},{5,4},{6,7},{7,6},{8,9},{9,8},{10,11... | collective-permute-start | bytes 417800 | tf_op jit(solution)/shard_map/ppermute | solution.py:289
  27.6 6.5 %collective-permute-start.16 = (bf16[32,2176]{1,0:T(8,128)(2,1)S(1)}, bf16[32,2176]{1,0:T(8,128)(2,1)S(1)}, u32[]{:S(2)}, u32[]{:S(2)}) collective-permute-start(bf16[32,2176]{1,0:T(8,128)(2,1)S(1)} %collective-permute-done.14.refs_0_), channel_id=1, source_target_pairs={{0,1},{1,0},{2,3},{3,2},{4,5},{5,4},{6,7},{7,6},{8,9},{9,8},{10,11... | collective-permute-start | bytes 417800 | tf_op jit(solution)/shard_map/ppermute | solution.py:289
  31.9 2.1 %collective-permute-start.17 = (bf16[32,2176]{1,0:T(8,128)(2,1)S(1)}, bf16[32,2176]{1,0:T(8,128)(2,1)S(1)}, u32[]{:S(2)}, u32[]{:S(2)}) collective-permute-start(bf16[32,2176]{1,0:T(8,128)(2,1)S(1)} %collective-permute-done.15.refs_1_), channel_id=1, source_target_pairs={{0,1},{1,0},{2,3},{3,2},{4,5},{5,4},{6,7},{7,6},{8,9},{9,8},{10,11... | collective-permute-start | bytes 417800 | tf_op jit(solution)/shard_map/ppermute | solution.py:289
  33.4 4.7 %collective-permute-start.11 = (bf16[64,2048]{1,0:T(8,128)(2,1)S(1)}, bf16[64,2048]{1,0:T(8,128)(2,1)S(1)}, u32[]{:S(2)}, u32[]{:S(2)}) collective-permute-start(bf16[64,2048]{1,0:T(8,128)(2,1)S(1)} %get-tuple-element.36), channel_id=1, source_target_pairs={{0,1},{1,0},{2,3},{3,2},{4,5},{5,4},{6,7},{7,6},{8,9},{9,8},{10,11... | collective-permute-start | bytes 786440 | tf_op jit(solution)/shard_map/ppermute | solution.py:289
  35.6 4.3 %collective-permute-start.18 = (bf16[64,2048]{1,0:T(8,128)(2,1)S(1)}, bf16[64,2048]{1,0:T(8,128)(2,1)S(1)}, u32[]{:S(2)}, u32[]{:S(2)}) collective-permute-start(bf16[64,2048]{1,0:T(8,128)(2,1)S(1)} %get-tuple-element.40), channel_id=1, source_target_pairs={{0,1},{1,0},{2,3},{3,2},{4,5},{5,4},{6,7},{7,6},{8,9},{9,8},{10,11... | collective-permute-start | bytes 786440 | tf_op jit(solution)/shard_map/ppermute | solution.py:289
  35.8 12.6 %collective-permute-start.5 = (bf16[64,2048]{1,0:T(8,128)(2,1)S(1)}, bf16[64,2048]{1,0:T(8,128)(2,1)S(1)}, u32[]{:S(2)}, u32[]{:S(2)}) collective-permute-start(bf16[64,2048]{1,0:T(8,128)(2,1)S(1)} %get-tuple-element.31), channel_id=1, source_target_pairs={{0,4},{1,5},{2,6},{3,7},{4,0},{5,1},{6,2},{7,3},{8,12},{9,13},{10,... | collective-permute-start | bytes 786440 | tf_op jit(solution)/shard_map/ppermute | solution.py:286
  38.2 6.4 %collective-permute-start.12 = (bf16[32,2048]{1,0:T(8,128)(2,1)S(1)}, bf16[32,2048]{1,0:T(8,128)(2,1)S(1)}, u32[]{:S(2)}, u32[]{:S(2)}) collective-permute-start(bf16[32,2048]{1,0:T(8,128)(2,1)S(1)} %get-tuple-element.38), channel_id=1, source_target_pairs={{0,2},{1,3},{2,0},{3,1},{4,6},{5,7},{6,4},{7,5},{8,10},{9,11},{10,... | collective-permute-start | bytes 393224 | tf_op jit(solution)/shard_map/ppermute | solution.py:286
  40.0 7.6 %collective-permute-start.19 = (bf16[32,2048]{1,0:T(8,128)(2,1)S(1)}, bf16[32,2048]{1,0:T(8,128)(2,1)S(1)}, u32[]{:S(2)}, u32[]{:S(2)}) collective-permute-start(bf16[32,2048]{1,0:T(8,128)(2,1)S(1)} %get-tuple-element.42), channel_id=1, source_target_pairs={{0,2},{1,3},{2,0},{3,1},{4,6},{5,7},{6,4},{7,5},{8,10},{9,11},{10,... | collective-permute-start | bytes 393224 | tf_op jit(solution)/shard_map/ppermute | solution.py:286
  44.7 8.0 %collective-permute-start.13 = (bf16[32,2048]{1,0:T(8,128)(2,1)S(1)}, bf16[32,2048]{1,0:T(8,128)(2,1)S(1)}, u32[]{:S(2)}, u32[]{:S(2)}) collective-permute-start(bf16[32,2048]{1,0:T(8,128)(2,1)S(1)} %shard_map.86), channel_id=1, source_target_pairs={{0,12},{1,13},{2,14},{3,15},{4,8},{5,9},{6,10},{7,11},{8,4},{9,5},... | collective-permute-start | bytes 393224 | tf_op jit(solution)/shard_map/ppermute | solution.py:286
  47.6 9.9 %collective-permute-start.20 = (bf16[32,2048]{1,0:T(8,128)(2,1)S(1)}, bf16[32,2048]{1,0:T(8,128)(2,1)S(1)}, u32[]{:S(2)}, u32[]{:S(2)}) collective-permute-start(bf16[32,2048]{1,0:T(8,128)(2,1)S(1)} %shard_map.88), channel_id=1, source_target_pairs={{0,8},{1,9},{2,10},{3,11},{4,12},{5,13},{6,14},{7,15},{8,0},{9,1},... | collective-permute-start | bytes 393224 | tf_op jit(solution)/shard_map/ppermute | solution.py:286
  48.5 9.0 %collective-permute-start.6 = (bf16[32,2048]{1,0:T(8,128)(2,1)S(1)}, bf16[32,2048]{1,0:T(8,128)(2,1)S(1)}, u32[]{:S(2)}, u32[]{:S(2)}) collective-permute-start(bf16[32,2048]{1,0:T(8,128)(2,1)S(1)} %get-tuple-element.33), channel_id=1, source_target_pairs={{0,2},{1,3},{2,0},{3,1},{4,6},{5,7},{6,4},{7,5},{8,10},{9,11},{10,... | collective-permute-start | bytes 393224 | tf_op jit(solution)/shard_map/ppermute | solution.py:286
  50.3 1.2 %collective-permute-start.21 = (f32[1,1024]{1,0:T(1,128)S(1)}, f32[1,1024]{1,0:T(1,128)S(1)}, u32[]{:S(2)}, u32[]{:S(2)}) collective-permute-start(f32[1,1024]{1,0:T(1,128)S(1)} %bitcast.19), channel_id=1, source_target_pairs={{0,1},{1,0},{2,3},{3,2},{4,5},{5,4},{6,7},{7,6},{8,9},{9,8},{10,11... | collective-permute-start | bytes 12296 | tf_op jit(solution)/shard_map/ppermute | solution.py:289
  50.3 1.3 %collective-permute-start.22 = (f32[1,1024]{1,0:T(1,128)S(1)}, f32[1,1024]{1,0:T(1,128)S(1)}, u32[]{:S(2)}, u32[]{:S(2)}) collective-permute-start(f32[1,1024]{1,0:T(1,128)S(1)} %bitcast.21), channel_id=1, source_target_pairs={{0,1},{1,0},{2,3},{3,2},{4,5},{5,4},{6,7},{7,6},{8,9},{9,8},{10,11... | collective-permute-start | bytes 12296 | tf_op jit(solution)/shard_map/ppermute | solution.py:289
  57.8 1.3 %collective-permute-start.23 = (bf16[32,1024]{1,0:T(8,128)(2,1)S(1)}, bf16[32,1024]{1,0:T(8,128)(2,1)S(1)}, u32[]{:S(2)}, u32[]{:S(2)}) collective-permute-start(bf16[32,1024]{1,0:T(8,128)(2,1)S(1)} %get-tuple-element.44), channel_id=1, source_target_pairs={{0,1},{1,0},{2,3},{3,2},{4,5},{5,4},{6,7},{7,6},{8,9},{9,8},{10,11... | collective-permute-start | bytes 196616 | tf_op jit(solution)/shard_map/ppermute | solution.py:289
  (5 other events, 87.5 us)

commit v5 on v4

--- a/solution.py
+++ b/solution.py
@@ -95,36 +95,10 @@
     all_ref[:, :width] = tokens_ref[...]
 
 
-def expert_kernel(experts, width, arrange, blocks, extra, fetch, *refs):
-    row_refs, extra_refs = refs[:blocks], refs[blocks : blocks + extra]
-    blocks += extra
-    sources = refs[blocks : blocks + 3]
-    mine_ref, theirs_ref = refs[blocks + 3 : blocks + 5]
-    wg_ref, wu_ref, wd_ref = refs[blocks + 5 : blocks + 8] if fetch else sources
-    ff = wg_ref.shape[1]
-    step, wide = 2 * LANES, 4 * LANES
-    units = [(start, min(step, ff - start)) for start in range(0, ff, step)]
-    copies = {}
-    if fetch:
-        done = refs[blocks + 8]
-
-        def bring(which, start, size):
-            part = pl.ds(start, size)
-            source, target = sources[which].at[:, part], refs[blocks + 5 + which].at[:, part]
-            copies[which, start] = pltpu.make_async_copy(source, target, done.at[len(copies)])
-
-        for start, size in units:
-            bring(0, start, size)
-            bring(1, start, size)
-        for start in range(0, width, wide):
-            bring(2, start, wide)
-        for copy in copies.values():
-            copy.start()
-
-    def ready(which, start):
-        if fetch:
-            copies[which, start].wait()
-
+def expert_kernel(experts, width, arrange, blocks, *refs):
+    row_refs, (wg_ref, wu_ref, wd_ref) = refs[:blocks], refs[blocks : blocks + 3]
+    *extra_refs, mine_ref, theirs_ref = refs[blocks + 3 :]
+    wide = 4 * LANES
     kept = mine_ref.shape[0]
     packed = jnp.concatenate(arrange(*(r[...] for r in row_refs)), axis=0)
     rows, codes = packed[:, :width], packed[:, width:].astype(jnp.float32)
@@ -133,22 +107,9 @@
     named = (lane == expert) | (lane == expert + experts)
     weight = jnp.sum(jnp.where(named, codes, 0.0), axis=1, keepdims=True)
     dot = functools.partial(jnp.dot, preferred_element_type=jnp.float32)
-    hidden = []
-    for start, size in units:
-        ready(0, start)
-        if size == step:
-            gate = dot(rows, wg_ref[:, start : start + size])
-            ready(1, start)
-            upper = dot(rows, wu_ref[:, start : start + size])
-        else:
-            ready(1, start)
-            both = jnp.concatenate([wg_ref[:, start:], wu_ref[:, start:]], axis=1)
-            both = dot(rows, both)
-            gate, upper = both[:, :size], both[:, size:]
-        hidden.append((jax.nn.silu(gate) * upper).astype(jnp.bfloat16))
-    hidden = jnp.concatenate(hidden, axis=1)
+    gate, upper = dot(rows, wg_ref[...]), dot(rows, wu_ref[...])
+    hidden = (jax.nn.silu(gate) * upper).astype(jnp.bfloat16)
     for start in range(0, width, wide):
-        ready(2, start)
         out = dot(hidden, wd_ref[:, start : start + wide]) * weight
         mine_ref[:, start : start + wide] = out[:kept]
         theirs_ref[:kept, start : start + wide] = out[kept:].astype(jnp.bfloat16)
@@ -177,30 +138,23 @@
     return mine, across, theirs, across_other
 
 
-def run_expert(experts, blocks, arrange, kept, weights, fetch=False, also=None):
+def run_expert(experts, blocks, arrange, kept, weights, *extra):
     width, ff = weights[0].shape
-    flops = 12 * kept * width * ff
-    out_shape = [
-        jax.ShapeDtypeStruct((kept, width), jnp.float32),
-        jax.ShapeDtypeStruct((kept if also is None else kept + also.shape[0], width), jnp.bfloat16),
-    ]
-    scratch = []
-    extra = [] if also is None else [also]
-    if fetch:
-        weights = [pltpu.with_memory_space_constraint(w, pltpu.HBM) for w in weights]
-        out_shape += [pltpu.VMEM(w.shape, w.dtype) for w in weights]
-        pieces = 2 * -(-ff // (2 * LANES)) + width // (4 * LANES)
-        scratch = [pltpu.SemaphoreType.DMA((pieces,))]
+    sent = kept + sum(x.shape[0] for x in extra)
     return pl.pallas_call(
-        functools.partial(expert_kernel, experts, width, arrange, len(blocks), len(extra), fetch),
-        out_shape=tuple(out_shape),
-        in_specs=[VMEM] * len(blocks + tuple(extra)) + [HBM if fetch else VMEM] * 3,
-        out_specs=(VMEM,) * len(out_shape),
-        scratch_shapes=scratch,
+        functools.partial(expert_kernel, experts, width, arrange, len(blocks)),
+        out_shape=(
+            jax.ShapeDtypeStruct((kept, width), jnp.float32),
+            jax.ShapeDtypeStruct((sent, width), jnp.bfloat16),
+        ),
+        in_specs=[VMEM] * (len(blocks) + 3 + len(extra)),
+        out_specs=(VMEM, VMEM),
         compiler_params=pltpu.CompilerParams(vmem_limit_bytes=24 * MIB),
-        cost_estimate=pl.CostEstimate(flops=flops, bytes_accessed=8 * MIB, transcendentals=0),
+        cost_estimate=pl.CostEstimate(
+            flops=12 * kept * width * ff, bytes_accessed=8 * MIB, transcendentals=0
+        ),
         name="expert",
-    )(*blocks, *extra, *weights)
+    )(*blocks, *weights, *extra)
 
 
 def small_call(body, out_shape, *operands, flops=1 << 26, moved=MIB):
@@ -213,11 +167,6 @@
         compiler_params=pltpu.CompilerParams(vmem_limit_bytes=8 * MIB),
         cost_estimate=pl.CostEstimate(flops=flops, bytes_accessed=moved, transcendentals=0),
     )(*operands)
-
-
-def share_kernel(block_ref, out_ref):
-    share = out_ref.shape[0]
-    out_ref[...] = jnp.where(lax.axis_index("tp") == 0, block_ref[:share], block_ref[share:])
 
 
 def near_kernel(kept_ref, near_kept_ref, came_ref, there_ref, here_ref):
@@ -307,15 +256,14 @@
     near = over_ep(full, (1, 2))
     got = {z: over_ep(own, (2 * z, 2 * z)) for z in far}
     near_other = over_tp(near)
-    near_own = small_call(share_kernel, shape((share, packed), bf16), near, flops=1<<34, moved=MIB)
-    near_across = over_ep(near_own, (2, 1))
+    near_across = over_ep(own, (3, 3))
     near_across_other = over_tp(near_across)
 
     weights = w_gate[0], w_up[0], w_down[0]
     kept, sent = run_expert(experts, (full, near, near_other), own_and_y, tok_rows, weights)
     near_kept = kept
     blocks = (near, near_other, near_across, near_across_other)
-    kept, sent = run_expert(experts, blocks, z_and_zy, tok_rows, weights, also=sent)
+    kept, sent = run_expert(experts, blocks, z_and_zy, tok_rows, weights, sent)
     came = over_tp(sent)
     kinds = (shape((tok_rows, width), bf16), shape((tok_rows, width), f32))
     near_there, near_here = small_call(near_kernel, kinds, kept, near_kept, came)
@@ -338,7 +286,9 @@
         terms.append(over_ep(total, (2 * z, 2 * z)))
 
     out = shape((share, half), bf16)
-    stay, go = small_call(functools.partial(norm_kernel, len(terms)), (out, out), *terms, own, *affine, *affine_other)
+    stay, go = small_call(
+        functools.partial(norm_kernel, len(terms)), (out, out), *terms, own, *affine, *affine_other
+    )
     came = over_tp(go)
     first = lax.axis_index("tp") == 0
     return jnp.concatenate([jnp.where(first, stay, came), jnp.where(first, came, stay)], axis=0)

time: 60 us -> 59.9 us (level)
  waiting for transfers between devices: 26.2 us -> 28.1 us
  starting transfers between devices: 24.9 us -> 23.1 us
    ppermute x12, waiting for transfers between devices: 24.1 us -> 26.1 us  [over_ep(): return lax.ppermute(x, ('ep', 'tp'), pairs)]
    ppermute x12, starting transfers between devices: 22.6 us -> 21.2 us  [over_ep(): return lax.ppermute(x, ('ep', 'tp'), pairs)]
  transfers between devices with their start and end apart: 24 -> 24, of which waited for: 11 -> 12; matrix products, arithmetic and copies ran while one was open for 0% -> 0% of each run, Pallas kernels for 11% -> 10%
where the time goes in v5:
time: 59.9 us; the launch traced here: 59.7 us
  waiting for transfers between devices  28.1 us (47%)
  starting transfers between devices  23.1 us (39%)
  Pallas kernels  7.63 us (13%)
  other arithmetic  0.68 us (1%)
    ppermute x12, waiting for transfers between devices, over_ep(): return lax.ppermute(x, ('ep', 'tp'), pairs)  26.1 us
    ppermute x12, starting transfers between devices, over_ep(): return lax.ppermute(x, ('ep', 'tp'), pairs)  21.2 us
    pallas_call x4, Pallas kernels, run_expert(): pl.pallas_call(functools.partial(expert_kernel, experts, width, arrange,...  5.86 us
    ppermute x12, waiting for transfers between devices, over_tp(): return lax.ppermute(x, 'tp', pairs)  2.08 us
    ppermute x12, starting transfers between devices, over_tp(): return lax.ppermute(x, 'tp', pairs)  1.94 us
  transfers between devices with their start and end apart: 24, of which 12 were waited for; matrix products, arithmetic and copies ran while one was open for 0% of the time, Pallas kernels for 10%

profile of v5, /device:TPU:0, one launch (start us, length us, event | category | flops | bytes accessed | tf_op | source)
XLA Modules:
  0.0 59.7 jit_solution(3120950697801337164)
XLA Ops:
  0.0 1.2 %rows.1 = (bf16[64,2176]{1,0:T(8,128)(2,1)S(1)}, bf16[32,2176]{1,0:T(8,128)(2,1)S(1)}) custom-call(bf16[64,2048]{1,0:T(8,128)(2,1)} %tokens_hbm.1, s32[4,64]{1,0:T(4,128)} %bitcast.23, f32[4,64]{1,0:T(4,128)} %bitcast.24), custom_call_target="tpu_custom_call" | custom-call | flops 17179869184 | bytes 1048576 | tf_op jit(solution)/shard_map/rows/pallas_call | solution.py:242
  1.2 3.1 %collective-permute-start = (bf16[64,2176]{1,0:T(8,128)(2,1)S(1)}, bf16[64,2176]{1,0:T(8,128)(2,1)S(1)}, u32[]{:S(2)}, u32[]{:S(2)}) collective-permute-start(bf16[64,2176]{1,0:T(8,128)(2,1)S(1)} %get-tuple-element.25.refs_0_), channel_id=1, source_target_pairs={{0,2},{1,5},{2,0},{3,7},{4,6},{5,1},{6,4},{7,3},{8,10},{9,13},{10,... | collective-permute-start | bytes 835592 | tf_op jit(solution)/shard_map/ppermute | solution.py:235
  4.3 4.5 %collective-permute-done.refs_1_.refs_0_ = bf16[64,2176]{1,0:T(8,128)(2,1)S(1)} collective-permute-done((bf16[64,2176]{1,0:T(8,128)(2,1)S(1)}, bf16[64,2176]{1,0:T(8,128)(2,1)S(1)}, u32[]{:S(2)}, u32[]{:S(2)}) %collective-permute-start) | collective-permute-done | bytes 278560 | tf_op jit(solution)/shard_map/ppermute | solution.py:235
  8.8 3.0 %collective-permute-start.2 = (bf16[32,2176]{1,0:T(8,128)(2,1)S(1)}, bf16[32,2176]{1,0:T(8,128)(2,1)S(1)}, u32[]{:S(2)}, u32[]{:S(2)}) collective-permute-start(bf16[32,2176]{1,0:T(8,128)(2,1)S(1)} %get-tuple-element.26.refs_4_), channel_id=1, source_target_pairs={{0,6},{1,7},{2,4},{3,5},{4,2},{5,3},{6,0},{7,1},{8,14},{9,15},{10,... | collective-permute-start | bytes 417800 | tf_op jit(solution)/shard_map/ppermute | solution.py:235
  11.8 2.5 %collective-permute-start.7 = (bf16[32,2176]{1,0:T(8,128)(2,1)S(1)}, bf16[32,2176]{1,0:T(8,128)(2,1)S(1)}, u32[]{:S(2)}, u32[]{:S(2)}) collective-permute-start(bf16[32,2176]{1,0:T(8,128)(2,1)S(1)} %get-tuple-element.26.refs_4_), channel_id=1, source_target_pairs={{0,12},{1,13},{2,14},{3,15},{4,8},{5,9},{6,10},{7,11},{8,4},{9,5},... | collective-permute-start | bytes 417800 | tf_op jit(solution)/shard_map/ppermute | solution.py:235
  14.3 1.9 %collective-permute-done.2.refs_2_ = bf16[32,2176]{1,0:T(8,128)(2,1)S(1)} collective-permute-done((bf16[32,2176]{1,0:T(8,128)(2,1)S(1)}, bf16[32,2176]{1,0:T(8,128)(2,1)S(1)}, u32[]{:S(2)}, u32[]{:S(2)}) %collective-permute-start.2) | collective-permute-done | bytes 139296 | tf_op jit(solution)/shard_map/ppermute | solution.py:235
  16.2 3.2 %collective-permute-start.14 = (bf16[32,2176]{1,0:T(8,128)(2,1)S(1)}, bf16[32,2176]{1,0:T(8,128)(2,1)S(1)}, u32[]{:S(2)}, u32[]{:S(2)}) collective-permute-start(bf16[32,2176]{1,0:T(8,128)(2,1)S(1)} %get-tuple-element.26.refs_4_), channel_id=1, source_target_pairs={{0,8},{1,9},{2,10},{3,11},{4,12},{5,13},{6,14},{7,15},{8,0},{9,1},... | collective-permute-start | bytes 417800 | tf_op jit(solution)/shard_map/ppermute | solution.py:235
  19.3 2.1 %collective-permute-done.7.refs_0_ = bf16[32,2176]{1,0:T(8,128)(2,1)S(1)} collective-permute-done((bf16[32,2176]{1,0:T(8,128)(2,1)S(1)}, bf16[32,2176]{1,0:T(8,128)(2,1)S(1)}, u32[]{:S(2)}, u32[]{:S(2)}) %collective-permute-start.7) | collective-permute-done | bytes 139296 | tf_op jit(solution)/shard_map/ppermute | solution.py:235
  22.0 1.5 %expert.4 = (f32[64,2048]{1,0:T(8,128)S(1)}, bf16[64,2048]{1,0:T(8,128)(2,1)S(1)}) custom-call(bf16[64,2176]{1,0:T(8,128)(2,1)S(1)} %get-tuple-element.25.refs_0_, bf16[64,2176]{1,0:T(8,128)(2,1)S(1)} %collective-permute-done.refs_1_.refs_0_, bf16[64,2176]{1,0:T(8,128)(2,1)S(1)} %collective-permute-done.1.refs_2_.refs_1_, bf16[2048,640]{1,0:T(8,128)(2,1)S(1)} %bitcast.7, ...), custom_call_target="tpu_custom_call" | custom-call | flops 1006632960 | bytes 8388608 | tf_op jit(solution)/shard_map/expert/pallas_call | solution.py:144
  23.4 1.5 %expert.5 = (f32[64,2048]{1,0:T(8,128)S(1)}, bf16[128,2048]{1,0:T(8,128)(2,1)S(1)}) custom-call(bf16[64,2176]{1,0:T(8,128)(2,1)S(1)} %collective-permute-done.refs_1_.refs_0_, bf16[64,2176]{1,0:T(8,128)(2,1)S(1)} %collective-permute-done.1.refs_2_.refs_1_, bf16[32,2176]{1,0:T(8,128)(2,1)S(1)} %collective-permute-done.2.refs_2_, ...), custom_call_target="tpu_custom_call" | custom-call | flops 1006632960 | bytes 8388608 | tf_op jit(solution)/shard_map/expert/pallas_call | solution.py:144
  25.0 2.4 %collective-permute-done.14.refs_0_ = bf16[32,2176]{1,0:T(8,128)(2,1)S(1)} collective-permute-done((bf16[32,2176]{1,0:T(8,128)(2,1)S(1)}, bf16[32,2176]{1,0:T(8,128)(2,1)S(1)}, u32[]{:S(2)}, u32[]{:S(2)}) %collective-permute-start.14) | collective-permute-done | bytes 139296 | tf_op jit(solution)/shard_map/ppermute | solution.py:235
  28.0 5.1 %collective-permute-done.15.refs_1_ = bf16[32,2176]{1,0:T(8,128)(2,1)S(1)} collective-permute-done((bf16[32,2176]{1,0:T(8,128)(2,1)S(1)}, bf16[32,2176]{1,0:T(8,128)(2,1)S(1)}, u32[]{:S(2)}, u32[]{:S(2)}) %collective-permute-start.15) | collective-permute-done | bytes 139296 | tf_op jit(solution)/shard_map/ppermute | solution.py:235
  33.1 1.5 %expert.6 = (f32[64,2048]{1,0:T(8,128)S(1)}, bf16[64,2048]{1,0:T(8,128)(2,1)S(1)}) custom-call(bf16[32,2176]{1,0:T(8,128)(2,1)S(1)} %collective-permute-done.7.refs_0_, bf16[32,2176]{1,0:T(8,128)(2,1)S(1)} %collective-permute-done.8.refs_1_, bf16[32,2176]{1,0:T(8,128)(2,1)S(1)} %collective-permute-done.9.refs_2_, ...), custom_call_target="tpu_custom_call" | custom-call | flops 1006632960 | bytes 8388608 | tf_op jit(solution)/shard_map/expert/pallas_call | solution.py:144
  35.2 1.5 %expert.7 = (f32[64,2048]{1,0:T(8,128)S(1)}, bf16[64,2048]{1,0:T(8,128)(2,1)S(1)}) custom-call(bf16[32,2176]{1,0:T(8,128)(2,1)S(1)} %collective-permute-done.14.refs_0_, bf16[32,2176]{1,0:T(8,128)(2,1)S(1)} %collective-permute-done.15.refs_1_, bf16[32,2176]{1,0:T(8,128)(2,1)S(1)} %collective-permute-done.16.refs_2_, ...), custom_call_target="tpu_custom_call" | custom-call | flops 1006632960 | bytes 8388608 | tf_op jit(solution)/shard_map/expert/pallas_call | solution.py:144
  36.9 1.0 %collective-permute-start.5 = (bf16[64,2048]{1,0:T(8,128)(2,1)S(1)}, bf16[64,2048]{1,0:T(8,128)(2,1)S(1)}, u32[]{:S(2)}, u32[]{:S(2)}) collective-permute-start(bf16[64,2048]{1,0:T(8,128)(2,1)S(1)} %get-tuple-element.32), channel_id=1, source_target_pairs={{0,4},{1,5},{2,6},{3,7},{4,0},{5,1},{6,2},{7,3},{8,12},{9,13},{10,... | collective-permute-start | bytes 786440 | tf_op jit(solution)/shard_map/ppermute | solution.py:235
  37.9 0.8 %collective-permute-start.12 = (bf16[32,2048]{1,0:T(8,128)(2,1)S(1)}, bf16[32,2048]{1,0:T(8,128)(2,1)S(1)}, u32[]{:S(2)}, u32[]{:S(2)}) collective-permute-start(bf16[32,2048]{1,0:T(8,128)(2,1)S(1)} %get-tuple-element.38), channel_id=1, source_target_pairs={{0,2},{1,3},{2,0},{3,1},{4,6},{5,7},{6,4},{7,5},{8,10},{9,11},{10,... | collective-permute-start | bytes 393224 | tf_op jit(solution)/shard_map/ppermute | solution.py:235
  38.8 1.3 %collective-permute-start.19 = (bf16[32,2048]{1,0:T(8,128)(2,1)S(1)}, bf16[32,2048]{1,0:T(8,128)(2,1)S(1)}, u32[]{:S(2)}, u32[]{:S(2)}) collective-permute-start(bf16[32,2048]{1,0:T(8,128)(2,1)S(1)} %get-tuple-element.42), channel_id=1, source_target_pairs={{0,2},{1,3},{2,0},{3,1},{4,6},{5,7},{6,4},{7,5},{8,10},{9,11},{10,... | collective-permute-start | bytes 393224 | tf_op jit(solution)/shard_map/ppermute | solution.py:235
  40.1 4.2 %collective-permute-done.12.refs_1_ = bf16[32,2048]{1,0:T(8,128)(2,1)S(1)} collective-permute-done((bf16[32,2048]{1,0:T(8,128)(2,1)S(1)}, bf16[32,2048]{1,0:T(8,128)(2,1)S(1)}, u32[]{:S(2)}, u32[]{:S(2)}) %collective-permute-start.12) | collective-permute-done | bytes 131104 | tf_op jit(solution)/shard_map/ppermute | solution.py:235
  44.4 1.8 %collective-permute-start.13 = (bf16[32,2048]{1,0:T(8,128)(2,1)S(1)}, bf16[32,2048]{1,0:T(8,128)(2,1)S(1)}, u32[]{:S(2)}, u32[]{:S(2)}) collective-permute-start(bf16[32,2048]{1,0:T(8,128)(2,1)S(1)} %shard_map.85), channel_id=1, source_target_pairs={{0,12},{1,13},{2,14},{3,15},{4,8},{5,9},{6,10},{7,11},{8,4},{9,5},... | collective-permute-start | bytes 393224 | tf_op jit(solution)/shard_map/ppermute | solution.py:235
  46.4 2.3 %collective-permute-start.20 = (bf16[32,2048]{1,0:T(8,128)(2,1)S(1)}, bf16[32,2048]{1,0:T(8,128)(2,1)S(1)}, u32[]{:S(2)}, u32[]{:S(2)}) collective-permute-start(bf16[32,2048]{1,0:T(8,128)(2,1)S(1)} %shard_map.87), channel_id=1, source_target_pairs={{0,8},{1,9},{2,10},{3,11},{4,12},{5,13},{6,14},{7,15},{8,0},{9,1},... | collective-permute-start | bytes 393224 | tf_op jit(solution)/shard_map/ppermute | solution.py:235
  48.8 1.6 %collective-permute-start.6 = (bf16[32,2048]{1,0:T(8,128)(2,1)S(1)}, bf16[32,2048]{1,0:T(8,128)(2,1)S(1)}, u32[]{:S(2)}, u32[]{:S(2)}) collective-permute-start(bf16[32,2048]{1,0:T(8,128)(2,1)S(1)} %get-tuple-element.34), channel_id=1, source_target_pairs={{0,2},{1,3},{2,0},{3,1},{4,6},{5,7},{6,4},{7,5},{8,10},{9,11},{10,... | collective-permute-start | bytes 393224 | tf_op jit(solution)/shard_map/ppermute | solution.py:235
  51.8 0.9 %collective-permute-done.13.refs_2_ = bf16[32,2048]{1,0:T(8,128)(2,1)S(1)} collective-permute-done((bf16[32,2048]{1,0:T(8,128)(2,1)S(1)}, bf16[32,2048]{1,0:T(8,128)(2,1)S(1)}, u32[]{:S(2)}, u32[]{:S(2)}) %collective-permute-start.13) | collective-permute-done | bytes 131104 | tf_op jit(solution)/shard_map/ppermute | solution.py:235
  52.7 4.7 %collective-permute-done.20.refs_3_ = bf16[32,2048]{1,0:T(8,128)(2,1)S(1)} collective-permute-done((bf16[32,2048]{1,0:T(8,128)(2,1)S(1)}, bf16[32,2048]{1,0:T(8,128)(2,1)S(1)}, u32[]{:S(2)}, u32[]{:S(2)}) %collective-permute-start.20) | collective-permute-done | bytes 131104 | tf_op jit(solution)/shard_map/ppermute | solution.py:235
  57.8 1.2 %collective-permute-done.23 = bf16[32,1024]{1,0:T(8,128)(2,1)S(1)} collective-permute-done((bf16[32,1024]{1,0:T(8,128)(2,1)S(1)}, bf16[32,1024]{1,0:T(8,128)(2,1)S(1)}, u32[]{:S(2)}, u32[]{:S(2)}) %collective-permute-start.23) | collective-permute-done | bytes 65568 | tf_op jit(solution)/shard_map/ppermute | solution.py:238
  (48 shorter events, 4.8 us)
Async XLA Ops:
  1.2 7.6 %collective-permute-start = (bf16[64,2176]{1,0:T(8,128)(2,1)S(1)}, bf16[64,2176]{1,0:T(8,128)(2,1)S(1)}, u32[]{:S(2)}, u32[]{:S(2)}) collective-permute-start(bf16[64,2176]{1,0:T(8,128)(2,1)S(1)} %get-tuple-element.25.refs_0_), channel_id=1, source_target_pairs={{0,2},{1,5},{2,0},{3,7},{4,6},{5,1},{6,4},{7,3},{8,10},{9,13},{10,... | collective-permute-start | bytes 835592 | tf_op jit(solution)/shard_map/ppermute | solution.py:235
  8.8 13.2 %collective-permute-start.1 = (bf16[64,2176]{1,0:T(8,128)(2,1)S(1)}, bf16[64,2176]{1,0:T(8,128)(2,1)S(1)}, u32[]{:S(2)}, u32[]{:S(2)}) collective-permute-start(bf16[64,2176]{1,0:T(8,128)(2,1)S(1)} %collective-permute-done.refs_1_.refs_0_), channel_id=1, source_target_pairs={{0,1},{1,0},{2,3},{3,2},{4,5},{5,4},{6,7},{7,6},{8,9},{9,8},{10,11... | collective-permute-start | bytes 835592 | tf_op jit(solution)/shard_map/ppermute | solution.py:238
  8.8 7.4 %collective-permute-start.2 = (bf16[32,2176]{1,0:T(8,128)(2,1)S(1)}, bf16[32,2176]{1,0:T(8,128)(2,1)S(1)}, u32[]{:S(2)}, u32[]{:S(2)}) collective-permute-start(bf16[32,2176]{1,0:T(8,128)(2,1)S(1)} %get-tuple-element.26.refs_4_), channel_id=1, source_target_pairs={{0,6},{1,7},{2,4},{3,5},{4,2},{5,3},{6,0},{7,1},{8,14},{9,15},{10,... | collective-permute-start | bytes 417800 | tf_op jit(solution)/shard_map/ppermute | solution.py:235
  11.8 9.6 %collective-permute-start.7 = (bf16[32,2176]{1,0:T(8,128)(2,1)S(1)}, bf16[32,2176]{1,0:T(8,128)(2,1)S(1)}, u32[]{:S(2)}, u32[]{:S(2)}) collective-permute-start(bf16[32,2176]{1,0:T(8,128)(2,1)S(1)} %get-tuple-element.26.refs_4_), channel_id=1, source_target_pairs={{0,12},{1,13},{2,14},{3,15},{4,8},{5,9},{6,10},{7,11},{8,4},{9,5},... | collective-permute-start | bytes 417800 | tf_op jit(solution)/shard_map/ppermute | solution.py:235
  16.2 7.3 %collective-permute-start.3 = (bf16[32,2176]{1,0:T(8,128)(2,1)S(1)}, bf16[32,2176]{1,0:T(8,128)(2,1)S(1)}, u32[]{:S(2)}, u32[]{:S(2)}) collective-permute-start(bf16[32,2176]{1,0:T(8,128)(2,1)S(1)} %collective-permute-done.2.refs_2_), channel_id=1, source_target_pairs={{0,1},{1,0},{2,3},{3,2},{4,5},{5,4},{6,7},{7,6},{8,9},{9,8},{10,11... | collective-permute-start | bytes 417800 | tf_op jit(solution)/shard_map/ppermute | solution.py:238
  16.2 11.3 %collective-permute-start.14 = (bf16[32,2176]{1,0:T(8,128)(2,1)S(1)}, bf16[32,2176]{1,0:T(8,128)(2,1)S(1)}, u32[]{:S(2)}, u32[]{:S(2)}) collective-permute-start(bf16[32,2176]{1,0:T(8,128)(2,1)S(1)} %get-tuple-element.26.refs_4_), channel_id=1, source_target_pairs={{0,8},{1,9},{2,10},{3,11},{4,12},{5,13},{6,14},{7,15},{8,0},{9,1},... | collective-permute-start | bytes 417800 | tf_op jit(solution)/shard_map/ppermute | solution.py:235
  21.4 6.1 %collective-permute-start.8 = (bf16[32,2176]{1,0:T(8,128)(2,1)S(1)}, bf16[32,2176]{1,0:T(8,128)(2,1)S(1)}, u32[]{:S(2)}, u32[]{:S(2)}) collective-permute-start(bf16[32,2176]{1,0:T(8,128)(2,1)S(1)} %collective-permute-done.7.refs_0_), channel_id=1, source_target_pairs={{0,2},{1,3},{2,0},{3,1},{4,6},{5,7},{6,4},{7,5},{8,10},{9,11},{10,... | collective-permute-start | bytes 417800 | tf_op jit(solution)/shard_map/ppermute | solution.py:235
  24.9 11.9 %collective-permute-start.4 = (bf16[128,2048]{1,0:T(8,128)(2,1)S(1)}, bf16[128,2048]{1,0:T(8,128)(2,1)S(1)}, u32[]{:S(2)}, u32[]{:S(2)}) collective-permute-start(bf16[128,2048]{1,0:T(8,128)(2,1)S(1)} %get-tuple-element.30), channel_id=1, source_target_pairs={{0,1},{1,0},{2,3},{3,2},{4,5},{5,4},{6,7},{7,6},{8,9},{9,8},{10,11... | collective-permute-start | bytes 1572872 | tf_op jit(solution)/shard_map/ppermute | solution.py:238
  27.4 5.7 %collective-permute-start.15 = (bf16[32,2176]{1,0:T(8,128)(2,1)S(1)}, bf16[32,2176]{1,0:T(8,128)(2,1)S(1)}, u32[]{:S(2)}, u32[]{:S(2)}) collective-permute-start(bf16[32,2176]{1,0:T(8,128)(2,1)S(1)} %collective-permute-done.14.refs_0_), channel_id=1, source_target_pairs={{0,2},{1,3},{2,0},{3,1},{4,6},{5,7},{6,4},{7,5},{8,10},{9,11},{10,... | collective-permute-start | bytes 417800 | tf_op jit(solution)/shard_map/ppermute | solution.py:235
  27.4 5.7 %collective-permute-start.9 = (bf16[32,2176]{1,0:T(8,128)(2,1)S(1)}, bf16[32,2176]{1,0:T(8,128)(2,1)S(1)}, u32[]{:S(2)}, u32[]{:S(2)}) collective-permute-start(bf16[32,2176]{1,0:T(8,128)(2,1)S(1)} %collective-permute-done.7.refs_0_), channel_id=1, source_target_pairs={{0,1},{1,0},{2,3},{3,2},{4,5},{5,4},{6,7},{7,6},{8,9},{9,8},{10,11... | collective-permute-start | bytes 417800 | tf_op jit(solution)/shard_map/ppermute | solution.py:238
  27.5 5.6 %collective-permute-start.10 = (bf16[32,2176]{1,0:T(8,128)(2,1)S(1)}, bf16[32,2176]{1,0:T(8,128)(2,1)S(1)}, u32[]{:S(2)}, u32[]{:S(2)}) collective-permute-start(bf16[32,2176]{1,0:T(8,128)(2,1)S(1)} %collective-permute-done.8.refs_1_), channel_id=1, source_target_pairs={{0,1},{1,0},{2,3},{3,2},{4,5},{5,4},{6,7},{7,6},{8,9},{9,8},{10,11... | collective-permute-start | bytes 417800 | tf_op jit(solution)/shard_map/ppermute | solution.py:238
  28.0 7.2 %collective-permute-start.16 = (bf16[32,2176]{1,0:T(8,128)(2,1)S(1)}, bf16[32,2176]{1,0:T(8,128)(2,1)S(1)}, u32[]{:S(2)}, u32[]{:S(2)}) collective-permute-start(bf16[32,2176]{1,0:T(8,128)(2,1)S(1)} %collective-permute-done.14.refs_0_), channel_id=1, source_target_pairs={{0,1},{1,0},{2,3},{3,2},{4,5},{5,4},{6,7},{7,6},{8,9},{9,8},{10,11... | collective-permute-start | bytes 417800 | tf_op jit(solution)/shard_map/ppermute | solution.py:238
  33.1 2.1 %collective-permute-start.17 = (bf16[32,2176]{1,0:T(8,128)(2,1)S(1)}, bf16[32,2176]{1,0:T(8,128)(2,1)S(1)}, u32[]{:S(2)}, u32[]{:S(2)}) collective-permute-start(bf16[32,2176]{1,0:T(8,128)(2,1)S(1)} %collective-permute-done.15.refs_1_), channel_id=1, source_target_pairs={{0,1},{1,0},{2,3},{3,2},{4,5},{5,4},{6,7},{7,6},{8,9},{9,8},{10,11... | collective-permute-start | bytes 417800 | tf_op jit(solution)/shard_map/ppermute | solution.py:238
  34.6 3.3 %collective-permute-start.11 = (bf16[64,2048]{1,0:T(8,128)(2,1)S(1)}, bf16[64,2048]{1,0:T(8,128)(2,1)S(1)}, u32[]{:S(2)}, u32[]{:S(2)}) collective-permute-start(bf16[64,2048]{1,0:T(8,128)(2,1)S(1)} %get-tuple-element.36), channel_id=1, source_target_pairs={{0,1},{1,0},{2,3},{3,2},{4,5},{5,4},{6,7},{7,6},{8,9},{9,8},{10,11... | collective-permute-start | bytes 786440 | tf_op jit(solution)/shard_map/ppermute | solution.py:238
  36.7 2.1 %collective-permute-start.18 = (bf16[64,2048]{1,0:T(8,128)(2,1)S(1)}, bf16[64,2048]{1,0:T(8,128)(2,1)S(1)}, u32[]{:S(2)}, u32[]{:S(2)}) collective-permute-start(bf16[64,2048]{1,0:T(8,128)(2,1)S(1)} %get-tuple-element.40), channel_id=1, source_target_pairs={{0,1},{1,0},{2,3},{3,2},{4,5},{5,4},{6,7},{7,6},{8,9},{9,8},{10,11... | collective-permute-start | bytes 786440 | tf_op jit(solution)/shard_map/ppermute | solution.py:238
  36.9 11.9 %collective-permute-start.5 = (bf16[64,2048]{1,0:T(8,128)(2,1)S(1)}, bf16[64,2048]{1,0:T(8,128)(2,1)S(1)}, u32[]{:S(2)}, u32[]{:S(2)}) collective-permute-start(bf16[64,2048]{1,0:T(8,128)(2,1)S(1)} %get-tuple-element.32), channel_id=1, source_target_pairs={{0,4},{1,5},{2,6},{3,7},{4,0},{5,1},{6,2},{7,3},{8,12},{9,13},{10,... | collective-permute-start | bytes 786440 | tf_op jit(solution)/shard_map/ppermute | solution.py:235
  37.9 6.4 %collective-permute-start.12 = (bf16[32,2048]{1,0:T(8,128)(2,1)S(1)}, bf16[32,2048]{1,0:T(8,128)(2,1)S(1)}, u32[]{:S(2)}, u32[]{:S(2)}) collective-permute-start(bf16[32,2048]{1,0:T(8,128)(2,1)S(1)} %get-tuple-element.38), channel_id=1, source_target_pairs={{0,2},{1,3},{2,0},{3,1},{4,6},{5,7},{6,4},{7,5},{8,10},{9,11},{10,... | collective-permute-start | bytes 393224 | tf_op jit(solution)/shard_map/ppermute | solution.py:235
  38.8 7.6 %collective-permute-start.19 = (bf16[32,2048]{1,0:T(8,128)(2,1)S(1)}, bf16[32,2048]{1,0:T(8,128)(2,1)S(1)}, u32[]{:S(2)}, u32[]{:S(2)}) collective-permute-start(bf16[32,2048]{1,0:T(8,128)(2,1)S(1)} %get-tuple-element.42), channel_id=1, source_target_pairs={{0,2},{1,3},{2,0},{3,1},{4,6},{5,7},{6,4},{7,5},{8,10},{9,11},{10,... | collective-permute-start | bytes 393224 | tf_op jit(solution)/shard_map/ppermute | solution.py:235
  44.4 8.3 %collective-permute-start.13 = (bf16[32,2048]{1,0:T(8,128)(2,1)S(1)}, bf16[32,2048]{1,0:T(8,128)(2,1)S(1)}, u32[]{:S(2)}, u32[]{:S(2)}) collective-permute-start(bf16[32,2048]{1,0:T(8,128)(2,1)S(1)} %shard_map.85), channel_id=1, source_target_pairs={{0,12},{1,13},{2,14},{3,15},{4,8},{5,9},{6,10},{7,11},{8,4},{9,5},... | collective-permute-start | bytes 393224 | tf_op jit(solution)/shard_map/ppermute | solution.py:235
  46.4 11.0 %collective-permute-start.20 = (bf16[32,2048]{1,0:T(8,128)(2,1)S(1)}, bf16[32,2048]{1,0:T(8,128)(2,1)S(1)}, u32[]{:S(2)}, u32[]{:S(2)}) collective-permute-start(bf16[32,2048]{1,0:T(8,128)(2,1)S(1)} %shard_map.87), channel_id=1, source_target_pairs={{0,8},{1,9},{2,10},{3,11},{4,12},{5,13},{6,14},{7,15},{8,0},{9,1},... | collective-permute-start | bytes 393224 | tf_op jit(solution)/shard_map/ppermute | solution.py:235
  48.8 8.6 %collective-permute-start.6 = (bf16[32,2048]{1,0:T(8,128)(2,1)S(1)}, bf16[32,2048]{1,0:T(8,128)(2,1)S(1)}, u32[]{:S(2)}, u32[]{:S(2)}) collective-permute-start(bf16[32,2048]{1,0:T(8,128)(2,1)S(1)} %get-tuple-element.34), channel_id=1, source_target_pairs={{0,2},{1,3},{2,0},{3,1},{4,6},{5,7},{6,4},{7,5},{8,10},{9,11},{10,... | collective-permute-start | bytes 393224 | tf_op jit(solution)/shard_map/ppermute | solution.py:235
  50.4 1.2 %collective-permute-start.21 = (f32[1,1024]{1,0:T(1,128)S(1)}, f32[1,1024]{1,0:T(1,128)S(1)}, u32[]{:S(2)}, u32[]{:S(2)}) collective-permute-start(f32[1,1024]{1,0:T(1,128)S(1)} %bitcast.19), channel_id=1, source_target_pairs={{0,1},{1,0},{2,3},{3,2},{4,5},{5,4},{6,7},{7,6},{8,9},{9,8},{10,11... | collective-permute-start | bytes 12296 | tf_op jit(solution)/shard_map/ppermute | solution.py:238
  50.4 1.3 %collective-permute-start.22 = (f32[1,1024]{1,0:T(1,128)S(1)}, f32[1,1024]{1,0:T(1,128)S(1)}, u32[]{:S(2)}, u32[]{:S(2)}) collective-permute-start(f32[1,1024]{1,0:T(1,128)S(1)} %bitcast.21), channel_id=1, source_target_pairs={{0,1},{1,0},{2,3},{3,2},{4,5},{5,4},{6,7},{7,6},{8,9},{9,8},{10,11... | collective-permute-start | bytes 12296 | tf_op jit(solution)/shard_map/ppermute | solution.py:238
  57.7 1.3 %collective-permute-start.23 = (bf16[32,1024]{1,0:T(8,128)(2,1)S(1)}, bf16[32,1024]{1,0:T(8,128)(2,1)S(1)}, u32[]{:S(2)}, u32[]{:S(2)}) collective-permute-start(bf16[32,1024]{1,0:T(8,128)(2,1)S(1)} %get-tuple-element.44), channel_id=1, source_target_pairs={{0,1},{1,0},{2,3},{3,2},{4,5},{5,4},{6,7},{7,6},{8,9},{9,8},{10,11... | collective-permute-start | bytes 196616 | tf_op jit(solution)/shard_map/ppermute | solution.py:238
  (5 other events, 93.4 us)
